TPU v7x, 512 devices: a whole 4x4x16 slice. The times are simulated.
512 devices in a mesh: sp: 128 (over z, x, core), tp: 4 (over y).
Axes of the slice: x: 4, y: 4, z: 16, core: 2. Of those that a mesh axis runs over, the one named last changes fastest.
Arguments:
- value_rows: bfloat16 [131072, 1024], P('sp', 'tp'), may hold values from -6 to 6
- gate_rows: bfloat16 [131072, 1024], P('sp', 'tp'), may hold values from -6 to 6
- conv_taps: bfloat16 [31, 1024], P(None, 'tp'), may hold values from -1 to 1
- norm_gain: float32 [1024], P('tp'), may hold values from 0.1 to 1.9
- point_weight: bfloat16 [1024, 1024], P(None, 'tp'), may hold values from -0.1875 to 0.1875
- out_grad: bfloat16 [131072, 1024], P('sp', 'tp'), may hold values from -24 to 24
Outputs:
- value_grad: bfloat16 [131072, 1024], P('sp', 'tp')
- gate_grad: bfloat16 [131072, 1024], P('sp', 'tp')
- taps_grad: float32 [31, 1024], P(None, 'tp')
- gain_grad: float32 [1024], P('tp')
- weight_grad: float32 [1024, 1024], P('sp', 'tp')
All inputs are finite; a program needn't handle non-finite values.
Results may differ from a plain program's by a relative error of at most 0.0051.
Values may be sent and summed in bfloat16 or wider, within the bound.
No kernel may reach another device: no remote copies, remote signals or barrier semaphores. Data moves between devices by JAX's collectives and lax.ppermute only.
A program may use at most 128 MiB of HBM per device.

v0:
```python
import jax
import jax.numpy as jnp
from jax import lax
from jax.sharding import Mesh
from jax.sharding import PartitionSpec as P

GROUP = 64
SP = ("sp_0", "sp_1", "sp_2")


EPS = 1e-06


def extended(value, sides, width):
    for axis, dim in sides:
        peers, length = (lax.axis_size(axis), value.shape[dim])
        up = [(i, (i + 1) % peers) for i in range(peers - 1)]
        down = [(j, i) for i, j in up]
        last = lax.slice_in_dim(value, length - width, length, axis=dim)
        initial = lax.slice_in_dim(value, 0, width, axis=dim)
        before = lax.ppermute(last, axis, up)
        after = lax.ppermute(initial, axis, down)
        value = jnp.concatenate([before, value, after], axis=dim)
    return value


def from_everyone(value, axis):
    copies = jnp.broadcast_to(value, (lax.axis_size(axis), *value.shape))
    return lax.all_to_all(copies, axis, split_axis=0, concat_axis=0, tiled=True)


def in_order(blocks, dim):
    blocks = jnp.moveaxis(blocks, 0, dim)
    lengths = blocks.shape
    return blocks.reshape(*lengths[:dim], lengths[dim] * lengths[dim + 1], *lengths[dim + 2 :])


def gather_directly(value, axis, dim):
    blocks = from_everyone(value, axis)
    return in_order(blocks, dim)


def cut_along(value, dim, peers):
    lengths = value.shape
    blocks = value.reshape(*lengths[:dim], peers, lengths[dim] // peers, *lengths[dim + 1 :])
    return jnp.moveaxis(blocks, dim, 0)


def sent_and_summed(value, axis, dim):
    peers = lax.axis_size(axis)
    blocks = lax.all_to_all(cut_along(value, dim, peers), axis, 0, 0, tiled=True)
    return jnp.sum(blocks, axis=0)


def summed_rows(value, axes, dim):
    far, near = axes
    own = sent_and_summed(cut_along(value, dim, lax.axis_size(far)), near, dim + 1)
    return jnp.sum(lax.all_to_all(own, far, 0, 0, tiled=True), axis=0)


def filled_up(lines, peers):
    spare = -lines.shape[0] % peers
    if not spare:
        return lines
    return jnp.concatenate([lines, jnp.zeros((spare, *lines.shape[1:]), lines.dtype)])


def gather_axes(value, axes, dim):
    far, near = axes
    initial = from_everyone(value, far)
    blocks = jnp.swapaxes(from_everyone(initial, near), 0, 1)
    return in_order(blocks.reshape(-1, *value.shape), dim)


def nested_sum(value, axes):
    own = summed_rows(filled_up(value, lax.axis_size(axes[0]) * lax.axis_size(axes[1])), axes, 0)
    whole = gather_axes(own, axes, 0)
    return whole[: len(value)].reshape(value.shape)


def together(arrays, axis):
    vector, at, gathered = (jnp.concatenate([a.reshape(-1) for a in arrays]), 0, [])
    total = nested_sum(vector, axis)
    for a in arrays:
        gathered.append(total[at : at + a.size].reshape(a.shape))
        at += a.size
    return tuple(gathered)


def per_device(value_rows, gate_rows, conv_taps, norm_gain, point_weight, out_grad):
    row_count = value_rows.shape[0]
    chan_count = value_rows.shape[1]
    tap_count = conv_taps.shape[0]
    half_width = tap_count // 2
    groups = chan_count // GROUP
    gate_sig = jax.nn.sigmoid(gate_rows.astype(jnp.float32))
    value_f = value_rows.astype(jnp.float32)
    gated = (value_f * gate_sig).astype(jnp.bfloat16)
    margin = 0
    gated_wide = extended(gated, ((SP, 0),), half_width)
    extent = row_count + 2 * margin
    taps_f = conv_taps.astype(jnp.float32)
    convolved = jnp.zeros((extent, chan_count), jnp.float32)
    for tap_index in range(tap_count):
        convolved = convolved + taps_f[tap_index] * gated_wide[
            tap_index : tap_index + extent
        ].astype(jnp.float32)
    grouped = convolved.reshape(extent, groups, GROUP)
    group_mean = jnp.mean(grouped, axis=-1, keepdims=True)
    centred = grouped - group_mean
    inv_std = lax.rsqrt(jnp.mean(centred * centred, axis=-1, keepdims=True) + EPS)
    unit_conv = centred * inv_std
    gain_g = norm_gain.reshape(groups, GROUP)
    pre_act = unit_conv * gain_g
    act_sig = jax.nn.sigmoid(pre_act)
    normed = (pre_act * act_sig).astype(jnp.bfloat16).reshape(extent, chan_count)
    full_grad = gather_directly(out_grad, "tp", 1)
    normed_grad = jnp.dot(full_grad, point_weight, preferred_element_type=jnp.float32).reshape(
        extent, groups, GROUP
    )
    weight_grad = summed_rows(
        lax.dot_general(
            full_grad, normed, (((0,), (0,)), ((), ())), preferred_element_type=jnp.float32
        ),
        (("sp_0", "sp_1"), "sp_2"),
        0,
    )
    act_grad = normed_grad * act_sig * (1.0 + pre_act * (1.0 - act_sig))
    gain_part = jnp.sum(act_grad * unit_conv, axis=0).reshape(chan_count)
    hat_grad = act_grad * gain_g
    conv_grad = inv_std * (
        hat_grad
        - jnp.mean(hat_grad, axis=-1, keepdims=True)
        - unit_conv * jnp.mean(hat_grad * unit_conv, axis=-1, keepdims=True)
    )
    conv_grad = conv_grad.reshape(extent, chan_count)
    grad_wide = extended(conv_grad, ((SP, 0),), half_width)
    taps_part = jnp.stack(
        [
            jnp.sum(
                conv_grad
                * gated_wide[margin + tap_index : margin + tap_index + row_count].astype(
                    jnp.float32
                ),
                axis=0,
            )
            for tap_index in range(tap_count)
        ]
    )
    taps_grad, gain_grad = together((taps_part, gain_part), (("sp_0", "sp_1"), "sp_2"))
    gated_grad = jnp.zeros((row_count, chan_count), jnp.float32)
    for tap_index in range(tap_count):
        lower = 2 * half_width - tap_index
        gated_grad = gated_grad + taps_f[tap_index] * grad_wide[lower : lower + row_count]
    value_grad = (gated_grad * gate_sig).astype(jnp.bfloat16)
    gate_grad = (gated_grad * value_f * gate_sig * (1.0 - gate_sig)).astype(jnp.bfloat16)
    return (value_grad, gate_grad, taps_grad, gain_grad, weight_grad)


def solution(mesh):
    finer = Mesh(mesh.devices.reshape(16, 4, 2, mesh.shape["tp"]), ("sp_0", "sp_1", "sp_2", "tp"))
    return jax.shard_map(
        per_device,
        mesh=finer,
        in_specs=(P(SP, "tp"), P(SP, "tp"), P(None, "tp"), P("tp"), P(None, "tp"), P(SP, "tp")),
        out_specs=(P(SP, "tp"), P(SP, "tp"), P(None, "tp"), P("tp"), P(SP, "tp")),
        check_vma=False,
    )
```

profile of v0, /device:TPU:96, one launch (start us, length us, event | category | flops | bytes accessed | tf_op | source)
XLA Modules:
  0.0 169.3 jit_solution(9547722019708035228)
XLA Ops:
  0.6 2.5 %broadcast_in_dim.6 = bf16[4,1024,256]{2,1,0:T(8,128)(2,1)} broadcast(bf16[1024,256]{1,0:T(8,128)(2,1)} %param.11), dimensions={1,2} | broadcast | bytes 2621440 | tf_op jit(solution)/shard_map/broadcast_in_dim | solution.py:28
  3.1 4.6 %all-to-all-start = ((bf16[4,1024,256]{2,1,0:T(8,128)(2,1)}), bf16[4,1024,256]{2,1,0:T(8,128)(2,1)}, u32[]{:S(2)}, u32[]{:S(2)}) async-start(bf16[4,1024,256]{2,1,0:T(8,128)(2,1)} %broadcast_in_dim.6), calls=%async_computation | async-start | bytes 4194304 | tf_op jit(solution)/shard_map/all_to_all | solution.py:29
  8.0 3.7 %collective-permute-start.1 = (bf16[15,256]{1,0:T(8,128)(2,1)S(1)}, bf16[15,256]{1,0:T(8,128)(2,1)S(1)}, u32[]{:S(2)}, u32[]{:S(2)}) collective-permute-start(bf16[15,256]{1,0:T(8,128)(2,1)S(1)} %get-tuple-element.47), channel_id=1, source_target_pairs={{4,0},{8,4},{12,8},{16,12},{20,16},{24,20},{28,24},{32,28},{36,32}... | collective-permute-start | bytes 23048 | tf_op jit(solution)/shard_map/ppermute | solution.py:22
  14.8 4.0 %collective-permute-done = bf16[15,256]{1,0:T(8,128)(2,1)S(1)} collective-permute-done((bf16[15,256]{1,0:T(8,128)(2,1)S(1)}, bf16[15,256]{1,0:T(8,128)(2,1)S(1)}, u32[]{:S(2)}, u32[]{:S(2)}) %collective-permute-start) | collective-permute-done | bytes 7712 | tf_op jit(solution)/shard_map/ppermute | solution.py:21
  18.8 6.6 %fusion.60 = f32[1024,256]{1,0:T(8,128)S(1)} fusion(bf16[1024,256]{1,0:T(8,128)(2,1)S(1)} %fusion.1, bf16[15,256]{1,0:T(8,128)(2,1)S(1)} %collective-permute-done.1, bf16[15,256]{1,0:T(8,128)(2,1)S(1)} %collective-permute-done, f32[256]{0:T(256)S(1)} %bitcast.169, f32[256]{0:T(256)S(1)} %bitcast.167, f32[256]{0:T(256)S(1)} %bitcast.165, ...), kind=kLoop, calls=%fused_computation.182 | loop fusion | flops 47710208 | bytes 1619968 | tf_op jit(solution)/shard_map/add | solution.py:105
  29.4 4.9 %all-to-all-done = bf16[4,1024,256]{2,1,0:T(8,128)(2,1)} async-done(((bf16[4,1024,256]{2,1,0:T(8,128)(2,1)}), bf16[4,1024,256]{2,1,0:T(8,128)(2,1)}, u32[]{:S(2)}, u32[]{:S(2)}) %all-to-all-start) | async-done | bytes 2097184 | tf_op jit(solution)/shard_map/all_to_all | solution.py:29
  34.4 4.5 %copy.182 = bf16[1024,4,256]{2,1,0:T(4,128)(2,1)} copy(bf16[1024,4,256]{2,0,1:T(8,128)(2,1)} %bitcast.32) | data formatting | bytes 4194304 | tf_op jit(solution)/shard_map/transpose | solution.py:33
  38.9 4.5 %reshape.73 = bf16[1024,1024,1]{1,0,2:T(8,128)(2,1)} reshape(bf16[1024,4,256]{2,1,0:T(4,128)(2,1)} %copy.182) | data formatting | bytes 4194304 | tf_op jit(solution)/shard_map/reshape | solution.py:35
  43.4 2.9 %multiply_reduce_fusion = (f32[4,64]{1,0:T(4,128)S(1)}, f32[1024,4]{0,1:T(4,128)S(1)}, f32[1024,4]{0,1:T(4,128)S(1)}, f32[1024,4,64]{0,2,1:T(8,128)S(1)}) fusion(f32[4,64]{1,0:T(4,128)S(1)} %mul.771, bf16[1024,1024,1]{1,0,2:T(8,128)(2,1)} %reshape.73, bf16[4,64,1024]{2,1,0:T(8,128)(2,1)S(1)} %bitcast.102, f32[1024,4]{0,1:T(4,128)S(1)} %add_rsqrt_fusion, ...), kind=kOutput, calls=%fused_computation.302 | convolution fusion | flops 541318912 | bytes 4786176 | tf_op jit(solution)/shard_map/dot_general | solution.py:118
  52.6 3.7 %all_to_all.43 = f32[2,1,4096]{2,1,0:T(1,128)S(1)} all-to-all(f32[2,1,4096]{2,1,0:T(1,128)S(1)} %reshape.75), channel_id=1, replica_groups=mesh['sp_0'=16,'sp_1'=4,'sp_2'=2,'tp'=4] {'sp_2'}, dimensions={0} | all-to-all | bytes 65536 | tf_op jit(solution)/shard_map/all_to_all | solution.py:51
  58.3 17.3 %all-to-all-start.2 = ((f32[64,1,64]{2,1,0:T(1,128)}), f32[64,1,64]{2,1,0:T(1,128)S(1)}, u32[]{:S(2)}, u32[]{:S(2)}) async-start(f32[64,1,64]{2,1,0:T(1,128)} %bitcast.70), calls=%async_computation.2 | async-start | bytes 65536 | tf_op jit(solution)/shard_map/all_to_all | solution.py:58
  80.0 2.5 %copy.225 = f32[1024,256]{1,0:T(8,128)} copy(f32[1024,256]{0,1:T(8,128)} %convolution_bitcast_fusion) | data formatting | bytes 2097152 | tf_op jit(solution)/shard_map/dot_general | solution.py:122
  82.5 2.3 %copy.226 = f32[2,64,8,256]{3,2,1,0:T(8,128)} copy(f32[2,64,8,256]{3,2,0,1:T(8,128)} %bitcast.98) | data formatting | bytes 2097152 | tf_op jit(solution)/shard_map/transpose | solution.py:46
  84.9 2.7 %all-to-all-done.2 = f32[64,1,64]{2,1,0:T(1,128)S(1)} async-done(((f32[64,1,64]{2,1,0:T(1,128)}), f32[64,1,64]{2,1,0:T(1,128)S(1)}, u32[]{:S(2)}, u32[]{:S(2)}) %all-to-all-start.2) | async-done | bytes 16416 | tf_op jit(solution)/shard_map/all_to_all | solution.py:58
  87.6 4.4 %all-to-all-start.5 = ((f32[2,64,8,256]{3,2,1,0:T(8,128)}), f32[2,64,8,256]{3,2,1,0:T(8,128)}, u32[]{:S(2)}, u32[]{:S(2)}) async-start(f32[2,64,8,256]{3,2,1,0:T(8,128)} %copy.226), calls=%async_computation.5 | async-start | bytes 2097152 | tf_op jit(solution)/shard_map/all_to_all | solution.py:51
  92.1 2.1 %all-to-all-done.5 = f32[2,64,8,256]{3,2,1,0:T(8,128)} async-done(((f32[2,64,8,256]{3,2,1,0:T(8,128)}), f32[2,64,8,256]{3,2,1,0:T(8,128)}, u32[]{:S(2)}, u32[]{:S(2)}) %all-to-all-start.5) | async-done | bytes 1048608 | tf_op jit(solution)/shard_map/all_to_all | solution.py:51
  94.8 12.4 %all-to-all-start.3 = ((f32[64,1,64]{2,1,0:T(1,128)}), f32[64,1,64]{2,1,0:T(1,128)S(1)}, u32[]{:S(2)}, u32[]{:S(2)}) async-start(f32[64,1,64]{2,1,0:T(1,128)} %broadcast_in_dim.14), calls=%async_computation.3 | async-start | bytes 65536 | tf_op jit(solution)/shard_map/all_to_all | solution.py:29
  107.2 2.2 %reduce_sum.398 = f32[64,8,256]{2,1,0:T(8,128)} reduce(f32[2,64,8,256]{3,2,1,0:T(8,128)} %all-to-all-done.5, f32[]{:T(128)} %constant.10.clone.1), dimensions={0}, to_apply=%region_38.0 | reduce | flops 131072 | bytes 1572868 | tf_op jit(solution)/shard_map/reduce_sum | solution.py:52
  109.4 9.8 %all-to-all-done.3 = f32[64,1,64]{2,1,0:T(1,128)S(1)} async-done(((f32[64,1,64]{2,1,0:T(1,128)}), f32[64,1,64]{2,1,0:T(1,128)S(1)}, u32[]{:S(2)}, u32[]{:S(2)}) %all-to-all-start.3) | async-done | bytes 16416 | tf_op jit(solution)/shard_map/all_to_all | solution.py:29
  119.3 3.7 %all_to_all.44 = f32[2,1,4096]{2,1,0:T(1,128)S(1)} all-to-all(f32[2,1,4096]{2,1,0:T(1,128)S(1)} %reshape.77), channel_id=1, replica_groups=mesh['sp_0'=16,'sp_1'=4,'sp_2'=2,'tp'=4] {'sp_2'}, dimensions={0} | all-to-all | bytes 65536 | tf_op jit(solution)/shard_map/all_to_all | solution.py:29
  123.0 8.0 %all-to-all-start.6 = ((f32[64,8,256]{2,1,0:T(8,128)}), f32[64,8,256]{2,1,0:T(8,128)}, u32[]{:S(2)}, u32[]{:S(2)}) async-start(f32[64,8,256]{2,1,0:T(8,128)} %reduce_sum.398), calls=%async_computation.6 | async-start | bytes 1048576 | tf_op jit(solution)/shard_map/all_to_all | solution.py:58
  133.2 5.8 %collective-permute-start.2 = (f32[15,256]{1,0:T(8,128)S(1)}, f32[15,256]{1,0:T(8,128)S(1)}, u32[]{:S(2)}, u32[]{:S(2)}) collective-permute-start(f32[15,256]{1,0:T(8,128)S(1)} %copy.184), channel_id=1, source_target_pairs={{4,0},{8,4},{12,8},{16,12},{20,16},{24,20},{28,24},{32,28},{36,32}... | collective-permute-start | bytes 46088 | tf_op jit(solution)/shard_map/ppermute | solution.py:22
  139.0 17.0 %collective-permute-done.3 = f32[15,256]{1,0:T(8,128)S(1)} collective-permute-done((f32[15,256]{1,0:T(8,128)S(1)}, f32[15,256]{1,0:T(8,128)S(1)}, u32[]{:S(2)}, u32[]{:S(2)}) %collective-permute-start.3) | collective-permute-done | bytes 15392 | tf_op jit(solution)/shard_map/ppermute | solution.py:21
  156.1 8.3 %fusion.4 = (bf16[1024,256]{1,0:T(8,128)(2,1)}, f32[1024,256]{1,0:T(8,128)S(1)}) fusion(bf16[1024,256]{1,0:T(8,128)(2,1)S(1)} %copy-done.4, bf16[1024,256]{1,0:T(8,128)(2,1)S(1)} %copy-done, f32[1024,256]{1,0:T(8,128)S(1)} %copy.185, f32[15,256]{1,0:T(8,128)S(1)} %collective-permute-done.3, f32[256]{0:T(256)} %bitcast.170, f32[256]{0:T(256)} %bitcast.168, ...), kind=kLoop, calls=%fused_computation.126 | loop fusion | flops 26476544 | bytes 3732480 | tf_op jit(solution)/shard_map/convert_element_type | solution.py:156
  (85 shorter events, 27.8 us)
Async XLA Ops:
  3.1 4.6 %copy-start = (bf16[1024,256]{1,0:T(8,128)(2,1)S(1)}, bf16[1024,256]{1,0:T(8,128)(2,1)}, u32[]{:S(2)}) copy-start(bf16[1024,256]{1,0:T(8,128)(2,1)} %param.7) | copy-start | bytes 1572868
  3.1 4.6 %copy-start.3 = (bf16[1024,256]{1,0:T(8,128)(2,1)S(1)}, bf16[1024,256]{1,0:T(8,128)(2,1)}, u32[]{:S(2)}) copy-start(bf16[1024,256]{1,0:T(8,128)(2,1)} %param.6) | copy-start | bytes 1572868
  3.1 10.5 %copy-start.9 = (bf16[31,256]{1,0:T(8,128)(2,1)S(1)}, bf16[31,256]{1,0:T(8,128)(2,1)}, u32[]{:S(2)}) copy-start(bf16[31,256]{1,0:T(8,128)(2,1)} %param.8) | copy-start | bytes 47620
  3.1 10.6 %copy-start.13 = (f32[256]{0:T(256)S(1)}, f32[256]{0:T(256)}, u32[]{:S(2)}) copy-start(f32[256]{0:T(256)} %param.9) | copy-start | bytes 3076
  3.1 10.7 %copy-start.7 = (bf16[1024,256]{1,0:T(8,128)(2,1)S(1)}, bf16[1024,256]{1,0:T(8,128)(2,1)}, u32[]{:S(2)}) copy-start(bf16[1024,256]{1,0:T(8,128)(2,1)} %param.10) | copy-start | bytes 1572868
  3.1 31.3 %all-to-all-start = ((bf16[4,1024,256]{2,1,0:T(8,128)(2,1)}), bf16[4,1024,256]{2,1,0:T(8,128)(2,1)}, u32[]{:S(2)}, u32[]{:S(2)}) async-start(bf16[4,1024,256]{2,1,0:T(8,128)(2,1)} %broadcast_in_dim.6), calls=%async_computation | async-start | bytes 4194304 | tf_op jit(solution)/shard_map/all_to_all | solution.py:29
  8.0 6.8 %collective-permute-start.1 = (bf16[15,256]{1,0:T(8,128)(2,1)S(1)}, bf16[15,256]{1,0:T(8,128)(2,1)S(1)}, u32[]{:S(2)}, u32[]{:S(2)}) collective-permute-start(bf16[15,256]{1,0:T(8,128)(2,1)S(1)} %get-tuple-element.47), channel_id=1, source_target_pairs={{4,0},{8,4},{12,8},{16,12},{20,16},{24,20},{28,24},{32,28},{36,32}... | collective-permute-start | bytes 23048 | tf_op jit(solution)/shard_map/ppermute | solution.py:22
  11.7 7.1 %collective-permute-start = (bf16[15,256]{1,0:T(8,128)(2,1)S(1)}, bf16[15,256]{1,0:T(8,128)(2,1)S(1)}, u32[]{:S(2)}, u32[]{:S(2)}) collective-permute-start(bf16[15,256]{1,0:T(8,128)(2,1)S(1)} %get-tuple-element.46), channel_id=1, source_target_pairs={{0,4},{4,8},{8,12},{12,16},{16,20},{20,24},{24,28},{28,32},{32,36}... | collective-permute-start | bytes 23048 | tf_op jit(solution)/shard_map/ppermute | solution.py:21
  13.7 11.7 %copy-start.10 = (f32[1,256]{1,0:T(1,128)}, f32[1,256]{1,0:T(1,128)S(1)}, u32[]{:S(2)}) copy-start(f32[1,256]{1,0:T(1,128)S(1)} %get-tuple-element.76) | copy-start | bytes 3076
  13.7 11.7 %copy-start.11 = (f32[1,256]{1,0:T(1,128)}, f32[1,256]{1,0:T(1,128)S(1)}, u32[]{:S(2)}) copy-start(f32[1,256]{1,0:T(1,128)S(1)} %get-tuple-element.77) | copy-start | bytes 3076
  13.7 11.7 %copy-start.12 = (f32[1,256]{1,0:T(1,128)}, f32[1,256]{1,0:T(1,128)S(1)}, u32[]{:S(2)}) copy-start(f32[1,256]{1,0:T(1,128)S(1)} %get-tuple-element.78) | copy-start | bytes 3076
  25.5 1.0 copy-start.1
  38.9 4.5 %copy-start.8 = (bf16[1024,256]{0,1:T(8,128)(2,1)S(1)}, bf16[1024,256]{0,1:T(8,128)(2,1)}, u32[]{:S(2)}) copy-start(bf16[1024,256]{0,1:T(8,128)(2,1)} %copy.183) | copy-start | bytes 1572868
  58.3 29.3 %all-to-all-start.2 = ((f32[64,1,64]{2,1,0:T(1,128)}), f32[64,1,64]{2,1,0:T(1,128)S(1)}, u32[]{:S(2)}, u32[]{:S(2)}) async-start(f32[64,1,64]{2,1,0:T(1,128)} %bitcast.70), calls=%async_computation.2 | async-start | bytes 65536 | tf_op jit(solution)/shard_map/all_to_all | solution.py:58
  75.6 2.1 %copy-start.2 = (f32[1024,256]{1,0:T(8,128)S(1)}, f32[1024,256]{1,0:T(8,128)}, u32[]{:S(2)}) copy-start(f32[1024,256]{1,0:T(8,128)} %copy-done.1) | copy-start | bytes 3145732
  75.6 2.2 %copy-start.5 = (f32[1024,256]{1,0:T(8,128)S(1)}, f32[1024,256]{1,0:T(8,128)}, u32[]{:S(2)}) copy-start(f32[1024,256]{1,0:T(8,128)} %copy.224) | copy-start | bytes 3145732
  75.6 2.5 %copy-start.6 = (f32[1024,256]{1,0:T(8,128)S(1)}, f32[1024,256]{1,0:T(8,128)}, u32[]{:S(2)}) copy-start(f32[1024,256]{1,0:T(8,128)} %copy.223) | copy-start | bytes 3145732
  87.6 6.6 %all-to-all-start.5 = ((f32[2,64,8,256]{3,2,1,0:T(8,128)}), f32[2,64,8,256]{3,2,1,0:T(8,128)}, u32[]{:S(2)}, u32[]{:S(2)}) async-start(f32[2,64,8,256]{3,2,1,0:T(8,128)} %copy.226), calls=%async_computation.5 | async-start | bytes 2097152 | tf_op jit(solution)/shard_map/all_to_all | solution.py:51
  92.0 64.1 %copy-start.4 = (bf16[1024,256]{1,0:T(8,128)(2,1)S(1)}, bf16[1024,256]{1,0:T(8,128)(2,1)}, u32[]{:S(2)}) copy-start(bf16[1024,256]{1,0:T(8,128)(2,1)} %param.6) | copy-start | bytes 1572868
  94.8 24.3 %all-to-all-start.3 = ((f32[64,1,64]{2,1,0:T(1,128)}), f32[64,1,64]{2,1,0:T(1,128)S(1)}, u32[]{:S(2)}, u32[]{:S(2)}) async-start(f32[64,1,64]{2,1,0:T(1,128)} %broadcast_in_dim.14), calls=%async_computation.3 | async-start | bytes 65536 | tf_op jit(solution)/shard_map/all_to_all | solution.py:29
  123.0 44.6 %all-to-all-start.6 = ((f32[64,8,256]{2,1,0:T(8,128)}), f32[64,8,256]{2,1,0:T(8,128)}, u32[]{:S(2)}, u32[]{:S(2)}) async-start(f32[64,8,256]{2,1,0:T(8,128)} %reduce_sum.398), calls=%async_computation.6 | async-start | bytes 1048576 | tf_op jit(solution)/shard_map/all_to_all | solution.py:58
  131.2 24.8 %collective-permute-start.3 = (f32[15,256]{1,0:T(8,128)S(1)}, f32[15,256]{1,0:T(8,128)S(1)}, u32[]{:S(2)}, u32[]{:S(2)}) collective-permute-start(f32[15,256]{1,0:T(8,128)S(1)} %copy.187), channel_id=1, source_target_pairs={{0,4},{4,8},{8,12},{12,16},{16,20},{20,24},{24,28},{28,32},{32,36}... | collective-permute-start | bytes 46088 | tf_op jit(solution)/shard_map/ppermute | solution.py:21
  133.2 22.8 %collective-permute-start.2 = (f32[15,256]{1,0:T(8,128)S(1)}, f32[15,256]{1,0:T(8,128)S(1)}, u32[]{:S(2)}, u32[]{:S(2)}) collective-permute-start(f32[15,256]{1,0:T(8,128)S(1)} %copy.184), channel_id=1, source_target_pairs={{4,0},{8,4},{12,8},{16,12},{20,16},{24,20},{28,24},{32,28},{36,32}... | collective-permute-start | bytes 46088 | tf_op jit(solution)/shard_map/ppermute | solution.py:22
where the time goes:
time: 170 us; the launch traced here: 169 us
  starting transfers between devices  60 us (35%)
  waiting for transfers between devices  40.5 us (24%)
  other arithmetic  28 us (16%)
  local copies, waits for them, and re-layouts  27.5 us (16%)
  blocking collectives  7.49 us (4%)
  matrix products  4.77 us (3%)
    all_to_all x2, starting transfers between devices, summed_rows(): return jnp.sum(lax.all_to_all(own, far, 0, 0, tiled=True), axis=0)  25.3 us
    ppermute x2, waiting for transfers between devices, extended(): before = lax.ppermute(last, axis, up)  21 us
    all_to_all x2, starting transfers between devices, from_everyone(): return lax.all_to_all(copies, axis, split_axis=0, concat_axis=0, tiled=True)  17 us
    all_to_all x2, waiting for transfers between devices, from_everyone(): return lax.all_to_all(copies, axis, split_axis=0, concat_axis=0, tiled=True)  14.7 us
    ppermute x2, starting transfers between devices, extended(): after = lax.ppermute(initial, axis, down)  9.4 us
    convert_element_type x1, other arithmetic, per_device(): (gated_grad * value_f * gate_sig * (1.0 - gate_sig)).astype(jnp.bfloat16)  8.25 us
    add x1, other arithmetic, per_device(): convolved + taps_f[tap_index] * gated_wide[tap_index:tap_index + extent]....  6.65 us
    reshape x2, local copies, waits for them, and re-layouts, in_order(): blocks.reshape(*lengths[:dim], lengths[dim] * lengths[dim + 1], *lengths[...  6.52 us
  transfers between devices with their start and end apart: 9, of which 6 were waited for; matrix products, arithmetic and copies ran while one was open for 20% of the time, Pallas kernels for 0%

commit v1 on v0

v1 whole, which is shorter than its diff:
```python
import functools

import jax
import jax.numpy as jnp
from jax import lax
from jax.experimental import pallas as pl
from jax.experimental.pallas import tpu as pltpu
from jax.sharding import Mesh
from jax.sharding import PartitionSpec as P

GROUP = 64
SP = ("z", "x", "c")
EPS = 1e-06
ROWS = 1024
CH = 256
LANES = 128
PAD = 16
HALO = ROWS + 2 * PAD
KW = 31
F32 = jnp.float32
BF16 = jnp.bfloat16
CHUNK = 256
VMEM = pl.BlockSpec(memory_space=pltpu.VMEM)
SMEM = pl.BlockSpec(memory_space=pltpu.SMEM)


def group_mean(x, avg):
    high = x.astype(BF16)
    low = (x - high.astype(F32)).astype(BF16)
    return jnp.dot(high, avg, preferred_element_type=F32) + jnp.dot(
        low, avg, preferred_element_type=F32
    )


def averaging():
    rows = lax.broadcasted_iota(jnp.int32, (CH, CH), 0) // GROUP
    cols = lax.broadcasted_iota(jnp.int32, (CH, CH), 1) // GROUP
    return jnp.where(rows == cols, 1.0 / GROUP, 0.0).astype(BF16)


def convolve(src, taps_at, store):
    tiles = 4
    for block in range(CH // LANES):

        def some_rows(step, _, block=block):
            start = pl.multiple_of(step * (8 * tiles), 8 * tiles)
            sums = [None] * tiles
            for k in range(KW):
                tap = taps_at(k, block)
                for j in range(tiles):
                    part = src[block, pl.ds(start + 8 * j + k + 1, 8), :] * tap
                    sums[j] = part if sums[j] is None else sums[j] + part
            for j in range(tiles):
                store(block, pl.multiple_of(start + 8 * j, 8), sums[j])
            return 0

        lax.fori_loop(0, ROWS // (8 * tiles), some_rows, 0)


def forward_kernel(value, gate, before, after, taps, gain, wide, unit, inv, normed, conv):
    lanes = [slice(b * LANES, (b + 1) * LANES) for b in range(2)]
    for b in range(2):
        wide[b, 0:PAD, :] = before[:, lanes[b]].astype(F32)
        wide[b, PAD + ROWS : HALO, :] = after[:, lanes[b]].astype(F32)

    def gate_rows(step, _):
        start = pl.multiple_of(step * 64, 64)
        rows = pl.ds(start, 64)
        gated = (value[rows, :].astype(F32) * jax.nn.sigmoid(gate[rows, :].astype(F32))).astype(
            BF16
        )
        for b in range(2):
            wide[b, pl.ds(pl.multiple_of(start + PAD, 16), 64), :] = gated[:, lanes[b]].astype(F32)
        return 0

    lax.fori_loop(0, ROWS // 64, gate_rows, 0)

    def store(block, start, rows):
        conv[pl.ds(start, 8), lanes[block]] = rows

    convolve(
        wide, lambda k, b: jnp.broadcast_to(taps[k : k + 1, lanes[b]], (8, LANES)), store
    )
    avg = averaging()
    gain_row = gain[...]

    def norm_rows(step, _):
        rows = pl.ds(pl.multiple_of(step * CHUNK, CHUNK), CHUNK)
        raw = conv[rows, :]
        centred = raw - group_mean(raw, avg)
        scale = lax.rsqrt(group_mean(centred * centred, avg) + EPS)
        unit_rows = centred * scale
        pre = unit_rows * gain_row
        unit[rows, :] = unit_rows
        inv[rows, :] = scale
        normed[rows, :] = (pre * jax.nn.sigmoid(pre)).astype(BF16)
        return 0

    lax.fori_loop(0, ROWS // CHUNK, norm_rows, 0)


def early_kernel(me, own, left, right, weight, normed, partial, wgrad):
    y = me[0]
    blocks = ((own, lax.rem(y, 4)), (left, lax.rem(y + 3, 4)), (right, lax.rem(y + 1, 4)))
    weights = [weight[pl.ds(pl.multiple_of(at * CH, CH), CH), :] for _, at in blocks]

    def some_rows(step, _):
        rows = pl.ds(pl.multiple_of(step * CHUNK, CHUNK), CHUNK)
        total = None
        for (ref, _), w in zip(blocks, weights):
            part = jnp.dot(ref[rows, :], w, preferred_element_type=F32)
            total = part if total is None else total + part
        partial[rows, :] = total
        return 0

    lax.fori_loop(0, ROWS // CHUNK, some_rows, 0)
    for d, (ref, _) in enumerate(blocks):
        grads = lax.dot_general(
            ref[...], normed[...], (((0,), (0,)), ((), ())), preferred_element_type=F32
        )
        put_weight(wgrad, d, grads)


def put_weight(out, d, grads):
    pieces = grads.reshape(4, 8, 8, CH).astype(BF16)
    for near in range(4):
        for peer in range(8):
            out[peer, d * 4 + near] = pieces[near, peer]


def late_kernel(
    me, far, weight, normed, partial, unit, inv, gain, wide, grad, head, tail, sums, conv
):
    y = me[0]
    w = weight[pl.ds(pl.multiple_of(lax.rem(y + 2, 4) * CH, CH), CH), :]
    avg = averaging()
    gain_row = gain[...]

    def some_rows(step, gain_sum):
        start = pl.multiple_of(step * CHUNK, CHUNK)
        rows = pl.ds(start, CHUNK)
        normed_grad = partial[rows, :] + jnp.dot(far[rows, :], w, preferred_element_type=F32)
        u = unit[rows, :]
        pre = u * gain_row
        s = jax.nn.sigmoid(pre)
        act = normed_grad * s * (1.0 + pre * (1.0 - s))
        au = act * u
        hat = act * gain_row
        hat_unit = au * gain_row
        rows_grad = inv[rows, :] * (
            hat - group_mean(hat, avg) - u * group_mean(hat_unit, avg)
        )
        for b in range(2):
            conv[b, rows, :] = rows_grad[:, b * LANES : (b + 1) * LANES]
        return gain_sum + jnp.sum(au.reshape(CHUNK // 8, 8, CH), axis=0)

    gain_sum = lax.fori_loop(0, ROWS // CHUNK, some_rows, jnp.zeros((8, CH), F32))
    for b in range(2):
        cols = slice(b * LANES, (b + 1) * LANES)
        head[:, cols] = conv[b, 0:PAD, :]
        tail[:, cols] = conv[b, ROWS - PAD : ROWS, :]
        grad[b] = conv[b]

    put_weight(
        sums,
        0,
        lax.dot_general(
            far[...], normed[...], (((0,), (0,)), ((), ())), preferred_element_type=F32
        ),
    )

    halves = []
    for b in range(2):

        def tile(step, carry, b=b):
            start = pl.multiple_of(step * 8, 8)
            g = conv[b, pl.ds(start, 8), :]
            return tuple(
                acc + g * wide[b, pl.ds(start + k + 1, 8), :] for k, acc in enumerate(carry)
            )

        accs = lax.fori_loop(
            0, ROWS // 8, tile, tuple(jnp.zeros((8, LANES), F32) for _ in range(KW))
        )
        lines = [jnp.sum(a, axis=0, keepdims=True) for a in accs]
        halves.append(jnp.concatenate(lines, axis=0))
    taps = jnp.concatenate(
        [
            jnp.concatenate(halves, axis=1),
            jnp.sum(gain_sum, axis=0, keepdims=True),
        ],
        axis=0,
    ).astype(BF16)
    for peer in range(8):
        for part in range(2):
            line = (peer % 2) * 16 + part * 8
            sums[peer, 4 + part] = taps[line : line + 8]


def backward_kernel(value, gate, grad, before, after, taps, value_grad, gate_grad, wide, conv):
    lanes = [slice(b * LANES, (b + 1) * LANES) for b in range(2)]
    for b in range(2):
        wide[b, 0:PAD, :] = before[:, lanes[b]]
        wide[b, PAD : PAD + ROWS, :] = grad[b]
        wide[b, PAD + ROWS : HALO, :] = after[:, lanes[b]]

    def store(block, start, rows):
        conv[pl.ds(start, 8), lanes[block]] = rows

    convolve(
        wide,
        lambda k, b: jnp.broadcast_to(taps[KW - 1 - k : KW - k, lanes[b]], (8, LANES)),
        store,
    )

    def finish(step, _):
        rows = pl.ds(pl.multiple_of(step * 64, 64), 64)
        s = jax.nn.sigmoid(gate[rows, :].astype(F32))
        down = conv[rows, :] * s
        value_grad[rows, :] = down.astype(BF16)
        gate_grad[rows, :] = (down * value[rows, :].astype(F32) * (1.0 - s)).astype(BF16)
        return 0

    lax.fori_loop(0, ROWS // 64, finish, 0)


def middle_kernel(me, early, late, out):
    y = me[0]
    taps = late[0, 4:6].astype(F32)
    for peer in range(1, 8):
        taps = taps + late[peer, 4:6].astype(F32)
    taps = taps.astype(BF16)
    for d, at in enumerate((y, y + 3, y + 1, y + 2)):
        home = lax.rem(at, 4)
        src, base = (early, d * 4) if d < 3 else (late, 0)
        for near in range(4):
            total = src[0, base + near].astype(F32)
            for peer in range(1, 8):
                total = total + src[peer, base + near].astype(F32)
            out[home * 4 + near, 0] = total.astype(BF16)
            out[home * 4 + near, 1:3] = taps


def call(kernel, outs, specs, scratch=(), name=None, cost=None):
    return pl.pallas_call(
        kernel,
        out_shape=outs,
        in_specs=specs,
        out_specs=jax.tree.map(lambda _: VMEM, outs),
        scratch_shapes=scratch,
        name=name,
        cost_estimate=cost,
        compiler_params=pltpu.CompilerParams(vmem_limit_bytes=48 * 1024 * 1024),
    )


def shape(*dims, dtype=F32):
    return jax.ShapeDtypeStruct(dims, dtype)


def cost(us):
    return pl.CostEstimate(flops=int(us * 1e-6 * 2e14), bytes_accessed=2**20, transcendentals=0)


def ring(size, by):
    return [(i, (i + by) % size) for i in range(size)]


def per_device(value_rows, gate_rows, conv_taps, norm_gain, point_weight, out_grad):
    peers = lax.axis_size(SP)
    up = [(i, i + 1) for i in range(peers - 1)]
    down = [(j, i) for i, j in up]
    me = lax.axis_index("tp").astype(jnp.int32).reshape(1)
    taps = conv_taps.astype(F32)
    gain = norm_gain.reshape(1, CH)

    left = lax.ppermute(out_grad, "tp", ring(4, 1))
    right = lax.ppermute(out_grad, "tp", ring(4, 3))
    far = lax.ppermute(out_grad, "tp", ring(4, 2))

    def gated_of(rows):
        return (
            value_rows[rows].astype(F32) * jax.nn.sigmoid(gate_rows[rows].astype(F32))
        ).astype(BF16)

    before = lax.ppermute(gated_of(slice(ROWS - PAD, ROWS)), SP, up)
    after = lax.ppermute(gated_of(slice(0, PAD)), SP, down)

    wide, unit, inv, normed = call(
        forward_kernel,
        (shape(2, HALO, LANES), shape(ROWS, CH), shape(ROWS, CH), shape(ROWS, CH, dtype=BF16)),
        [VMEM] * 6,
        [pltpu.VMEM((ROWS, CH), F32)],
        "forward",
        cost(7),
    )(value_rows, gate_rows, before, after, taps, gain)

    partial, wgrad = call(
        early_kernel,
        (shape(ROWS, CH), shape(8, 12, 8, CH, dtype=BF16)),
        [SMEM] + [VMEM] * 5,
        (),
        "early",
        cost(4),
    )(me, out_grad, left, right, point_weight, normed)
    early = lax.all_to_all(wgrad, ("x", "c"), 0, 0, tiled=True)

    grad, head, tail, sums = call(
        late_kernel,
        (
            shape(2, ROWS, LANES),
            shape(PAD, CH),
            shape(PAD, CH),
            shape(8, 6, 8, CH, dtype=BF16),
        ),
        [SMEM] + [VMEM] * 8,
        [pltpu.VMEM((2, ROWS, LANES), F32)],
        "late",
        cost(8),
    )(me, far, point_weight, normed, partial, unit, inv, gain, wide)
    late = lax.all_to_all(sums, ("x", "c"), 0, 0, tiled=True)

    grad_before = lax.ppermute(tail, SP, up)
    grad_after = lax.ppermute(head, SP, down)
    value_grad, gate_grad = call(
        backward_kernel,
        (shape(ROWS, CH, dtype=BF16), shape(ROWS, CH, dtype=BF16)),
        [VMEM] * 6,
        [pltpu.VMEM((2, HALO, LANES), F32), pltpu.VMEM((ROWS, CH), F32)],
        "backward",
        cost(6),
    )(value_rows, gate_rows, grad, grad_before, grad_after, taps)

    sent = call(
        middle_kernel,
        shape(16, 3, 8, CH, dtype=BF16),
        [SMEM, VMEM, VMEM],
        (),
        "middle",
        cost(1),
    )(me, early, late)
    whole = jnp.sum(lax.all_to_all(sent, "z", 0, 0, tiled=True).astype(F32), axis=0)
    mine = whole[1:3].reshape(16, CH)
    other = lax.ppermute(mine, "c", ring(2, 1))
    first = lax.axis_index("c") == 0
    low = jnp.where(first, mine, other)
    high = jnp.where(first, other, mine)
    return value_grad, gate_grad, jnp.concatenate([low, high[:15]]), high[15], whole[0]


def solution(mesh):
    finer = Mesh(mesh.devices.reshape(16, 4, 2, mesh.shape["tp"]), ("z", "x", "c", "tp"))
    return jax.shard_map(
        per_device,
        mesh=finer,
        in_specs=(P(SP, "tp"), P(SP, "tp"), P(None, "tp"), P("tp"), P(None, "tp"), P(SP, "tp")),
        out_specs=(P(SP, "tp"), P(SP, "tp"), P(None, "tp"), P("tp"), P(SP, "tp")),
        check_vma=False,
    )
```

time: 170 us -> 102 us (0.60)
  the two profiles are of different devices: /device:TPU:96 before, /device:TPU:127 now
where the time goes in v1:
time: 102 us; the launch traced here: 101 us
  starting transfers between devices  41.7 us (41%)
  blocking collectives  23.7 us (23%)
  Pallas kernels  20.7 us (20%)
  waiting for transfers between devices  7.73 us (8%)
  local copies, waits for them, and re-layouts  3.96 us (4%)
  other arithmetic  2.15 us (2%)
    all_to_all x1, starting transfers between devices, per_device(): lax.all_to_all(sent, 'z', 0, 0, tiled=True).astype(F32)  13.7 us
    all_to_all x1, blocking collectives, per_device(): late = lax.all_to_all(sums, ('x', 'c'), 0, 0, tiled=True)  12.2 us
    all_to_all x1, blocking collectives, per_device(): early = lax.all_to_all(wgrad, ('x', 'c'), 0, 0, tiled=True)  11.5 us
    pallas_call x1, Pallas kernels, per_device(): call(late_kernel, (shape(2, ROWS, LANES), shape(PAD, CH), shape(PAD, CH),...  8.79 us
    ppermute x1, starting transfers between devices, per_device(): grad_before = lax.ppermute(tail, SP, up)  7.11 us
    ppermute x1, waiting for transfers between devices, per_device(): grad_after = lax.ppermute(head, SP, down)  6.84 us
    ppermute x1, starting transfers between devices, per_device(): before = lax.ppermute(gated_of(slice(ROWS - PAD, ROWS)), SP, up)  5.46 us
    pallas_call x1, Pallas kernels, per_device(): call(forward_kernel, (shape(2, HALO, LANES), shape(ROWS, CH), shape(ROWS,...  5.27 us
  transfers between devices with their start and end apart: 9, of which 3 were waited for; matrix products, arithmetic and copies ran while one was open for 2% of the time, Pallas kernels for 11%

profile of v1, /device:TPU:127, one launch (start us, length us, event | category | flops | bytes accessed | tf_op | source)
XLA Modules:
  0.0 100.8 jit_solution(5319619657699238497)
XLA Ops:
  0.6 1.9 %collective-permute-start.3 = (bf16[1024,256]{1,0:T(8,128)(2,1)}, bf16[1024,256]{1,0:T(8,128)(2,1)S(1)}, u32[]{:S(2)}, u32[]{:S(2)}) collective-permute-start(bf16[1024,256]{1,0:T(8,128)(2,1)} %own.1), channel_id=1, source_target_pairs={{0,1},{1,2},{2,3},{3,0},{4,5},{5,6},{6,7},{7,4},{8,9},{9,10},{10,1... | collective-permute-start | bytes 1572872 | tf_op jit(solution)/shard_map/ppermute | solution.py:277
  2.6 3.4 %collective-permute-start.4 = (bf16[1024,256]{1,0:T(8,128)(2,1)}, bf16[1024,256]{1,0:T(8,128)(2,1)S(1)}, u32[]{:S(2)}, u32[]{:S(2)}) collective-permute-start(bf16[1024,256]{1,0:T(8,128)(2,1)} %own.1), channel_id=1, source_target_pairs={{0,3},{1,0},{2,1},{3,2},{4,7},{5,4},{6,5},{7,6},{8,11},{9,8},{10,9... | collective-permute-start | bytes 1572872 | tf_op jit(solution)/shard_map/ppermute | solution.py:278
  5.9 2.9 %collective-permute-start = (bf16[1024,256]{1,0:T(8,128)(2,1)}, bf16[1024,256]{1,0:T(8,128)(2,1)S(1)}, u32[]{:S(2)}, u32[]{:S(2)}) collective-permute-start(bf16[1024,256]{1,0:T(8,128)(2,1)} %own.1), channel_id=1, source_target_pairs={{0,2},{1,3},{2,0},{3,1},{4,6},{5,7},{6,4},{7,5},{8,10},{9,11},{10,... | collective-permute-start | bytes 1572872 | tf_op jit(solution)/shard_map/ppermute | solution.py:279
  8.8 0.8 multiply_convert_fusion
  9.6 3.4 %collective-permute-start.2 = (bf16[16,256]{1,0:T(8,128)(2,1)S(1)}, bf16[16,256]{1,0:T(8,128)(2,1)S(1)}, u32[]{:S(2)}, u32[]{:S(2)}) collective-permute-start(bf16[16,256]{1,0:T(8,128)(2,1)S(1)} %get-tuple-element.29), channel_id=1, source_target_pairs={{4,0},{8,4},{12,8},{16,12},{20,16},{24,20},{28,24},{32,28},{36,32}... | collective-permute-start | bytes 24584 | tf_op jit(solution)/shard_map/ppermute | solution.py:287
  13.0 5.5 %collective-permute-start.1 = (bf16[16,256]{1,0:T(8,128)(2,1)S(1)}, bf16[16,256]{1,0:T(8,128)(2,1)S(1)}, u32[]{:S(2)}, u32[]{:S(2)}) collective-permute-start(bf16[16,256]{1,0:T(8,128)(2,1)S(1)} %get-tuple-element.30), channel_id=1, source_target_pairs={{0,4},{4,8},{8,12},{12,16},{16,20},{20,24},{24,28},{28,32},{32,36}... | collective-permute-start | bytes 24584 | tf_op jit(solution)/shard_map/ppermute | solution.py:286
  18.5 0.7 convert_element_type.30.taps
  19.3 1.0 %copy-done = bf16[1024,256]{1,0:T(8,128)(2,1)S(1)} copy-done((bf16[1024,256]{1,0:T(8,128)(2,1)S(1)}, bf16[1024,256]{1,0:T(8,128)(2,1)}, u32[]{:S(2)}) %copy-start) | copy-done | bytes 524312
  20.3 1.0 %copy-done.2 = bf16[1024,256]{1,0:T(8,128)(2,1)S(1)} copy-done((bf16[1024,256]{1,0:T(8,128)(2,1)S(1)}, bf16[1024,256]{1,0:T(8,128)(2,1)}, u32[]{:S(2)}) %copy-start.2) | copy-done | bytes 524312
  21.3 0.7 copy-done.6
  22.0 5.3 %forward.1 = (f32[2,1056,128]{2,1,0:T(8,128)S(1)}, f32[1024,256]{1,0:T(8,128)S(1)}, f32[1024,256]{1,0:T(8,128)S(1)}, bf16[1024,256]{1,0:T(8,128)(2,1)S(1)}) custom-call(bf16[1024,256]{1,0:T(8,128)(2,1)S(1)} %copy-done, bf16[1024,256]{1,0:T(8,128)(2,1)S(1)} %copy-done.2, bf16[16,256]{1,0:T(8,128)(2,1)S(1)} %collective-permute-done.1.before, ...), custom_call_target="tpu_custom_call" | custom-call | flops 1400000000 | bytes 1048576 | tf_op jit(solution)/shard_map/forward/pallas_call | solution.py:289
  27.4 1.8 %early.1 = (f32[1024,256]{1,0:T(8,128)S(1)}, bf16[8,12,8,256]{3,2,1,0:T(8,128)(2,1)S(1)}) custom-call(s32[1]{0:T(128)} %bitcast.me, bf16[1024,256]{1,0:T(8,128)(2,1)S(1)} %copy-done.4, bf16[1024,256]{1,0:T(8,128)(2,1)S(1)} %collective-permute-done.3.left, bf16[1024,256]{1,0:T(8,128)(2,1)S(1)} %collective-permute-done.4.right, ...), custom_call_target="tpu_custom_call" | custom-call | flops 800000000 | bytes 1048576 | tf_op jit(solution)/shard_map/early/pallas_call | solution.py:298
  29.4 8.8 %late.1 = (f32[2,1024,128]{2,1,0:T(8,128)S(1)}, f32[16,256]{1,0:T(8,128)S(1)}, f32[16,256]{1,0:T(8,128)S(1)}, bf16[8,6,8,256]{3,2,1,0:T(8,128)(2,1)S(1)}) custom-call(s32[1]{0:T(128)} %bitcast.me, bf16[1024,256]{1,0:T(8,128)(2,1)S(1)} %collective-permute-done.far, bf16[1024,256]{1,0:T(8,128)(2,1)S(1)} %copy-done.5, ...), custom_call_target="tpu_custom_call" | custom-call | flops 1600000000 | bytes 1048576 | tf_op jit(solution)/shard_map/late/pallas_call | solution.py:308
  38.2 12.2 %all_to_all.15.late = bf16[8,6,8,256]{3,2,1,0:T(8,128)(2,1)S(1)} all-to-all(bf16[8,6,8,256]{3,2,1,0:T(8,128)(2,1)S(1)} %get-tuple-element.28), channel_id=1, replica_groups=mesh['z'=16,'x'=4,'c'=2,'tp'=4] {'x','c'}, dimensions={0} | all-to-all | bytes 393216 | tf_op jit(solution)/shard_map/all_to_all | solution.py:321
  50.4 11.5 %all_to_all.16.early = bf16[8,12,8,256]{3,2,1,0:T(8,128)(2,1)S(1)} all-to-all(bf16[8,12,8,256]{3,2,1,0:T(8,128)(2,1)S(1)} %get-tuple-element.27), channel_id=1, replica_groups=mesh['z'=16,'x'=4,'c'=2,'tp'=4] {'x','c'}, dimensions={0} | all-to-all | bytes 786432 | tf_op jit(solution)/shard_map/all_to_all | solution.py:306
  61.9 0.8 middle.1
  62.7 13.7 %all-to-all-start.2 = ((bf16[16,3,8,256]{3,2,1,0:T(8,128)(2,1)}), bf16[16,3,8,256]{3,2,1,0:T(8,128)(2,1)S(1)}, u32[]{:S(2)}, u32[]{:S(2)}) async-start(bf16[16,3,8,256]{3,2,1,0:T(8,128)(2,1)} %middle.1), calls=%async_computation.2 | async-start | bytes 393216 | tf_op jit(solution)/shard_map/all_to_all | solution.py:342
  76.4 7.1 %collective-permute-start.5 = (f32[16,256]{1,0:T(8,128)S(1)}, f32[16,256]{1,0:T(8,128)S(1)}, u32[]{:S(2)}, u32[]{:S(2)}) collective-permute-start(f32[16,256]{1,0:T(8,128)S(1)} %get-tuple-element.23), channel_id=1, source_target_pairs={{0,4},{4,8},{8,12},{12,16},{16,20},{20,24},{24,28},{28,32},{32,36}... | collective-permute-start | bytes 49160 | tf_op jit(solution)/shard_map/ppermute | solution.py:323
  83.5 1.9 %collective-permute-start.6 = (f32[16,256]{1,0:T(8,128)S(1)}, f32[16,256]{1,0:T(8,128)S(1)}, u32[]{:S(2)}, u32[]{:S(2)}) collective-permute-start(f32[16,256]{1,0:T(8,128)S(1)} %get-tuple-element.24), channel_id=1, source_target_pairs={{4,0},{8,4},{12,8},{16,12},{20,16},{24,20},{28,24},{32,28},{36,32}... | collective-permute-start | bytes 49160 | tf_op jit(solution)/shard_map/ppermute | solution.py:324
  85.5 6.8 %collective-permute-done.6.after = f32[16,256]{1,0:T(8,128)S(1)} collective-permute-done((f32[16,256]{1,0:T(8,128)S(1)}, f32[16,256]{1,0:T(8,128)S(1)}, u32[]{:S(2)}, u32[]{:S(2)}) %collective-permute-start.6) | collective-permute-done | bytes 16416 | tf_op jit(solution)/shard_map/ppermute | solution.py:324
  92.3 4.2 %backward.1 = (bf16[1024,256]{1,0:T(8,128)(2,1)}, bf16[1024,256]{1,0:T(8,128)(2,1)}) custom-call(bf16[1024,256]{1,0:T(8,128)(2,1)S(1)} %copy-done.1, bf16[1024,256]{1,0:T(8,128)(2,1)S(1)} %copy-done.3, f32[2,1024,128]{2,1,0:T(8,128)S(1)} %get-tuple-element.22.grad, f32[16,256]{1,0:T(8,128)S(1)} %collective-permute-done.5.before, ...), custom_call_target="tpu_custom_call" | custom-call | flops 1200000000 | bytes 1048576 | tf_op jit(solution)/shard_map/backward/pallas_call | solution.py:325
  96.5 1.9 %collective-permute-start.7 = (f32[16,256]{1,0:T(8,128)S(1)}, f32[16,256]{1,0:T(8,128)S(1)}, u32[]{:S(2)}, u32[]{:S(2)}) collective-permute-start(f32[16,256]{1,0:T(8,128)S(1)} %slice_bitcast_fusion), channel_id=1, source_target_pairs={{0,4},{4,0},{1,5},{5,1},{2,6},{6,2},{3,7},{7,3},{8,12},{12,8},{9,1... | collective-permute-start | bytes 49160 | tf_op jit(solution)/shard_map/ppermute | solution.py:344
  98.5 0.6 slice_bitcast_fusion.1
  100.2 0.6 pad_maximum_fusion
  (27 shorter events, 1.5 us)
Async XLA Ops:
  0.6 26.7 %collective-permute-start.3 = (bf16[1024,256]{1,0:T(8,128)(2,1)}, bf16[1024,256]{1,0:T(8,128)(2,1)S(1)}, u32[]{:S(2)}, u32[]{:S(2)}) collective-permute-start(bf16[1024,256]{1,0:T(8,128)(2,1)} %own.1), channel_id=1, source_target_pairs={{0,1},{1,2},{2,3},{3,0},{4,5},{5,6},{6,7},{7,4},{8,9},{9,10},{10,1... | collective-permute-start | bytes 1572872 | tf_op jit(solution)/shard_map/ppermute | solution.py:277
  2.6 24.8 %collective-permute-start.4 = (bf16[1024,256]{1,0:T(8,128)(2,1)}, bf16[1024,256]{1,0:T(8,128)(2,1)S(1)}, u32[]{:S(2)}, u32[]{:S(2)}) collective-permute-start(bf16[1024,256]{1,0:T(8,128)(2,1)} %own.1), channel_id=1, source_target_pairs={{0,3},{1,0},{2,1},{3,2},{4,7},{5,4},{6,5},{7,6},{8,11},{9,8},{10,9... | collective-permute-start | bytes 1572872 | tf_op jit(solution)/shard_map/ppermute | solution.py:278
  5.9 23.5 %collective-permute-start = (bf16[1024,256]{1,0:T(8,128)(2,1)}, bf16[1024,256]{1,0:T(8,128)(2,1)S(1)}, u32[]{:S(2)}, u32[]{:S(2)}) collective-permute-start(bf16[1024,256]{1,0:T(8,128)(2,1)} %own.1), channel_id=1, source_target_pairs={{0,2},{1,3},{2,0},{3,1},{4,6},{5,7},{6,4},{7,5},{8,10},{9,11},{10,... | collective-permute-start | bytes 1572872 | tf_op jit(solution)/shard_map/ppermute | solution.py:279
  9.6 9.6 %collective-permute-start.2 = (bf16[16,256]{1,0:T(8,128)(2,1)S(1)}, bf16[16,256]{1,0:T(8,128)(2,1)S(1)}, u32[]{:S(2)}, u32[]{:S(2)}) collective-permute-start(bf16[16,256]{1,0:T(8,128)(2,1)S(1)} %get-tuple-element.29), channel_id=1, source_target_pairs={{4,0},{8,4},{12,8},{16,12},{20,16},{24,20},{28,24},{32,28},{36,32}... | collective-permute-start | bytes 24584 | tf_op jit(solution)/shard_map/ppermute | solution.py:287
  13.0 6.2 %collective-permute-start.1 = (bf16[16,256]{1,0:T(8,128)(2,1)S(1)}, bf16[16,256]{1,0:T(8,128)(2,1)S(1)}, u32[]{:S(2)}, u32[]{:S(2)}) collective-permute-start(bf16[16,256]{1,0:T(8,128)(2,1)S(1)} %get-tuple-element.30), channel_id=1, source_target_pairs={{0,4},{4,8},{8,12},{12,16},{16,20},{20,24},{24,28},{28,32},{32,36}... | collective-permute-start | bytes 24584 | tf_op jit(solution)/shard_map/ppermute | solution.py:286
  19.3 1.0 %copy-start = (bf16[1024,256]{1,0:T(8,128)(2,1)S(1)}, bf16[1024,256]{1,0:T(8,128)(2,1)}, u32[]{:S(2)}) copy-start(bf16[1024,256]{1,0:T(8,128)(2,1)} %value.3) | copy-start | bytes 1572868
  20.3 1.0 %copy-start.2 = (bf16[1024,256]{1,0:T(8,128)(2,1)S(1)}, bf16[1024,256]{1,0:T(8,128)(2,1)}, u32[]{:S(2)}) copy-start(bf16[1024,256]{1,0:T(8,128)(2,1)} %gate.3) | copy-start | bytes 1572868
  21.3 0.7 copy-start.6
  22.0 5.3 %copy-start.4 = (bf16[1024,256]{1,0:T(8,128)(2,1)S(1)}, bf16[1024,256]{1,0:T(8,128)(2,1)}, u32[]{:S(2)}) copy-start(bf16[1024,256]{1,0:T(8,128)(2,1)} %own.1) | copy-start | bytes 1572868
  22.0 5.3 %copy-start.5 = (bf16[1024,256]{1,0:T(8,128)(2,1)S(1)}, bf16[1024,256]{1,0:T(8,128)(2,1)}, u32[]{:S(2)}) copy-start(bf16[1024,256]{1,0:T(8,128)(2,1)} %weight.3) | copy-start | bytes 1572868
  27.3 1.8 %copy-start.8 = (f32[2,1056,128]{2,1,0:T(8,128)}, f32[2,1056,128]{2,1,0:T(8,128)S(1)}, u32[]{:S(2)}) copy-start(f32[2,1056,128]{2,1,0:T(8,128)S(1)} %get-tuple-element.21.wide) | copy-start | bytes 3244036
  27.3 2.1 %copy-start.7 = (f32[256]{0:T(256)S(1)}, f32[256]{0:T(256)}, u32[]{:S(2)}) copy-start(f32[256]{0:T(256)} %param.9) | copy-start | bytes 3076
  50.4 41.9 %copy-start.1 = (bf16[1024,256]{1,0:T(8,128)(2,1)S(1)}, bf16[1024,256]{1,0:T(8,128)(2,1)}, u32[]{:S(2)}) copy-start(bf16[1024,256]{1,0:T(8,128)(2,1)} %value.3) | copy-start | bytes 1572868
  50.4 41.9 %copy-start.3 = (bf16[1024,256]{1,0:T(8,128)(2,1)S(1)}, bf16[1024,256]{1,0:T(8,128)(2,1)}, u32[]{:S(2)}) copy-start(bf16[1024,256]{1,0:T(8,128)(2,1)} %gate.3) | copy-start | bytes 1572868
  62.7 33.8 %all-to-all-start.2 = ((bf16[16,3,8,256]{3,2,1,0:T(8,128)(2,1)}), bf16[16,3,8,256]{3,2,1,0:T(8,128)(2,1)S(1)}, u32[]{:S(2)}, u32[]{:S(2)}) async-start(bf16[16,3,8,256]{3,2,1,0:T(8,128)(2,1)} %middle.1), calls=%async_computation.2 | async-start | bytes 393216 | tf_op jit(solution)/shard_map/all_to_all | solution.py:342
  76.4 9.1 %collective-permute-start.5 = (f32[16,256]{1,0:T(8,128)S(1)}, f32[16,256]{1,0:T(8,128)S(1)}, u32[]{:S(2)}, u32[]{:S(2)}) collective-permute-start(f32[16,256]{1,0:T(8,128)S(1)} %get-tuple-element.23), channel_id=1, source_target_pairs={{0,4},{4,8},{8,12},{12,16},{16,20},{20,24},{24,28},{28,32},{32,36}... | collective-permute-start | bytes 49160 | tf_op jit(solution)/shard_map/ppermute | solution.py:323
  83.5 8.8 %collective-permute-start.6 = (f32[16,256]{1,0:T(8,128)S(1)}, f32[16,256]{1,0:T(8,128)S(1)}, u32[]{:S(2)}, u32[]{:S(2)}) collective-permute-start(f32[16,256]{1,0:T(8,128)S(1)} %get-tuple-element.24), channel_id=1, source_target_pairs={{4,0},{8,4},{12,8},{16,12},{20,16},{24,20},{28,24},{32,28},{36,32}... | collective-permute-start | bytes 49160 | tf_op jit(solution)/shard_map/ppermute | solution.py:324
  96.5 3.1 %collective-permute-start.7 = (f32[16,256]{1,0:T(8,128)S(1)}, f32[16,256]{1,0:T(8,128)S(1)}, u32[]{:S(2)}, u32[]{:S(2)}) collective-permute-start(f32[16,256]{1,0:T(8,128)S(1)} %slice_bitcast_fusion), channel_id=1, source_target_pairs={{0,4},{4,0},{1,5},{5,1},{2,6},{6,2},{3,7},{7,3},{8,12},{12,8},{9,1... | collective-permute-start | bytes 49160 | tf_op jit(solution)/shard_map/ppermute | solution.py:344

commit v2 on v1

--- a/solution.py
+++ b/solution.py
@@ -1,5 +1,3 @@
-import functools
-
 import jax
 import jax.numpy as jnp
 from jax import lax
@@ -7,6 +5,7 @@
 from jax.experimental.pallas import tpu as pltpu
 from jax.sharding import Mesh
 from jax.sharding import PartitionSpec as P
+
 
 GROUP = 64
 SP = ("z", "x", "c")
@@ -57,11 +56,18 @@
         lax.fori_loop(0, ROWS // (8 * tiles), some_rows, 0)
 
 
-def forward_kernel(value, gate, before, after, taps, gain, wide, unit, inv, normed, conv):
+def sides(second, inner, outer):
+    return jnp.where(second, inner, outer), jnp.where(second, outer, inner)
+
+
+def forward_kernel(
+    me, value, gate, inner, outer, taps, gain, wide, unit, inv, slope, normed, conv
+):
     lanes = [slice(b * LANES, (b + 1) * LANES) for b in range(2)]
+    before, after = sides(me[1] == 1, inner[...].astype(F32), outer[...].astype(F32))
     for b in range(2):
-        wide[b, 0:PAD, :] = before[:, lanes[b]].astype(F32)
-        wide[b, PAD + ROWS : HALO, :] = after[:, lanes[b]].astype(F32)
+        wide[b, 0:PAD, :] = before[:, lanes[b]]
+        wide[b, PAD + ROWS : HALO, :] = after[:, lanes[b]]
 
     def gate_rows(step, _):
         start = pl.multiple_of(step * 64, 64)
@@ -78,8 +84,9 @@
     def store(block, start, rows):
         conv[pl.ds(start, 8), lanes[block]] = rows
 
+    lines = taps[...].astype(F32)
     convolve(
-        wide, lambda k, b: jnp.broadcast_to(taps[k : k + 1, lanes[b]], (8, LANES)), store
+        wide, lambda k, b: jnp.broadcast_to(lines[k : k + 1, lanes[b]], (8, LANES)), store
     )
     avg = averaging()
     gain_row = gain[...]
@@ -91,9 +98,11 @@
         scale = lax.rsqrt(group_mean(centred * centred, avg) + EPS)
         unit_rows = centred * scale
         pre = unit_rows * gain_row
+        s = jax.nn.sigmoid(pre)
         unit[rows, :] = unit_rows
         inv[rows, :] = scale
-        normed[rows, :] = (pre * jax.nn.sigmoid(pre)).astype(BF16)
+        slope[rows, :] = s * (1.0 + pre * (1.0 - s))
+        normed[rows, :] = (pre * s).astype(BF16)
         return 0
 
     lax.fori_loop(0, ROWS // CHUNK, norm_rows, 0)
@@ -129,7 +138,7 @@
 
 
 def late_kernel(
-    me, far, weight, normed, partial, unit, inv, gain, wide, grad, head, tail, sums, conv
+    me, far, weight, normed, partial, unit, inv, slope, gain, wide, begun, grad, swap_in, swap_out, sums
 ):
     y = me[0]
     w = weight[pl.ds(pl.multiple_of(lax.rem(y + 2, 4) * CH, CH), CH), :]
@@ -141,9 +150,7 @@
         rows = pl.ds(start, CHUNK)
         normed_grad = partial[rows, :] + jnp.dot(far[rows, :], w, preferred_element_type=F32)
         u = unit[rows, :]
-        pre = u * gain_row
-        s = jax.nn.sigmoid(pre)
-        act = normed_grad * s * (1.0 + pre * (1.0 - s))
+        act = normed_grad * slope[rows, :]
         au = act * u
         hat = act * gain_row
         hat_unit = au * gain_row
@@ -151,19 +158,18 @@
             hat - group_mean(hat, avg) - u * group_mean(hat_unit, avg)
         )
         for b in range(2):
-            conv[b, rows, :] = rows_grad[:, b * LANES : (b + 1) * LANES]
+            grad[b, rows, :] = rows_grad[:, b * LANES : (b + 1) * LANES]
         return gain_sum + jnp.sum(au.reshape(CHUNK // 8, 8, CH), axis=0)
 
     gain_sum = lax.fori_loop(0, ROWS // CHUNK, some_rows, jnp.zeros((8, CH), F32))
     for b in range(2):
         cols = slice(b * LANES, (b + 1) * LANES)
-        head[:, cols] = conv[b, 0:PAD, :]
-        tail[:, cols] = conv[b, ROWS - PAD : ROWS, :]
-        grad[b] = conv[b]
+        head, tail = grad[b, 0:PAD, :], grad[b, ROWS - PAD : ROWS, :]
+        swap_in[:, cols], swap_out[:, cols] = sides(me[1] == 1, head, tail)
 
     put_weight(
         sums,
-        0,
+        3,
         lax.dot_general(
             far[...], normed[...], (((0,), (0,)), ((), ())), preferred_element_type=F32
         ),
@@ -174,7 +180,7 @@
 
         def tile(step, carry, b=b):
             start = pl.multiple_of(step * 8, 8)
-            g = conv[b, pl.ds(start, 8), :]
+            g = grad[b, pl.ds(start, 8), :]
             return tuple(
                 acc + g * wide[b, pl.ds(start + k + 1, 8), :] for k, acc in enumerate(carry)
             )
@@ -194,10 +200,14 @@
     for peer in range(8):
         for part in range(2):
             line = (peer % 2) * 16 + part * 8
-            sums[peer, 4 + part] = taps[line : line + 8]
-
-
-def backward_kernel(value, gate, grad, before, after, taps, value_grad, gate_grad, wide, conv):
+            sums[peer, 16 + part] = taps[line : line + 8]
+
+
+def backward_kernel(
+    me, value, gate, grad, inner, outer, taps, value_grad, gate_grad, wide, conv
+):
+    before, after = sides(me[1] == 1, inner[...], outer[...])
+    lines = taps[...].astype(F32)
     lanes = [slice(b * LANES, (b + 1) * LANES) for b in range(2)]
     for b in range(2):
         wide[b, 0:PAD, :] = before[:, lanes[b]]
@@ -209,7 +219,7 @@
 
     convolve(
         wide,
-        lambda k, b: jnp.broadcast_to(taps[KW - 1 - k : KW - k, lanes[b]], (8, LANES)),
+        lambda k, b: jnp.broadcast_to(lines[KW - 1 - k : KW - k, lanes[b]], (8, LANES)),
         store,
     )
 
@@ -224,33 +234,48 @@
     lax.fori_loop(0, ROWS // 64, finish, 0)
 
 
-def middle_kernel(me, early, late, out):
+def middle_kernel(me, late, out):
     y = me[0]
-    taps = late[0, 4:6].astype(F32)
+    taps = late[0, 16:18].astype(F32)
     for peer in range(1, 8):
-        taps = taps + late[peer, 4:6].astype(F32)
+        taps = taps + late[peer, 16:18].astype(F32)
     taps = taps.astype(BF16)
     for d, at in enumerate((y, y + 3, y + 1, y + 2)):
         home = lax.rem(at, 4)
-        src, base = (early, d * 4) if d < 3 else (late, 0)
         for near in range(4):
-            total = src[0, base + near].astype(F32)
+            total = late[0, d * 4 + near].astype(F32)
             for peer in range(1, 8):
-                total = total + src[peer, base + near].astype(F32)
+                total = total + late[peer, d * 4 + near].astype(F32)
             out[home * 4 + near, 0] = total.astype(BF16)
             out[home * 4 + near, 1:3] = taps
 
 
-def call(kernel, outs, specs, scratch=(), name=None, cost=None):
+def whole_kernel(got, weight, mine):
+    total = got[0].astype(F32)
+    for peer in range(1, 16):
+        total = total + got[peer].astype(F32)
+    weight[...] = total[0]
+    mine[0:8] = total[1]
+    mine[8:16] = total[2]
+
+
+def last_kernel(me, mine, other, taps, gain):
+    low, high = sides(me[1] == 1, other[...], mine[...])
+    taps[0:16] = low
+    taps[16:31] = high[:15]
+    gain[...] = high[15:16]
+
+
+def call(kernel, outs, specs, scratch=(), cost=None, alias={}):
     return pl.pallas_call(
         kernel,
         out_shape=outs,
         in_specs=specs,
         out_specs=jax.tree.map(lambda _: VMEM, outs),
         scratch_shapes=scratch,
-        name=name,
         cost_estimate=cost,
-        compiler_params=pltpu.CompilerParams(vmem_limit_bytes=48 * 1024 * 1024),
+        input_output_aliases=alias,
+        compiler_params=pltpu.CompilerParams(vmem_limit_bytes=8 * 1024 * 1024),
     )
 
 
@@ -266,92 +291,95 @@
     return [(i, (i + by) % size) for i in range(size)]
 
 
-def per_device(value_rows, gate_rows, conv_taps, norm_gain, point_weight, out_grad):
+def body(value_rows, gate_rows, conv_taps, norm_gain, point_weight, out_grad):
     peers = lax.axis_size(SP)
-    up = [(i, i + 1) for i in range(peers - 1)]
-    down = [(j, i) for i, j in up]
-    me = lax.axis_index("tp").astype(jnp.int32).reshape(1)
-    taps = conv_taps.astype(F32)
+    pairs = [(i, i ^ 1) for i in range(peers)]
+    apart = [(i, i + 1) for i in range(1, peers - 1, 2)]
+    apart = apart + [(j, i) for i, j in apart]
+    second = lax.axis_index("c").astype(jnp.int32)
+    me = jnp.stack([lax.axis_index("tp").astype(jnp.int32), second])
     gain = norm_gain.reshape(1, CH)
 
-    left = lax.ppermute(out_grad, "tp", ring(4, 1))
-    right = lax.ppermute(out_grad, "tp", ring(4, 3))
-    far = lax.ppermute(out_grad, "tp", ring(4, 2))
+    def exchange(array, axis):
+        return lax.all_to_all(array, axis, 0, 0, tiled=True)
 
     def gated_of(rows):
         return (
             value_rows[rows].astype(F32) * jax.nn.sigmoid(gate_rows[rows].astype(F32))
         ).astype(BF16)
 
-    before = lax.ppermute(gated_of(slice(ROWS - PAD, ROWS)), SP, up)
-    after = lax.ppermute(gated_of(slice(0, PAD)), SP, down)
-
-    wide, unit, inv, normed = call(
+    swap_in, swap_out = sides(
+        second == 1, gated_of(slice(0, PAD)), gated_of(slice(ROWS - PAD, ROWS))
+    )
+    left = lax.ppermute(out_grad, "tp", ring(4, 1))
+    right = lax.ppermute(out_grad, "tp", ring(4, 3))
+    inner = lax.ppermute(swap_in, SP, pairs)
+    outer = lax.ppermute(swap_out, SP, apart)
+    far = lax.ppermute(out_grad, "tp", ring(4, 2))
+
+    wide, unit, inv, slope, normed = call(
         forward_kernel,
-        (shape(2, HALO, LANES), shape(ROWS, CH), shape(ROWS, CH), shape(ROWS, CH, dtype=BF16)),
-        [VMEM] * 6,
+        (
+            shape(2, HALO, LANES),
+            shape(ROWS, CH),
+            shape(ROWS, CH),
+            shape(ROWS, CH),
+            shape(ROWS, CH, dtype=BF16),
+        ),
+        [SMEM] + [VMEM] * 6,
         [pltpu.VMEM((ROWS, CH), F32)],
-        "forward",
         cost(7),
-    )(value_rows, gate_rows, before, after, taps, gain)
+    )(me, value_rows, gate_rows, inner, outer, conv_taps, gain)
 
     partial, wgrad = call(
         early_kernel,
-        (shape(ROWS, CH), shape(8, 12, 8, CH, dtype=BF16)),
+        (shape(ROWS, CH), shape(8, 18, 8, CH, dtype=BF16)),
         [SMEM] + [VMEM] * 5,
         (),
-        "early",
         cost(4),
     )(me, out_grad, left, right, point_weight, normed)
-    early = lax.all_to_all(wgrad, ("x", "c"), 0, 0, tiled=True)
-
-    grad, head, tail, sums = call(
+
+    grad, swap_in, swap_out, sums = call(
         late_kernel,
         (
             shape(2, ROWS, LANES),
             shape(PAD, CH),
             shape(PAD, CH),
-            shape(8, 6, 8, CH, dtype=BF16),
+            shape(8, 18, 8, CH, dtype=BF16),
         ),
-        [SMEM] + [VMEM] * 8,
-        [pltpu.VMEM((2, ROWS, LANES), F32)],
-        "late",
+        [SMEM] + [VMEM] * 10,
+        (),
         cost(8),
-    )(me, far, point_weight, normed, partial, unit, inv, gain, wide)
-    late = lax.all_to_all(sums, ("x", "c"), 0, 0, tiled=True)
-
-    grad_before = lax.ppermute(tail, SP, up)
-    grad_after = lax.ppermute(head, SP, down)
+        {10: 3},
+    )(me, far, point_weight, normed, partial, unit, inv, slope, gain, wide, wgrad)
+    late = exchange(sums, ("x", "c"))
+
+    sent = call(middle_kernel, shape(16, 3, 8, CH, dtype=BF16), [SMEM, VMEM], (), cost(1))(me, late)
+    got = exchange(sent, "z")
+
+    inner = lax.ppermute(swap_in, SP, pairs)
+    outer = lax.ppermute(swap_out, SP, apart)
     value_grad, gate_grad = call(
         backward_kernel,
         (shape(ROWS, CH, dtype=BF16), shape(ROWS, CH, dtype=BF16)),
-        [VMEM] * 6,
+        [SMEM] + [VMEM] * 6,
         [pltpu.VMEM((2, HALO, LANES), F32), pltpu.VMEM((ROWS, CH), F32)],
-        "backward",
         cost(6),
-    )(value_rows, gate_rows, grad, grad_before, grad_after, taps)
-
-    sent = call(
-        middle_kernel,
-        shape(16, 3, 8, CH, dtype=BF16),
-        [SMEM, VMEM, VMEM],
-        (),
-        "middle",
-        cost(1),
-    )(me, early, late)
-    whole = jnp.sum(lax.all_to_all(sent, "z", 0, 0, tiled=True).astype(F32), axis=0)
-    mine = whole[1:3].reshape(16, CH)
+    )(me, value_rows, gate_rows, grad, inner, outer, conv_taps)
+
+    got, value_grad, gate_grad = lax.optimization_barrier((got, value_grad, gate_grad))
+    weight_grad, mine = call(whole_kernel, (shape(8, CH), shape(16, CH)), [VMEM], (), cost(1))(got)
     other = lax.ppermute(mine, "c", ring(2, 1))
-    first = lax.axis_index("c") == 0
-    low = jnp.where(first, mine, other)
-    high = jnp.where(first, other, mine)
-    return value_grad, gate_grad, jnp.concatenate([low, high[:15]]), high[15], whole[0]
+    taps_grad, gain_grad = call(
+        last_kernel, (shape(KW, CH), shape(1, CH)), [SMEM, VMEM, VMEM], (), cost(1)
+    )(me, mine, other)
+    return value_grad, gate_grad, taps_grad, gain_grad.reshape(CH), weight_grad
 
 
 def solution(mesh):
     finer = Mesh(mesh.devices.reshape(16, 4, 2, mesh.shape["tp"]), ("z", "x", "c", "tp"))
     return jax.shard_map(
-        per_device,
+        body,
         mesh=finer,
         in_specs=(P(SP, "tp"), P(SP, "tp"), P(None, "tp"), P("tp"), P(None, "tp"), P(SP, "tp")),
         out_specs=(P(SP, "tp"), P(SP, "tp"), P(None, "tp"), P("tp"), P(SP, "tp")),

time: 102 us -> 95 us (0.931)
  the two profiles are of different devices: /device:TPU:127 before, /device:TPU:25 now
where the time goes in v2:
time: 95 us; the launch traced here: 94.4 us
  starting transfers between devices  41.9 us (44%)
  Pallas kernels  24.3 us (26%)
  blocking collectives  18.1 us (19%)
  waiting for transfers between devices  4.8 us (5%)
  local copies, waits for them, and re-layouts  3.5 us (4%)
    all_to_all x1, blocking collectives, exchange(): return lax.all_to_all(array, axis, 0, 0, tiled=True)  18.1 us
    all_to_all x1, starting transfers between devices, exchange(): return lax.all_to_all(array, axis, 0, 0, tiled=True)  14.9 us
    pallas_call x1, Pallas kernels, body(): call(late_kernel, (shape(2, ROWS, LANES), shape(PAD, CH), shape(PAD, CH),...  7.95 us
    ppermute x2, starting transfers between devices, body(): outer = lax.ppermute(swap_out, SP, apart)  6.61 us
    ppermute x2, starting transfers between devices, body(): inner = lax.ppermute(swap_in, SP, pairs)  6.28 us
    pallas_call x1, Pallas kernels, body(): call(forward_kernel, (shape(2, HALO, LANES), shape(ROWS, CH), shape(ROWS,...  6.09 us
    ppermute x1, starting transfers between devices, body(): other = lax.ppermute(mine, 'c', ring(2, 1))  5.99 us
    pallas_call x1, Pallas kernels, body(): call(backward_kernel, (shape(ROWS, CH, dtype=BF16), shape(ROWS, CH, dtype...  4.94 us
  transfers between devices with their start and end apart: 9, of which 3 were waited for; matrix products, arithmetic and copies ran while one was open for 1% of the time, Pallas kernels for 14%

profile of v2, /device:TPU:25, one launch (start us, length us, event | category | flops | bytes accessed | tf_op | source)
XLA Modules:
  0.0 94.4 jit_solution(5274993090378742445)
XLA Ops:
  0.6 1.9 %collective-permute-start.3 = (bf16[1024,256]{1,0:T(8,128)(2,1)}, bf16[1024,256]{1,0:T(8,128)(2,1)S(1)}, u32[]{:S(2)}, u32[]{:S(2)}) collective-permute-start(bf16[1024,256]{1,0:T(8,128)(2,1)} %own.1), channel_id=1, source_target_pairs={{0,1},{1,2},{2,3},{3,0},{4,5},{5,6},{6,7},{7,4},{8,9},{9,10},{10,1... | collective-permute-start | bytes 1572872 | tf_op jit(solution)/shard_map/ppermute | solution.py:314
  2.6 3.4 %collective-permute-start.4 = (bf16[1024,256]{1,0:T(8,128)(2,1)}, bf16[1024,256]{1,0:T(8,128)(2,1)S(1)}, u32[]{:S(2)}, u32[]{:S(2)}) collective-permute-start(bf16[1024,256]{1,0:T(8,128)(2,1)} %own.1), channel_id=1, source_target_pairs={{0,3},{1,0},{2,1},{3,2},{4,7},{5,4},{6,5},{7,6},{8,11},{9,8},{10,9... | collective-permute-start | bytes 1572872 | tf_op jit(solution)/shard_map/ppermute | solution.py:315
  5.9 2.9 %collective-permute-start = (bf16[1024,256]{1,0:T(8,128)(2,1)}, bf16[1024,256]{1,0:T(8,128)(2,1)S(1)}, u32[]{:S(2)}, u32[]{:S(2)}) collective-permute-start(bf16[1024,256]{1,0:T(8,128)(2,1)} %own.1), channel_id=1, source_target_pairs={{0,2},{1,3},{2,0},{3,1},{4,6},{5,7},{6,4},{7,5},{8,10},{9,11},{10,... | collective-permute-start | bytes 1572872 | tf_op jit(solution)/shard_map/ppermute | solution.py:318
  8.8 0.8 broadcast_select_fusion
  9.6 4.5 %collective-permute-start.2 = (bf16[16,256]{1,0:T(8,128)(2,1)S(1)}, bf16[16,256]{1,0:T(8,128)(2,1)S(1)}, u32[]{:S(2)}, u32[]{:S(2)}) collective-permute-start(bf16[16,256]{1,0:T(8,128)(2,1)S(1)} %get-tuple-element.45), channel_id=1, source_target_pairs={{4,8},{12,16},{20,24},{28,32},{36,40},{44,48},{52,56},{60,64},{68,... | collective-permute-start | bytes 24584 | tf_op jit(solution)/shard_map/ppermute | solution.py:317
  14.1 3.3 %collective-permute-start.1 = (bf16[16,256]{1,0:T(8,128)(2,1)S(1)}, bf16[16,256]{1,0:T(8,128)(2,1)S(1)}, u32[]{:S(2)}, u32[]{:S(2)}) collective-permute-start(bf16[16,256]{1,0:T(8,128)(2,1)S(1)} %get-tuple-element.46), channel_id=1, source_target_pairs={{0,4},{4,0},{8,12},{12,8},{16,20},{20,16},{24,28},{28,24},{32,36},... | collective-permute-start | bytes 24584 | tf_op jit(solution)/shard_map/ppermute | solution.py:316
  17.6 0.7 collective-permute-done.1.inner
  18.3 0.7 copy-done.1
  19.0 1.0 %copy-done.2 = bf16[1024,256]{1,0:T(8,128)(2,1)S(1)} copy-done((bf16[1024,256]{1,0:T(8,128)(2,1)S(1)}, bf16[1024,256]{1,0:T(8,128)(2,1)}, u32[]{:S(2)}) %copy-start.2) | copy-done | bytes 524312
  20.0 1.0 %copy-done.4 = bf16[1024,256]{1,0:T(8,128)(2,1)S(1)} copy-done((bf16[1024,256]{1,0:T(8,128)(2,1)S(1)}, bf16[1024,256]{1,0:T(8,128)(2,1)}, u32[]{:S(2)}) %copy-start.4) | copy-done | bytes 524312
  21.0 0.7 copy-done.7
  21.8 6.1 %shard_map.101 = (f32[2,1056,128]{2,1,0:T(8,128)S(1)}, f32[1024,256]{1,0:T(8,128)S(1)}, f32[1024,256]{1,0:T(8,128)S(1)}, f32[1024,256]{1,0:T(8,128)S(1)}, bf16[1024,256]{1,0:T(8,128)(2,1)S(1)}) custom-call(s32[2]{0:T(128)S(1)} %pad_add_fusion.me, bf16[1024,256]{1,0:T(8,128)(2,1)S(1)} %copy-done.2, bf16[1024,256]{1,0:T(8,128)(2,1)S(1)} %copy-done.4, ...), custom_call_target="tpu_custom_call" | custom-call | flops 1400000000 | bytes 1048576 | tf_op jit(solution)/shard_map/pallas_call | solution.py:320
  27.9 2.3 %shard_map.102 = (f32[1024,256]{1,0:T(8,128)S(1)}, bf16[8,18,8,256]{3,2,1,0:T(8,128)(2,1)S(1)}) custom-call(s32[2]{0:T(128)S(1)} %pad_add_fusion.me, bf16[1024,256]{1,0:T(8,128)(2,1)S(1)} %copy-done.6, bf16[1024,256]{1,0:T(8,128)(2,1)S(1)} %collective-permute-done.3.left, bf16[1024,256]{1,0:T(8,128)(2,1)S(1)} %collective-permute-done.4.right, ...), custom_call_target="tpu_custom_call" | custom-call | flops 800000000 | bytes 1048576 | tf_op jit(solution)/shard_map/pallas_call | solution.py:334
  30.2 8.0 %shard_map.103 = (f32[2,1024,128]{2,1,0:T(8,128)S(1)}, f32[16,256]{1,0:T(8,128)S(1)}, f32[16,256]{1,0:T(8,128)S(1)}, bf16[8,18,8,256]{3,2,1,0:T(8,128)(2,1)S(1)}) custom-call(s32[2]{0:T(128)S(1)} %pad_add_fusion.me, bf16[1024,256]{1,0:T(8,128)(2,1)S(1)} %collective-permute-done.far, bf16[1024,256]{1,0:T(8,128)(2,1)S(1)} %copy-done, ...), custom_call_target="tpu_custom_call", output_to_operand_aliasing={{3}: (10, {})} | custom-call | flops 1600000000 | bytes 1048576 | tf_op jit(solution)/shard_map/pallas_call | solution.py:342
  38.2 18.1 %all_to_all.10.late = bf16[8,18,8,256]{3,2,1,0:T(8,128)(2,1)S(1)} all-to-all(bf16[8,18,8,256]{3,2,1,0:T(8,128)(2,1)S(1)} %get-tuple-element.32), channel_id=1, replica_groups=mesh['z'=16,'x'=4,'c'=2,'tp'=4] {'x','c'}, dimensions={0} | all-to-all | bytes 1179648 | tf_op jit(solution)/shard_map/all_to_all | solution.py:304
  56.3 1.3 %shard_map.104 = bf16[16,3,8,256]{3,2,1,0:T(8,128)(2,1)} custom-call(s32[2]{0:T(128)S(1)} %pad_add_fusion.me, bf16[8,18,8,256]{3,2,1,0:T(8,128)(2,1)S(1)} %all_to_all.10.late), custom_call_target="tpu_custom_call" | custom-call | flops 200000000 | bytes 1048576 | tf_op jit(solution)/shard_map/pallas_call | solution.py:357
  57.6 14.9 %all-to-all-start.1 = ((bf16[16,3,8,256]{3,2,1,0:T(8,128)(2,1)}), bf16[16,3,8,256]{3,2,1,0:T(8,128)(2,1)S(1)}, u32[]{:S(2)}, u32[]{:S(2)}) async-start(bf16[16,3,8,256]{3,2,1,0:T(8,128)(2,1)} %shard_map.104), calls=%async_computation.1 | async-start | bytes 393216 | tf_op jit(solution)/shard_map/all_to_all | solution.py:304
  72.5 2.9 %collective-permute-start.5 = (f32[16,256]{1,0:T(8,128)S(1)}, f32[16,256]{1,0:T(8,128)S(1)}, u32[]{:S(2)}, u32[]{:S(2)}) collective-permute-start(f32[16,256]{1,0:T(8,128)S(1)} %get-tuple-element.34), channel_id=1, source_target_pairs={{0,4},{4,0},{8,12},{12,8},{16,20},{20,16},{24,28},{28,24},{32,36},... | collective-permute-start | bytes 49160 | tf_op jit(solution)/shard_map/ppermute | solution.py:360
  75.5 2.1 %collective-permute-start.6 = (f32[16,256]{1,0:T(8,128)S(1)}, f32[16,256]{1,0:T(8,128)S(1)}, u32[]{:S(2)}, u32[]{:S(2)}) collective-permute-start(f32[16,256]{1,0:T(8,128)S(1)} %get-tuple-element.35), channel_id=1, source_target_pairs={{4,8},{12,16},{20,24},{28,32},{36,40},{44,48},{52,56},{60,64},{68,... | collective-permute-start | bytes 49160 | tf_op jit(solution)/shard_map/ppermute | solution.py:361
  77.6 3.2 %collective-permute-done.6.outer = f32[16,256]{1,0:T(8,128)S(1)} collective-permute-done((f32[16,256]{1,0:T(8,128)S(1)}, f32[16,256]{1,0:T(8,128)S(1)}, u32[]{:S(2)}, u32[]{:S(2)}) %collective-permute-start.6) | collective-permute-done | bytes 16416 | tf_op jit(solution)/shard_map/ppermute | solution.py:361
  80.8 4.9 %shard_map.105 = (bf16[1024,256]{1,0:T(8,128)(2,1)}, bf16[1024,256]{1,0:T(8,128)(2,1)}) custom-call(s32[2]{0:T(128)S(1)} %pad_add_fusion.me, bf16[1024,256]{1,0:T(8,128)(2,1)S(1)} %copy-done.3, bf16[1024,256]{1,0:T(8,128)(2,1)S(1)} %copy-done.5, f32[2,1024,128]{2,1,0:T(8,128)S(1)} %get-tuple-element.33.grad, f32[16,256]{1,0:T(8,128)S(1)} %collective-permute-done.5.inner, ...), custom_call_target="tpu_custom_call" | custom-call | flops 1200000000 | bytes 1048576 | tf_op jit(solution)/shard_map/pallas_call | solution.py:362
  86.4 6.0 %collective-permute-start.7 = (f32[16,256]{1,0:T(8,128)S(1)}, f32[16,256]{1,0:T(8,128)S(1)}, u32[]{:S(2)}, u32[]{:S(2)}) collective-permute-start(f32[16,256]{1,0:T(8,128)S(1)} %get-tuple-element.41.mine), channel_id=1, source_target_pairs={{0,4},{4,0},{1,5},{5,1},{2,6},{6,2},{3,7},{7,3},{8,12},{12,8},{9,1... | collective-permute-start | bytes 49160 | tf_op jit(solution)/shard_map/ppermute | solution.py:372
  92.4 0.8 collective-permute-done.7.other
  93.2 1.2 %shard_map.107 = (f32[31,256]{1,0:T(8,128)}, f32[1,256]{1,0:T(1,128)}) custom-call(s32[2]{0:T(128)S(1)} %pad_add_fusion.me, f32[16,256]{1,0:T(8,128)S(1)} %get-tuple-element.41.mine, f32[16,256]{1,0:T(8,128)S(1)} %collective-permute-done.7.other), custom_call_target="tpu_custom_call" | custom-call | flops 200000000 | bytes 1048576 | tf_op jit(solution)/shard_map/pallas_call | solution.py:373
  (22 shorter events, 0.7 us)
Async XLA Ops:
  0.6 27.2 %collective-permute-start.3 = (bf16[1024,256]{1,0:T(8,128)(2,1)}, bf16[1024,256]{1,0:T(8,128)(2,1)S(1)}, u32[]{:S(2)}, u32[]{:S(2)}) collective-permute-start(bf16[1024,256]{1,0:T(8,128)(2,1)} %own.1), channel_id=1, source_target_pairs={{0,1},{1,2},{2,3},{3,0},{4,5},{5,6},{6,7},{7,4},{8,9},{9,10},{10,1... | collective-permute-start | bytes 1572872 | tf_op jit(solution)/shard_map/ppermute | solution.py:314
  2.6 25.3 %collective-permute-start.4 = (bf16[1024,256]{1,0:T(8,128)(2,1)}, bf16[1024,256]{1,0:T(8,128)(2,1)S(1)}, u32[]{:S(2)}, u32[]{:S(2)}) collective-permute-start(bf16[1024,256]{1,0:T(8,128)(2,1)} %own.1), channel_id=1, source_target_pairs={{0,3},{1,0},{2,1},{3,2},{4,7},{5,4},{6,5},{7,6},{8,11},{9,8},{10,9... | collective-permute-start | bytes 1572872 | tf_op jit(solution)/shard_map/ppermute | solution.py:315
  5.9 24.3 %collective-permute-start = (bf16[1024,256]{1,0:T(8,128)(2,1)}, bf16[1024,256]{1,0:T(8,128)(2,1)S(1)}, u32[]{:S(2)}, u32[]{:S(2)}) collective-permute-start(bf16[1024,256]{1,0:T(8,128)(2,1)} %own.1), channel_id=1, source_target_pairs={{0,2},{1,3},{2,0},{3,1},{4,6},{5,7},{6,4},{7,5},{8,10},{9,11},{10,... | collective-permute-start | bytes 1572872 | tf_op jit(solution)/shard_map/ppermute | solution.py:318
  9.6 8.0 %collective-permute-start.2 = (bf16[16,256]{1,0:T(8,128)(2,1)S(1)}, bf16[16,256]{1,0:T(8,128)(2,1)S(1)}, u32[]{:S(2)}, u32[]{:S(2)}) collective-permute-start(bf16[16,256]{1,0:T(8,128)(2,1)S(1)} %get-tuple-element.45), channel_id=1, source_target_pairs={{4,8},{12,16},{20,24},{28,32},{36,40},{44,48},{52,56},{60,64},{68,... | collective-permute-start | bytes 24584 | tf_op jit(solution)/shard_map/ppermute | solution.py:317
  14.1 4.2 %collective-permute-start.1 = (bf16[16,256]{1,0:T(8,128)(2,1)S(1)}, bf16[16,256]{1,0:T(8,128)(2,1)S(1)}, u32[]{:S(2)}, u32[]{:S(2)}) collective-permute-start(bf16[16,256]{1,0:T(8,128)(2,1)S(1)} %get-tuple-element.46), channel_id=1, source_target_pairs={{0,4},{4,0},{8,12},{12,8},{16,20},{20,16},{24,28},{28,24},{32,36},... | collective-permute-start | bytes 24584 | tf_op jit(solution)/shard_map/ppermute | solution.py:316
  18.3 0.7 copy-start.1
  19.0 1.0 %copy-start.2 = (bf16[1024,256]{1,0:T(8,128)(2,1)S(1)}, bf16[1024,256]{1,0:T(8,128)(2,1)}, u32[]{:S(2)}) copy-start(bf16[1024,256]{1,0:T(8,128)(2,1)} %value.3) | copy-start | bytes 1572868
  20.0 1.0 %copy-start.4 = (bf16[1024,256]{1,0:T(8,128)(2,1)S(1)}, bf16[1024,256]{1,0:T(8,128)(2,1)}, u32[]{:S(2)}) copy-start(bf16[1024,256]{1,0:T(8,128)(2,1)} %gate.3) | copy-start | bytes 1572868
  21.0 0.7 copy-start.7
  21.8 6.1 %copy-start = (bf16[1024,256]{1,0:T(8,128)(2,1)S(1)}, bf16[1024,256]{1,0:T(8,128)(2,1)}, u32[]{:S(2)}) copy-start(bf16[1024,256]{1,0:T(8,128)(2,1)} %weight.3) | copy-start | bytes 1572868
  21.8 6.1 %copy-start.6 = (bf16[1024,256]{1,0:T(8,128)(2,1)S(1)}, bf16[1024,256]{1,0:T(8,128)(2,1)}, u32[]{:S(2)}) copy-start(bf16[1024,256]{1,0:T(8,128)(2,1)} %own.1) | copy-start | bytes 1572868
  38.2 42.7 %copy-start.3 = (bf16[1024,256]{1,0:T(8,128)(2,1)S(1)}, bf16[1024,256]{1,0:T(8,128)(2,1)}, u32[]{:S(2)}) copy-start(bf16[1024,256]{1,0:T(8,128)(2,1)} %value.3) | copy-start | bytes 1572868
  38.2 42.6 %copy-start.5 = (bf16[1024,256]{1,0:T(8,128)(2,1)S(1)}, bf16[1024,256]{1,0:T(8,128)(2,1)}, u32[]{:S(2)}) copy-start(bf16[1024,256]{1,0:T(8,128)(2,1)} %gate.3) | copy-start | bytes 1572868
  38.2 42.6 %copy-start.8 = (bf16[31,256]{1,0:T(8,128)(2,1)S(1)}, bf16[31,256]{1,0:T(8,128)(2,1)}, u32[]{:S(2)}) copy-start(bf16[31,256]{1,0:T(8,128)(2,1)} %taps.3) | copy-start | bytes 47620
  57.6 28.2 %all-to-all-start.1 = ((bf16[16,3,8,256]{3,2,1,0:T(8,128)(2,1)}), bf16[16,3,8,256]{3,2,1,0:T(8,128)(2,1)S(1)}, u32[]{:S(2)}, u32[]{:S(2)}) async-start(bf16[16,3,8,256]{3,2,1,0:T(8,128)(2,1)} %shard_map.104), calls=%async_computation.1 | async-start | bytes 393216 | tf_op jit(solution)/shard_map/all_to_all | solution.py:304
  72.5 5.0 %collective-permute-start.5 = (f32[16,256]{1,0:T(8,128)S(1)}, f32[16,256]{1,0:T(8,128)S(1)}, u32[]{:S(2)}, u32[]{:S(2)}) collective-permute-start(f32[16,256]{1,0:T(8,128)S(1)} %get-tuple-element.34), channel_id=1, source_target_pairs={{0,4},{4,0},{8,12},{12,8},{16,20},{20,16},{24,28},{28,24},{32,36},... | collective-permute-start | bytes 49160 | tf_op jit(solution)/shard_map/ppermute | solution.py:360
  75.5 5.4 %collective-permute-start.6 = (f32[16,256]{1,0:T(8,128)S(1)}, f32[16,256]{1,0:T(8,128)S(1)}, u32[]{:S(2)}, u32[]{:S(2)}) collective-permute-start(f32[16,256]{1,0:T(8,128)S(1)} %get-tuple-element.35), channel_id=1, source_target_pairs={{4,8},{12,16},{20,24},{28,32},{36,40},{44,48},{52,56},{60,64},{68,... | collective-permute-start | bytes 49160 | tf_op jit(solution)/shard_map/ppermute | solution.py:361
  86.4 6.8 %collective-permute-start.7 = (f32[16,256]{1,0:T(8,128)S(1)}, f32[16,256]{1,0:T(8,128)S(1)}, u32[]{:S(2)}, u32[]{:S(2)}) collective-permute-start(f32[16,256]{1,0:T(8,128)S(1)} %get-tuple-element.41.mine), channel_id=1, source_target_pairs={{0,4},{4,0},{1,5},{5,1},{2,6},{6,2},{3,7},{7,3},{8,12},{12,8},{9,1... | collective-permute-start | bytes 49160 | tf_op jit(solution)/shard_map/ppermute | solution.py:372

commit v3 on v2

--- a/solution.py
+++ b/solution.py
@@ -20,7 +20,6 @@
 BF16 = jnp.bfloat16
 CHUNK = 256
 VMEM = pl.BlockSpec(memory_space=pltpu.VMEM)
-SMEM = pl.BlockSpec(memory_space=pltpu.SMEM)
 
 
 def group_mean(x, avg):
@@ -56,15 +55,28 @@
         lax.fori_loop(0, ROWS // (8 * tiles), some_rows, 0)
 
 
+def is_second():
+    return lax.axis_index("c") == 1
+
+
 def sides(second, inner, outer):
     return jnp.where(second, inner, outer), jnp.where(second, outer, inner)
 
 
+def edge_kernel(value_head, gate_head, value_tail, gate_tail, swap_in, swap_out):
+    def gated(value, gate):
+        return value[...].astype(F32) * jax.nn.sigmoid(gate[...].astype(F32))
+
+    inner, outer = sides(is_second(), gated(value_head, gate_head), gated(value_tail, gate_tail))
+    swap_in[...] = inner.astype(BF16)
+    swap_out[...] = outer.astype(BF16)
+
+
 def forward_kernel(
-    me, value, gate, inner, outer, taps, gain, wide, unit, inv, slope, normed, conv
+    value, gate, inner, outer, taps, gain, wide, unit, inv, slope, normed, conv
 ):
     lanes = [slice(b * LANES, (b + 1) * LANES) for b in range(2)]
-    before, after = sides(me[1] == 1, inner[...].astype(F32), outer[...].astype(F32))
+    before, after = sides(is_second(), inner[...].astype(F32), outer[...].astype(F32))
     for b in range(2):
         wide[b, 0:PAD, :] = before[:, lanes[b]]
         wide[b, PAD + ROWS : HALO, :] = after[:, lanes[b]]
@@ -108,8 +120,8 @@
     lax.fori_loop(0, ROWS // CHUNK, norm_rows, 0)
 
 
-def early_kernel(me, own, left, right, weight, normed, partial, wgrad):
-    y = me[0]
+def early_kernel(own, left, right, weight, normed, partial, wgrad):
+    y = lax.axis_index("tp")
     blocks = ((own, lax.rem(y, 4)), (left, lax.rem(y + 3, 4)), (right, lax.rem(y + 1, 4)))
     weights = [weight[pl.ds(pl.multiple_of(at * CH, CH), CH), :] for _, at in blocks]
 
@@ -138,9 +150,9 @@
 
 
 def late_kernel(
-    me, far, weight, normed, partial, unit, inv, slope, gain, wide, begun, grad, swap_in, swap_out, sums
+    far, weight, normed, partial, unit, inv, slope, gain, wide, begun, grad, swap_in, swap_out, sums
 ):
-    y = me[0]
+    y = lax.axis_index("tp")
     w = weight[pl.ds(pl.multiple_of(lax.rem(y + 2, 4) * CH, CH), CH), :]
     avg = averaging()
     gain_row = gain[...]
@@ -165,8 +177,10 @@
     for b in range(2):
         cols = slice(b * LANES, (b + 1) * LANES)
         head, tail = grad[b, 0:PAD, :], grad[b, ROWS - PAD : ROWS, :]
-        swap_in[:, cols], swap_out[:, cols] = sides(me[1] == 1, head, tail)
-
+        swap_in[:, cols], swap_out[:, cols] = sides(is_second(), head, tail)
+
+    for peer in range(8):
+        sums[peer, 0:12] = begun[peer]
     put_weight(
         sums,
         3,
@@ -177,18 +191,22 @@
 
     halves = []
     for b in range(2):
-
-        def tile(step, carry, b=b):
-            start = pl.multiple_of(step * 8, 8)
-            g = grad[b, pl.ds(start, 8), :]
-            return tuple(
-                acc + g * wide[b, pl.ds(start + k + 1, 8), :] for k, acc in enumerate(carry)
+        lines = []
+        for group in (range(0, 16), range(16, KW)):
+
+            def tiles(step, carry, b=b, group=group):
+                accs = list(carry)
+                for j in range(4):
+                    start = pl.multiple_of(step * 32, 32) + 8 * j
+                    g = grad[b, pl.ds(start, 8), :]
+                    for i, k in enumerate(group):
+                        accs[i] = accs[i] + g * wide[b, pl.ds(start + k + 1, 8), :]
+                return tuple(accs)
+
+            accs = lax.fori_loop(
+                0, ROWS // 32, tiles, tuple(jnp.zeros((8, LANES), F32) for _ in group)
             )
-
-        accs = lax.fori_loop(
-            0, ROWS // 8, tile, tuple(jnp.zeros((8, LANES), F32) for _ in range(KW))
-        )
-        lines = [jnp.sum(a, axis=0, keepdims=True) for a in accs]
+            lines += [jnp.sum(a, axis=0, keepdims=True) for a in accs]
         halves.append(jnp.concatenate(lines, axis=0))
     taps = jnp.concatenate(
         [
@@ -204,9 +222,9 @@
 
 
 def backward_kernel(
-    me, value, gate, grad, inner, outer, taps, value_grad, gate_grad, wide, conv
+    value, gate, grad, inner, outer, taps, value_grad, gate_grad, wide, conv
 ):
-    before, after = sides(me[1] == 1, inner[...], outer[...])
+    before, after = sides(is_second(), inner[...], outer[...])
     lines = taps[...].astype(F32)
     lanes = [slice(b * LANES, (b + 1) * LANES) for b in range(2)]
     for b in range(2):
@@ -234,8 +252,8 @@
     lax.fori_loop(0, ROWS // 64, finish, 0)
 
 
-def middle_kernel(me, late, out):
-    y = me[0]
+def middle_kernel(late, out):
+    y = lax.axis_index("tp")
     taps = late[0, 16:18].astype(F32)
     for peer in range(1, 8):
         taps = taps + late[peer, 16:18].astype(F32)
@@ -259,14 +277,14 @@
     mine[8:16] = total[2]
 
 
-def last_kernel(me, mine, other, taps, gain):
-    low, high = sides(me[1] == 1, other[...], mine[...])
+def last_kernel(mine, other, taps, gain):
+    low, high = sides(is_second(), other[...], mine[...])
     taps[0:16] = low
     taps[16:31] = high[:15]
     gain[...] = high[15:16]
 
 
-def call(kernel, outs, specs, scratch=(), cost=None, alias={}):
+def call(kernel, outs, specs, scratch=(), cost=None):
     return pl.pallas_call(
         kernel,
         out_shape=outs,
@@ -274,7 +292,6 @@
         out_specs=jax.tree.map(lambda _: VMEM, outs),
         scratch_shapes=scratch,
         cost_estimate=cost,
-        input_output_aliases=alias,
         compiler_params=pltpu.CompilerParams(vmem_limit_bytes=8 * 1024 * 1024),
     )
 
@@ -296,26 +313,26 @@
     pairs = [(i, i ^ 1) for i in range(peers)]
     apart = [(i, i + 1) for i in range(1, peers - 1, 2)]
     apart = apart + [(j, i) for i, j in apart]
-    second = lax.axis_index("c").astype(jnp.int32)
-    me = jnp.stack([lax.axis_index("tp").astype(jnp.int32), second])
     gain = norm_gain.reshape(1, CH)
 
     def exchange(array, axis):
         return lax.all_to_all(array, axis, 0, 0, tiled=True)
 
-    def gated_of(rows):
-        return (
-            value_rows[rows].astype(F32) * jax.nn.sigmoid(gate_rows[rows].astype(F32))
-        ).astype(BF16)
-
-    swap_in, swap_out = sides(
-        second == 1, gated_of(slice(0, PAD)), gated_of(slice(ROWS - PAD, ROWS))
-    )
+    first_rows = pl.BlockSpec((PAD, CH), lambda i: (0, 0))
+    last_rows = pl.BlockSpec((PAD, CH), lambda i: (ROWS // PAD - 1, 0))
+    swap_in, swap_out = pl.pallas_call(
+        edge_kernel,
+        out_shape=(shape(PAD, CH, dtype=BF16),) * 2,
+        grid=(1,),
+        in_specs=[first_rows, first_rows, last_rows, last_rows],
+        out_specs=(first_rows, first_rows),
+        name="edges",
+    )(value_rows, gate_rows, value_rows, gate_rows)
     left = lax.ppermute(out_grad, "tp", ring(4, 1))
     right = lax.ppermute(out_grad, "tp", ring(4, 3))
+    far = lax.ppermute(out_grad, "tp", ring(4, 2))
     inner = lax.ppermute(swap_in, SP, pairs)
     outer = lax.ppermute(swap_out, SP, apart)
-    far = lax.ppermute(out_grad, "tp", ring(4, 2))
 
     wide, unit, inv, slope, normed = call(
         forward_kernel,
@@ -326,18 +343,14 @@
             shape(ROWS, CH),
             shape(ROWS, CH, dtype=BF16),
         ),
-        [SMEM] + [VMEM] * 6,
+        [VMEM] * 6,
         [pltpu.VMEM((ROWS, CH), F32)],
         cost(7),
-    )(me, value_rows, gate_rows, inner, outer, conv_taps, gain)
+    )(value_rows, gate_rows, inner, outer, conv_taps, gain)
 
     partial, wgrad = call(
-        early_kernel,
-        (shape(ROWS, CH), shape(8, 18, 8, CH, dtype=BF16)),
-        [SMEM] + [VMEM] * 5,
-        (),
-        cost(4),
-    )(me, out_grad, left, right, point_weight, normed)
+        early_kernel, (shape(ROWS, CH), shape(8, 12, 8, CH, dtype=BF16)), [VMEM] * 5, (), cost(4)
+    )(out_grad, left, right, point_weight, normed)
 
     grad, swap_in, swap_out, sums = call(
         late_kernel,
@@ -347,32 +360,32 @@
             shape(PAD, CH),
             shape(8, 18, 8, CH, dtype=BF16),
         ),
-        [SMEM] + [VMEM] * 10,
+        [VMEM] * 10,
         (),
         cost(8),
-        {10: 3},
-    )(me, far, point_weight, normed, partial, unit, inv, slope, gain, wide, wgrad)
+    )(far, point_weight, normed, partial, unit, inv, slope, gain, wide, wgrad)
     late = exchange(sums, ("x", "c"))
-
-    sent = call(middle_kernel, shape(16, 3, 8, CH, dtype=BF16), [SMEM, VMEM], (), cost(1))(me, late)
-    got = exchange(sent, "z")
 
     inner = lax.ppermute(swap_in, SP, pairs)
     outer = lax.ppermute(swap_out, SP, apart)
+    late, inner, outer = lax.optimization_barrier((late, inner, outer))
+    sent = call(middle_kernel, shape(16, 3, 8, CH, dtype=BF16), [VMEM], (), cost(1))(late)
+    got = exchange(sent, "z")
+
     value_grad, gate_grad = call(
         backward_kernel,
         (shape(ROWS, CH, dtype=BF16), shape(ROWS, CH, dtype=BF16)),
-        [SMEM] + [VMEM] * 6,
+        [VMEM] * 6,
         [pltpu.VMEM((2, HALO, LANES), F32), pltpu.VMEM((ROWS, CH), F32)],
         cost(6),
-    )(me, value_rows, gate_rows, grad, inner, outer, conv_taps)
+    )(value_rows, gate_rows, grad, inner, outer, conv_taps)
 
     got, value_grad, gate_grad = lax.optimization_barrier((got, value_grad, gate_grad))
     weight_grad, mine = call(whole_kernel, (shape(8, CH), shape(16, CH)), [VMEM], (), cost(1))(got)
     other = lax.ppermute(mine, "c", ring(2, 1))
     taps_grad, gain_grad = call(
-        last_kernel, (shape(KW, CH), shape(1, CH)), [SMEM, VMEM, VMEM], (), cost(1)
-    )(me, mine, other)
+        last_kernel, (shape(KW, CH), shape(1, CH)), [VMEM, VMEM], (), cost(1)
+    )(mine, other)
     return value_grad, gate_grad, taps_grad, gain_grad.reshape(CH), weight_grad
 
 

time: 95 us -> 91.7 us (0.965)
  the two profiles are of different devices: /device:TPU:25 before, /device:TPU:57 now
where the time goes in v3:
time: 91.7 us; the launch traced here: 91.1 us
  starting transfers between devices  48 us (52%)
  Pallas kernels  21.3 us (23%)
  waiting for transfers between devices  20.9 us (23%)
    all_to_all x2, starting transfers between devices, exchange(): return lax.all_to_all(array, axis, 0, 0, tiled=True)  22.7 us
    all_to_all x2, waiting for transfers between devices, exchange(): return lax.all_to_all(array, axis, 0, 0, tiled=True)  11.1 us
    ppermute x2, starting transfers between devices, body(): outer = lax.ppermute(swap_out, SP, apart)  6.66 us
    pallas_call x1, Pallas kernels, body(): call(late_kernel, (shape(2, ROWS, LANES), shape(PAD, CH), shape(PAD, CH),...  6.21 us
    ppermute x2, waiting for transfers between devices, body(): outer = lax.ppermute(swap_out, SP, apart)  6.05 us
    pallas_call x1, Pallas kernels, body(): call(forward_kernel, (shape(2, HALO, LANES), shape(ROWS, CH), shape(ROWS,...  5.56 us
    ppermute x2, starting transfers between devices, body(): inner = lax.ppermute(swap_in, SP, pairs)  5.32 us
    ppermute x1, starting transfers between devices, body(): other = lax.ppermute(mine, 'c', ring(2, 1))  5.05 us
  transfers between devices with their start and end apart: 10, of which 6 were waited for; matrix products, arithmetic and copies ran while one was open for 0% of the time, Pallas kernels for 14%

profile of v3, /device:TPU:57, one launch (start us, length us, event | category | flops | bytes accessed | tf_op | source)
XLA Modules:
  0.0 91.1 jit_solution(9884581507844704379)
XLA Ops:
  0.7 2.1 %collective-permute-start.3 = (bf16[1024,256]{1,0:T(8,128)(2,1)}, bf16[1024,256]{1,0:T(8,128)(2,1)S(1)}, u32[]{:S(2)}, u32[]{:S(2)}) collective-permute-start(bf16[1024,256]{1,0:T(8,128)(2,1)} %own.1), channel_id=1, source_target_pairs={{0,1},{1,2},{2,3},{3,0},{4,5},{5,6},{6,7},{7,4},{8,9},{9,10},{10,1... | collective-permute-start | bytes 1572872 | tf_op jit(solution)/shard_map/ppermute | solution.py:331
  2.7 3.4 %collective-permute-start.4 = (bf16[1024,256]{1,0:T(8,128)(2,1)}, bf16[1024,256]{1,0:T(8,128)(2,1)S(1)}, u32[]{:S(2)}, u32[]{:S(2)}) collective-permute-start(bf16[1024,256]{1,0:T(8,128)(2,1)} %own.1), channel_id=1, source_target_pairs={{0,3},{1,0},{2,1},{3,2},{4,7},{5,4},{6,5},{7,6},{8,11},{9,8},{10,9... | collective-permute-start | bytes 1572872 | tf_op jit(solution)/shard_map/ppermute | solution.py:332
  6.1 2.9 %collective-permute-start = (bf16[1024,256]{1,0:T(8,128)(2,1)}, bf16[1024,256]{1,0:T(8,128)(2,1)S(1)}, u32[]{:S(2)}, u32[]{:S(2)}) collective-permute-start(bf16[1024,256]{1,0:T(8,128)(2,1)} %own.1), channel_id=1, source_target_pairs={{0,2},{1,3},{2,0},{3,1},{4,6},{5,7},{6,4},{7,5},{8,10},{9,11},{10,... | collective-permute-start | bytes 1572872 | tf_op jit(solution)/shard_map/ppermute | solution.py:333
  9.0 1.4 %edges.1 = (bf16[16,256]{1,0:T(8,128)(2,1)}, bf16[16,256]{1,0:T(8,128)(2,1)}) custom-call(bf16[1024,256]{1,0:T(8,128)(2,1)} %value.3, bf16[1024,256]{1,0:T(8,128)(2,1)} %gate.3, bf16[1024,256]{1,0:T(8,128)(2,1)} %value.3, bf16[1024,256]{1,0:T(8,128)(2,1)} %gate.3), custom_call_target="tpu_custom_call" | custom-call | tf_op jit(solution)/shard_map/edges/pallas_call | solution.py:323
  10.3 3.4 %collective-permute-start.1 = (bf16[16,256]{1,0:T(8,128)(2,1)}, bf16[16,256]{1,0:T(8,128)(2,1)S(1)}, u32[]{:S(2)}, u32[]{:S(2)}) collective-permute-start(bf16[16,256]{1,0:T(8,128)(2,1)} %get-tuple-element.30), channel_id=1, source_target_pairs={{0,4},{4,0},{8,12},{12,8},{16,20},{20,16},{24,28},{28,24},{32,36},... | collective-permute-start | bytes 24584 | tf_op jit(solution)/shard_map/ppermute | solution.py:334
  13.8 3.0 %collective-permute-start.2 = (bf16[16,256]{1,0:T(8,128)(2,1)}, bf16[16,256]{1,0:T(8,128)(2,1)S(1)}, u32[]{:S(2)}, u32[]{:S(2)}) collective-permute-start(bf16[16,256]{1,0:T(8,128)(2,1)} %get-tuple-element.31), channel_id=1, source_target_pairs={{4,8},{12,16},{20,24},{28,32},{36,40},{44,48},{52,56},{60,64},{68,... | collective-permute-start | bytes 24584 | tf_op jit(solution)/shard_map/ppermute | solution.py:335
  16.8 2.4 %collective-permute-done.2.outer = bf16[16,256]{1,0:T(8,128)(2,1)S(1)} collective-permute-done((bf16[16,256]{1,0:T(8,128)(2,1)}, bf16[16,256]{1,0:T(8,128)(2,1)S(1)}, u32[]{:S(2)}, u32[]{:S(2)}) %collective-permute-start.2) | collective-permute-done | bytes 8224 | tf_op jit(solution)/shard_map/ppermute | solution.py:335
  19.3 5.6 %shard_map.101 = (f32[2,1056,128]{2,1,0:T(8,128)S(1)}, f32[1024,256]{1,0:T(8,128)S(1)}, f32[1024,256]{1,0:T(8,128)S(1)}, f32[1024,256]{1,0:T(8,128)S(1)}, bf16[1024,256]{1,0:T(8,128)(2,1)S(1)}) custom-call(bf16[1024,256]{1,0:T(8,128)(2,1)S(1)} %copy-done, bf16[1024,256]{1,0:T(8,128)(2,1)S(1)} %copy-done.1, bf16[16,256]{1,0:T(8,128)(2,1)S(1)} %collective-permute-done.1.inner, ...), custom_call_target="tpu_custom_call" | custom-call | flops 1400000000 | bytes 1048576 | tf_op jit(solution)/shard_map/pallas_call | solution.py:337
  24.9 1.8 %shard_map.102 = (f32[1024,256]{1,0:T(8,128)S(1)}, bf16[8,12,8,256]{3,2,1,0:T(8,128)(2,1)S(1)}) custom-call(bf16[1024,256]{1,0:T(8,128)(2,1)S(1)} %copy-done.4, bf16[1024,256]{1,0:T(8,128)(2,1)S(1)} %collective-permute-done.3.left, bf16[1024,256]{1,0:T(8,128)(2,1)S(1)} %collective-permute-done.4.right, bf16[1024,256]{1,0:T(8,128)(2,1)S(1)} %copy-done.2, ...), custom_call_target="tpu_custom_call" | custom-call | flops 800000000 | bytes 1048576 | tf_op jit(solution)/shard_map/pallas_call | solution.py:351
  26.7 2.9 %collective-permute-done.far = bf16[1024,256]{1,0:T(8,128)(2,1)S(1)} collective-permute-done((bf16[1024,256]{1,0:T(8,128)(2,1)}, bf16[1024,256]{1,0:T(8,128)(2,1)S(1)}, u32[]{:S(2)}, u32[]{:S(2)}) %collective-permute-start) | collective-permute-done | bytes 524320 | tf_op jit(solution)/shard_map/ppermute | solution.py:333
  29.6 6.2 %shard_map.103 = (f32[2,1024,128]{2,1,0:T(8,128)S(1)}, f32[16,256]{1,0:T(8,128)S(1)}, f32[16,256]{1,0:T(8,128)S(1)}, bf16[8,18,8,256]{3,2,1,0:T(8,128)(2,1)}) custom-call(bf16[1024,256]{1,0:T(8,128)(2,1)S(1)} %collective-permute-done.far, bf16[1024,256]{1,0:T(8,128)(2,1)S(1)} %copy-done.2, bf16[1024,256]{1,0:T(8,128)(2,1)S(1)} %get-tuple-element.32.normed, ...), custom_call_target="tpu_custom_call" | custom-call | flops 1600000000 | bytes 1048576 | tf_op jit(solution)/shard_map/pallas_call | solution.py:355
  35.8 8.1 %all-to-all-start = ((bf16[8,18,8,256]{3,2,1,0:T(8,128)(2,1)}), bf16[8,18,8,256]{3,2,1,0:T(8,128)(2,1)S(1)}, u32[]{:S(2)}, u32[]{:S(2)}) async-start(bf16[8,18,8,256]{3,2,1,0:T(8,128)(2,1)} %get-tuple-element.39), calls=%async_computation | async-start | bytes 1179648 | tf_op jit(solution)/shard_map/all_to_all | solution.py:319
  43.9 1.9 %collective-permute-start.5 = (f32[16,256]{1,0:T(8,128)S(1)}, f32[16,256]{1,0:T(8,128)S(1)}, u32[]{:S(2)}, u32[]{:S(2)}) collective-permute-start(f32[16,256]{1,0:T(8,128)S(1)} %get-tuple-element.40), channel_id=1, source_target_pairs={{0,4},{4,0},{8,12},{12,8},{16,20},{20,16},{24,28},{28,24},{32,36},... | collective-permute-start | bytes 49160 | tf_op jit(solution)/shard_map/ppermute | solution.py:369
  45.8 3.6 %collective-permute-start.6 = (f32[16,256]{1,0:T(8,128)S(1)}, f32[16,256]{1,0:T(8,128)S(1)}, u32[]{:S(2)}, u32[]{:S(2)}) collective-permute-start(f32[16,256]{1,0:T(8,128)S(1)} %get-tuple-element.41), channel_id=1, source_target_pairs={{4,8},{12,16},{20,24},{28,32},{36,40},{44,48},{52,56},{60,64},{68,... | collective-permute-start | bytes 49160 | tf_op jit(solution)/shard_map/ppermute | solution.py:370
  49.5 3.6 %collective-permute-done.6.outer = f32[16,256]{1,0:T(8,128)S(1)} collective-permute-done((f32[16,256]{1,0:T(8,128)S(1)}, f32[16,256]{1,0:T(8,128)S(1)}, u32[]{:S(2)}, u32[]{:S(2)}) %collective-permute-start.6) | collective-permute-done | bytes 16416 | tf_op jit(solution)/shard_map/ppermute | solution.py:370
  53.1 0.9 all-to-all-done.late
  54.0 0.8 shard_map.104
  54.7 14.6 %all-to-all-start.1 = ((bf16[16,3,8,256]{3,2,1,0:T(8,128)(2,1)}), bf16[16,3,8,256]{3,2,1,0:T(8,128)(2,1)S(1)}, u32[]{:S(2)}, u32[]{:S(2)}) async-start(bf16[16,3,8,256]{3,2,1,0:T(8,128)(2,1)} %shard_map.104), calls=%async_computation.1 | async-start | bytes 393216 | tf_op jit(solution)/shard_map/all_to_all | solution.py:319
  69.4 4.4 %shard_map.105 = (bf16[1024,256]{1,0:T(8,128)(2,1)}, bf16[1024,256]{1,0:T(8,128)(2,1)}) custom-call(bf16[1024,256]{1,0:T(8,128)(2,1)S(1)} %copy-done, bf16[1024,256]{1,0:T(8,128)(2,1)S(1)} %copy-done.1, f32[2,1024,128]{2,1,0:T(8,128)S(1)} %get-tuple-element.43.grad, f32[16,256]{1,0:T(8,128)S(1)} %collective-permute-done.5.inner, ...), custom_call_target="tpu_custom_call" | custom-call | flops 1200000000 | bytes 1048576 | tf_op jit(solution)/shard_map/pallas_call | solution.py:375
  73.8 10.2 %all-to-all-done.1.got = bf16[16,3,8,256]{3,2,1,0:T(8,128)(2,1)S(1)} async-done(((bf16[16,3,8,256]{3,2,1,0:T(8,128)(2,1)}), bf16[16,3,8,256]{3,2,1,0:T(8,128)(2,1)S(1)}, u32[]{:S(2)}, u32[]{:S(2)}) %all-to-all-start.1) | async-done | bytes 196640 | tf_op jit(solution)/shard_map/all_to_all | solution.py:319
  84.0 0.6 shard_map.106
  84.6 5.1 %collective-permute-start.7 = (f32[16,256]{1,0:T(8,128)S(1)}, f32[16,256]{1,0:T(8,128)S(1)}, u32[]{:S(2)}, u32[]{:S(2)}) collective-permute-start(f32[16,256]{1,0:T(8,128)S(1)} %get-tuple-element.51.mine), channel_id=1, source_target_pairs={{0,4},{4,0},{1,5},{5,1},{2,6},{6,2},{3,7},{7,3},{8,12},{12,8},{9,1... | collective-permute-start | bytes 49160 | tf_op jit(solution)/shard_map/ppermute | solution.py:385
  89.7 0.8 collective-permute-done.7.other
  90.5 0.6 shard_map.107
  (16 shorter events, 0.0 us)
Async XLA Ops:
  0.6 18.6 %copy-start.1 = (bf16[1024,256]{1,0:T(8,128)(2,1)S(1)}, bf16[1024,256]{1,0:T(8,128)(2,1)}, u32[]{:S(2)}) copy-start(bf16[1024,256]{1,0:T(8,128)(2,1)} %gate.3) | copy-start | bytes 1572868
  0.6 18.6 %copy-start = (bf16[1024,256]{1,0:T(8,128)(2,1)S(1)}, bf16[1024,256]{1,0:T(8,128)(2,1)}, u32[]{:S(2)}) copy-start(bf16[1024,256]{1,0:T(8,128)(2,1)} %value.3) | copy-start | bytes 1572868
  0.7 18.6 %copy-start.5 = (bf16[31,256]{1,0:T(8,128)(2,1)S(1)}, bf16[31,256]{1,0:T(8,128)(2,1)}, u32[]{:S(2)}) copy-start(bf16[31,256]{1,0:T(8,128)(2,1)} %taps.3) | copy-start | bytes 47620
  0.7 18.6 %copy-start.3 = (f32[256]{0:T(256)S(1)}, f32[256]{0:T(256)}, u32[]{:S(2)}) copy-start(f32[256]{0:T(256)} %param.9) | copy-start | bytes 3076
  0.7 24.2 %collective-permute-start.3 = (bf16[1024,256]{1,0:T(8,128)(2,1)}, bf16[1024,256]{1,0:T(8,128)(2,1)S(1)}, u32[]{:S(2)}, u32[]{:S(2)}) collective-permute-start(bf16[1024,256]{1,0:T(8,128)(2,1)} %own.1), channel_id=1, source_target_pairs={{0,1},{1,2},{2,3},{3,0},{4,5},{5,6},{6,7},{7,4},{8,9},{9,10},{10,1... | collective-permute-start | bytes 1572872 | tf_op jit(solution)/shard_map/ppermute | solution.py:331
  2.7 22.1 %collective-permute-start.4 = (bf16[1024,256]{1,0:T(8,128)(2,1)}, bf16[1024,256]{1,0:T(8,128)(2,1)S(1)}, u32[]{:S(2)}, u32[]{:S(2)}) collective-permute-start(bf16[1024,256]{1,0:T(8,128)(2,1)} %own.1), channel_id=1, source_target_pairs={{0,3},{1,0},{2,1},{3,2},{4,7},{5,4},{6,5},{7,6},{8,11},{9,8},{10,9... | collective-permute-start | bytes 1572872 | tf_op jit(solution)/shard_map/ppermute | solution.py:332
  6.1 23.5 %collective-permute-start = (bf16[1024,256]{1,0:T(8,128)(2,1)}, bf16[1024,256]{1,0:T(8,128)(2,1)S(1)}, u32[]{:S(2)}, u32[]{:S(2)}) collective-permute-start(bf16[1024,256]{1,0:T(8,128)(2,1)} %own.1), channel_id=1, source_target_pairs={{0,2},{1,3},{2,0},{3,1},{4,6},{5,7},{6,4},{7,5},{8,10},{9,11},{10,... | collective-permute-start | bytes 1572872 | tf_op jit(solution)/shard_map/ppermute | solution.py:333
  10.3 6.4 %collective-permute-start.1 = (bf16[16,256]{1,0:T(8,128)(2,1)}, bf16[16,256]{1,0:T(8,128)(2,1)S(1)}, u32[]{:S(2)}, u32[]{:S(2)}) collective-permute-start(bf16[16,256]{1,0:T(8,128)(2,1)} %get-tuple-element.30), channel_id=1, source_target_pairs={{0,4},{4,0},{8,12},{12,8},{16,20},{20,16},{24,28},{28,24},{32,36},... | collective-permute-start | bytes 24584 | tf_op jit(solution)/shard_map/ppermute | solution.py:334
  13.8 5.5 %collective-permute-start.2 = (bf16[16,256]{1,0:T(8,128)(2,1)}, bf16[16,256]{1,0:T(8,128)(2,1)S(1)}, u32[]{:S(2)}, u32[]{:S(2)}) collective-permute-start(bf16[16,256]{1,0:T(8,128)(2,1)} %get-tuple-element.31), channel_id=1, source_target_pairs={{4,8},{12,16},{20,24},{28,32},{36,40},{44,48},{52,56},{60,64},{68,... | collective-permute-start | bytes 24584 | tf_op jit(solution)/shard_map/ppermute | solution.py:335
  19.3 5.6 %copy-start.2 = (bf16[1024,256]{1,0:T(8,128)(2,1)S(1)}, bf16[1024,256]{1,0:T(8,128)(2,1)}, u32[]{:S(2)}) copy-start(bf16[1024,256]{1,0:T(8,128)(2,1)} %weight.3) | copy-start | bytes 1572868
  19.3 5.6 %copy-start.4 = (bf16[1024,256]{1,0:T(8,128)(2,1)S(1)}, bf16[1024,256]{1,0:T(8,128)(2,1)}, u32[]{:S(2)}) copy-start(bf16[1024,256]{1,0:T(8,128)(2,1)} %own.1) | copy-start | bytes 1572868
  35.8 18.2 %all-to-all-start = ((bf16[8,18,8,256]{3,2,1,0:T(8,128)(2,1)}), bf16[8,18,8,256]{3,2,1,0:T(8,128)(2,1)S(1)}, u32[]{:S(2)}, u32[]{:S(2)}) async-start(bf16[8,18,8,256]{3,2,1,0:T(8,128)(2,1)} %get-tuple-element.39), calls=%async_computation | async-start | bytes 1179648 | tf_op jit(solution)/shard_map/all_to_all | solution.py:319
  43.9 5.6 %collective-permute-start.5 = (f32[16,256]{1,0:T(8,128)S(1)}, f32[16,256]{1,0:T(8,128)S(1)}, u32[]{:S(2)}, u32[]{:S(2)}) collective-permute-start(f32[16,256]{1,0:T(8,128)S(1)} %get-tuple-element.40), channel_id=1, source_target_pairs={{0,4},{4,0},{8,12},{12,8},{16,20},{20,16},{24,28},{28,24},{32,36},... | collective-permute-start | bytes 49160 | tf_op jit(solution)/shard_map/ppermute | solution.py:369
  45.8 7.3 %collective-permute-start.6 = (f32[16,256]{1,0:T(8,128)S(1)}, f32[16,256]{1,0:T(8,128)S(1)}, u32[]{:S(2)}, u32[]{:S(2)}) collective-permute-start(f32[16,256]{1,0:T(8,128)S(1)} %get-tuple-element.41), channel_id=1, source_target_pairs={{4,8},{12,16},{20,24},{28,32},{36,40},{44,48},{52,56},{60,64},{68,... | collective-permute-start | bytes 49160 | tf_op jit(solution)/shard_map/ppermute | solution.py:370
  54.7 29.3 %all-to-all-start.1 = ((bf16[16,3,8,256]{3,2,1,0:T(8,128)(2,1)}), bf16[16,3,8,256]{3,2,1,0:T(8,128)(2,1)S(1)}, u32[]{:S(2)}, u32[]{:S(2)}) async-start(bf16[16,3,8,256]{3,2,1,0:T(8,128)(2,1)} %shard_map.104), calls=%async_computation.1 | async-start | bytes 393216 | tf_op jit(solution)/shard_map/all_to_all | solution.py:319
  84.6 5.9 %collective-permute-start.7 = (f32[16,256]{1,0:T(8,128)S(1)}, f32[16,256]{1,0:T(8,128)S(1)}, u32[]{:S(2)}, u32[]{:S(2)}) collective-permute-start(f32[16,256]{1,0:T(8,128)S(1)} %get-tuple-element.51.mine), channel_id=1, source_target_pairs={{0,4},{4,0},{1,5},{5,1},{2,6},{6,2},{3,7},{7,3},{8,12},{12,8},{9,1... | collective-permute-start | bytes 49160 | tf_op jit(solution)/shard_map/ppermute | solution.py:385

commit v4 on v3

--- a/solution.py
+++ b/solution.py
@@ -37,7 +37,7 @@
 
 
 def convolve(src, taps_at, store):
-    tiles = 4
+    tiles = 8
     for block in range(CH // LANES):
 
         def some_rows(step, _, block=block):
@@ -63,20 +63,26 @@
     return jnp.where(second, inner, outer), jnp.where(second, outer, inner)
 
 
-def edge_kernel(value_head, gate_head, value_tail, gate_tail, swap_in, swap_out):
+def neighbours(inner, outer):
+    second = is_second()
+    before = jnp.where(second, inner[PAD : 2 * PAD].astype(F32), outer[PAD : 2 * PAD].astype(F32))
+    after = jnp.where(second, outer[0:PAD].astype(F32), inner[0:PAD].astype(F32))
+    return before, after
+
+
+def edge_kernel(value_head, gate_head, value_tail, gate_tail, edges):
     def gated(value, gate):
-        return value[...].astype(F32) * jax.nn.sigmoid(gate[...].astype(F32))
-
-    inner, outer = sides(is_second(), gated(value_head, gate_head), gated(value_tail, gate_tail))
-    swap_in[...] = inner.astype(BF16)
-    swap_out[...] = outer.astype(BF16)
+        return (value[...].astype(F32) * jax.nn.sigmoid(gate[...].astype(F32))).astype(BF16)
+
+    edges[0:PAD, :] = gated(value_head, gate_head)
+    edges[PAD : 2 * PAD, :] = gated(value_tail, gate_tail)
 
 
 def forward_kernel(
     value, gate, inner, outer, taps, gain, wide, unit, inv, slope, normed, conv
 ):
     lanes = [slice(b * LANES, (b + 1) * LANES) for b in range(2)]
-    before, after = sides(is_second(), inner[...].astype(F32), outer[...].astype(F32))
+    before, after = neighbours(inner, outer)
     for b in range(2):
         wide[b, 0:PAD, :] = before[:, lanes[b]]
         wide[b, PAD + ROWS : HALO, :] = after[:, lanes[b]]
@@ -150,7 +156,7 @@
 
 
 def late_kernel(
-    far, weight, normed, partial, unit, inv, slope, gain, wide, begun, grad, swap_in, swap_out, sums
+    far, weight, normed, partial, unit, inv, slope, gain, wide, begun, grad, ends, sums
 ):
     y = lax.axis_index("tp")
     w = weight[pl.ds(pl.multiple_of(lax.rem(y + 2, 4) * CH, CH), CH), :]
@@ -176,8 +182,8 @@
     gain_sum = lax.fori_loop(0, ROWS // CHUNK, some_rows, jnp.zeros((8, CH), F32))
     for b in range(2):
         cols = slice(b * LANES, (b + 1) * LANES)
-        head, tail = grad[b, 0:PAD, :], grad[b, ROWS - PAD : ROWS, :]
-        swap_in[:, cols], swap_out[:, cols] = sides(is_second(), head, tail)
+        ends[0:PAD, cols] = grad[b, 0:PAD, :]
+        ends[PAD : 2 * PAD, cols] = grad[b, ROWS - PAD : ROWS, :]
 
     for peer in range(8):
         sums[peer, 0:12] = begun[peer]
@@ -224,7 +230,7 @@
 def backward_kernel(
     value, gate, grad, inner, outer, taps, value_grad, gate_grad, wide, conv
 ):
-    before, after = sides(is_second(), inner[...], outer[...])
+    before, after = neighbours(inner, outer)
     lines = taps[...].astype(F32)
     lanes = [slice(b * LANES, (b + 1) * LANES) for b in range(2)]
     for b in range(2):
@@ -320,19 +326,19 @@
 
     first_rows = pl.BlockSpec((PAD, CH), lambda i: (0, 0))
     last_rows = pl.BlockSpec((PAD, CH), lambda i: (ROWS // PAD - 1, 0))
-    swap_in, swap_out = pl.pallas_call(
+    edges = pl.pallas_call(
         edge_kernel,
-        out_shape=(shape(PAD, CH, dtype=BF16),) * 2,
+        out_shape=shape(2 * PAD, CH, dtype=BF16),
         grid=(1,),
         in_specs=[first_rows, first_rows, last_rows, last_rows],
-        out_specs=(first_rows, first_rows),
+        out_specs=pl.BlockSpec((2 * PAD, CH), lambda i: (0, 0)),
         name="edges",
     )(value_rows, gate_rows, value_rows, gate_rows)
     left = lax.ppermute(out_grad, "tp", ring(4, 1))
     right = lax.ppermute(out_grad, "tp", ring(4, 3))
+    inner = lax.ppermute(edges, SP, pairs)
+    outer = lax.ppermute(edges, SP, apart)
     far = lax.ppermute(out_grad, "tp", ring(4, 2))
-    inner = lax.ppermute(swap_in, SP, pairs)
-    outer = lax.ppermute(swap_out, SP, apart)
 
     wide, unit, inv, slope, normed = call(
         forward_kernel,
@@ -352,12 +358,11 @@
         early_kernel, (shape(ROWS, CH), shape(8, 12, 8, CH, dtype=BF16)), [VMEM] * 5, (), cost(4)
     )(out_grad, left, right, point_weight, normed)
 
-    grad, swap_in, swap_out, sums = call(
+    grad, ends, sums = call(
         late_kernel,
         (
             shape(2, ROWS, LANES),
-            shape(PAD, CH),
-            shape(PAD, CH),
+            shape(2 * PAD, CH),
             shape(8, 18, 8, CH, dtype=BF16),
         ),
         [VMEM] * 10,
@@ -366,8 +371,8 @@
     )(far, point_weight, normed, partial, unit, inv, slope, gain, wide, wgrad)
     late = exchange(sums, ("x", "c"))
 
-    inner = lax.ppermute(swap_in, SP, pairs)
-    outer = lax.ppermute(swap_out, SP, apart)
+    inner = lax.ppermute(ends, SP, pairs)
+    outer = lax.ppermute(ends, SP, apart)
     late, inner, outer = lax.optimization_barrier((late, inner, outer))
     sent = call(middle_kernel, shape(16, 3, 8, CH, dtype=BF16), [VMEM], (), cost(1))(late)
     got = exchange(sent, "z")

time: 91.7 us -> 91.9 us (level)
  starting transfers between devices: 48 us -> 49.3 us
    ppermute x1, waiting for transfers between devices: 2.93 us -> 4.37 us  [body(): far = lax.ppermute(out_grad, 'tp', ring(4, 2))]
    ppermute x4, waiting for transfers between devices: 6.05 us -> 4.8 us  [the longest x1 3.44 us: body(): outer = lax.ppermute(ends, SP, apart)]
where the time goes in v4:
time: 91.9 us; the launch traced here: 91.3 us
  starting transfers between devices  49.3 us (54%)
  Pallas kernels  20.6 us (22%)
  waiting for transfers between devices  20.5 us (22%)
    all_to_all x2, starting transfers between devices, exchange(): return lax.all_to_all(array, axis, 0, 0, tiled=True)  22.7 us
    all_to_all x2, waiting for transfers between devices, exchange(): return lax.all_to_all(array, axis, 0, 0, tiled=True)  10.5 us
    pallas_call x1, Pallas kernels, body(): call(late_kernel, (shape(2, ROWS, LANES), shape(2 * PAD, CH), shape(8, 18...  6.21 us
    ppermute x1, starting transfers between devices, body(): other = lax.ppermute(mine, 'c', ring(2, 1))  5.54 us
    pallas_call x1, Pallas kernels, body(): call(forward_kernel, (shape(2, HALO, LANES), shape(ROWS, CH), shape(ROWS,...  5.21 us
    ppermute x1, starting transfers between devices, body(): outer = lax.ppermute(edges, SP, apart)  4.51 us
    ppermute x1, waiting for transfers between devices, body(): far = lax.ppermute(out_grad, 'tp', ring(4, 2))  4.37 us
    pallas_call x1, Pallas kernels, body(): call(backward_kernel, (shape(ROWS, CH, dtype=BF16), shape(ROWS, CH, dtype...  4.08 us
  transfers between devices with their start and end apart: 10, of which 6 were waited for; matrix products, arithmetic and copies ran while one was open for 0% of the time, Pallas kernels for 14%

profile of v4, /device:TPU:57, one launch (start us, length us, event | category | flops | bytes accessed | tf_op | source)
XLA Modules:
  0.0 91.3 jit_solution(14843601787550031235)
XLA Ops:
  0.7 2.1 %collective-permute-start.3 = (bf16[1024,256]{1,0:T(8,128)(2,1)}, bf16[1024,256]{1,0:T(8,128)(2,1)S(1)}, u32[]{:S(2)}, u32[]{:S(2)}) collective-permute-start(bf16[1024,256]{1,0:T(8,128)(2,1)} %own.1), channel_id=1, source_target_pairs={{0,1},{1,2},{2,3},{3,0},{4,5},{5,6},{6,7},{7,4},{8,9},{9,10},{10,1... | collective-permute-start | bytes 1572872 | tf_op jit(solution)/shard_map/ppermute | solution.py:337
  2.7 3.4 %collective-permute-start.4 = (bf16[1024,256]{1,0:T(8,128)(2,1)}, bf16[1024,256]{1,0:T(8,128)(2,1)S(1)}, u32[]{:S(2)}, u32[]{:S(2)}) collective-permute-start(bf16[1024,256]{1,0:T(8,128)(2,1)} %own.1), channel_id=1, source_target_pairs={{0,3},{1,0},{2,1},{3,2},{4,7},{5,4},{6,5},{7,6},{8,11},{9,8},{10,9... | collective-permute-start | bytes 1572872 | tf_op jit(solution)/shard_map/ppermute | solution.py:338
  6.1 2.9 %collective-permute-start = (bf16[1024,256]{1,0:T(8,128)(2,1)}, bf16[1024,256]{1,0:T(8,128)(2,1)S(1)}, u32[]{:S(2)}, u32[]{:S(2)}) collective-permute-start(bf16[1024,256]{1,0:T(8,128)(2,1)} %own.1), channel_id=1, source_target_pairs={{0,2},{1,3},{2,0},{3,1},{4,6},{5,7},{6,4},{7,5},{8,10},{9,11},{10,... | collective-permute-start | bytes 1572872 | tf_op jit(solution)/shard_map/ppermute | solution.py:341
  9.0 1.4 %edges.1 = bf16[32,256]{1,0:T(8,128)(2,1)} custom-call(bf16[1024,256]{1,0:T(8,128)(2,1)} %value.3, bf16[1024,256]{1,0:T(8,128)(2,1)} %gate.3, bf16[1024,256]{1,0:T(8,128)(2,1)} %value.3, bf16[1024,256]{1,0:T(8,128)(2,1)} %gate.3), custom_call_target="tpu_custom_call" | custom-call | tf_op jit(solution)/shard_map/edges/pallas_call | solution.py:329
  10.3 4.5 %collective-permute-start.2 = (bf16[32,256]{1,0:T(8,128)(2,1)}, bf16[32,256]{1,0:T(8,128)(2,1)S(1)}, u32[]{:S(2)}, u32[]{:S(2)}) collective-permute-start(bf16[32,256]{1,0:T(8,128)(2,1)} %edges.1), channel_id=1, source_target_pairs={{4,8},{12,16},{20,24},{28,32},{36,40},{44,48},{52,56},{60,64},{68,... | collective-permute-start | bytes 49160 | tf_op jit(solution)/shard_map/ppermute | solution.py:340
  14.9 1.9 %collective-permute-start.1 = (bf16[32,256]{1,0:T(8,128)(2,1)}, bf16[32,256]{1,0:T(8,128)(2,1)S(1)}, u32[]{:S(2)}, u32[]{:S(2)}) collective-permute-start(bf16[32,256]{1,0:T(8,128)(2,1)} %edges.1), channel_id=1, source_target_pairs={{0,4},{4,0},{8,12},{12,8},{16,20},{20,16},{24,28},{28,24},{32,36},... | collective-permute-start | bytes 49160 | tf_op jit(solution)/shard_map/ppermute | solution.py:339
  16.8 1.3 %collective-permute-done.1.inner = bf16[32,256]{1,0:T(8,128)(2,1)S(1)} collective-permute-done((bf16[32,256]{1,0:T(8,128)(2,1)}, bf16[32,256]{1,0:T(8,128)(2,1)S(1)}, u32[]{:S(2)}, u32[]{:S(2)}) %collective-permute-start.1) | collective-permute-done | bytes 16416 | tf_op jit(solution)/shard_map/ppermute | solution.py:339
  18.2 5.2 %shard_map.101 = (f32[2,1056,128]{2,1,0:T(8,128)S(1)}, f32[1024,256]{1,0:T(8,128)S(1)}, f32[1024,256]{1,0:T(8,128)S(1)}, f32[1024,256]{1,0:T(8,128)S(1)}, bf16[1024,256]{1,0:T(8,128)(2,1)S(1)}) custom-call(bf16[1024,256]{1,0:T(8,128)(2,1)S(1)} %copy-done, bf16[1024,256]{1,0:T(8,128)(2,1)S(1)} %copy-done.1, bf16[32,256]{1,0:T(8,128)(2,1)S(1)} %collective-permute-done.1.inner, ...), custom_call_target="tpu_custom_call" | custom-call | flops 1400000000 | bytes 1048576 | tf_op jit(solution)/shard_map/pallas_call | solution.py:343
  23.5 1.8 %shard_map.102 = (f32[1024,256]{1,0:T(8,128)S(1)}, bf16[8,12,8,256]{3,2,1,0:T(8,128)(2,1)S(1)}) custom-call(bf16[1024,256]{1,0:T(8,128)(2,1)S(1)} %copy-done.4, bf16[1024,256]{1,0:T(8,128)(2,1)S(1)} %collective-permute-done.3.left, bf16[1024,256]{1,0:T(8,128)(2,1)S(1)} %collective-permute-done.4.right, bf16[1024,256]{1,0:T(8,128)(2,1)S(1)} %copy-done.2, ...), custom_call_target="tpu_custom_call" | custom-call | flops 800000000 | bytes 1048576 | tf_op jit(solution)/shard_map/pallas_call | solution.py:357
  25.2 4.4 %collective-permute-done.far = bf16[1024,256]{1,0:T(8,128)(2,1)S(1)} collective-permute-done((bf16[1024,256]{1,0:T(8,128)(2,1)}, bf16[1024,256]{1,0:T(8,128)(2,1)S(1)}, u32[]{:S(2)}, u32[]{:S(2)}) %collective-permute-start) | collective-permute-done | bytes 524320 | tf_op jit(solution)/shard_map/ppermute | solution.py:341
  29.6 6.2 %shard_map.103 = (f32[2,1024,128]{2,1,0:T(8,128)S(1)}, f32[32,256]{1,0:T(8,128)S(1)}, bf16[8,18,8,256]{3,2,1,0:T(8,128)(2,1)}) custom-call(bf16[1024,256]{1,0:T(8,128)(2,1)S(1)} %collective-permute-done.far, bf16[1024,256]{1,0:T(8,128)(2,1)S(1)} %copy-done.2, bf16[1024,256]{1,0:T(8,128)(2,1)S(1)} %get-tuple-element.27.normed, ...), custom_call_target="tpu_custom_call" | custom-call | flops 1600000000 | bytes 1048576 | tf_op jit(solution)/shard_map/pallas_call | solution.py:361
  35.8 8.1 %all-to-all-start = ((bf16[8,18,8,256]{3,2,1,0:T(8,128)(2,1)}), bf16[8,18,8,256]{3,2,1,0:T(8,128)(2,1)S(1)}, u32[]{:S(2)}, u32[]{:S(2)}) async-start(bf16[8,18,8,256]{3,2,1,0:T(8,128)(2,1)} %get-tuple-element.34), calls=%async_computation | async-start | bytes 1179648 | tf_op jit(solution)/shard_map/all_to_all | solution.py:325
  43.9 3.5 %collective-permute-start.6 = (f32[32,256]{1,0:T(8,128)S(1)}, f32[32,256]{1,0:T(8,128)S(1)}, u32[]{:S(2)}, u32[]{:S(2)}) collective-permute-start(f32[32,256]{1,0:T(8,128)S(1)} %get-tuple-element.35), channel_id=1, source_target_pairs={{4,8},{12,16},{20,24},{28,32},{36,40},{44,48},{52,56},{60,64},{68,... | collective-permute-start | bytes 98312 | tf_op jit(solution)/shard_map/ppermute | solution.py:375
  47.4 2.8 %collective-permute-start.5 = (f32[32,256]{1,0:T(8,128)S(1)}, f32[32,256]{1,0:T(8,128)S(1)}, u32[]{:S(2)}, u32[]{:S(2)}) collective-permute-start(f32[32,256]{1,0:T(8,128)S(1)} %get-tuple-element.35), channel_id=1, source_target_pairs={{0,4},{4,0},{8,12},{12,8},{16,20},{20,16},{24,28},{28,24},{32,36},... | collective-permute-start | bytes 98312 | tf_op jit(solution)/shard_map/ppermute | solution.py:374
  50.2 3.4 %collective-permute-done.6.outer = f32[32,256]{1,0:T(8,128)S(1)} collective-permute-done((f32[32,256]{1,0:T(8,128)S(1)}, f32[32,256]{1,0:T(8,128)S(1)}, u32[]{:S(2)}, u32[]{:S(2)}) %collective-permute-start.6) | collective-permute-done | bytes 32800 | tf_op jit(solution)/shard_map/ppermute | solution.py:375
  53.7 0.3 all-to-all-done.late
  54.0 0.7 shard_map.104
  54.7 14.6 %all-to-all-start.1 = ((bf16[16,3,8,256]{3,2,1,0:T(8,128)(2,1)}), bf16[16,3,8,256]{3,2,1,0:T(8,128)(2,1)S(1)}, u32[]{:S(2)}, u32[]{:S(2)}) async-start(bf16[16,3,8,256]{3,2,1,0:T(8,128)(2,1)} %shard_map.104), calls=%async_computation.1 | async-start | bytes 393216 | tf_op jit(solution)/shard_map/all_to_all | solution.py:325
  69.3 4.1 %shard_map.105 = (bf16[1024,256]{1,0:T(8,128)(2,1)}, bf16[1024,256]{1,0:T(8,128)(2,1)}) custom-call(bf16[1024,256]{1,0:T(8,128)(2,1)S(1)} %copy-done, bf16[1024,256]{1,0:T(8,128)(2,1)S(1)} %copy-done.1, f32[2,1024,128]{2,1,0:T(8,128)S(1)} %get-tuple-element.37.grad, f32[32,256]{1,0:T(8,128)S(1)} %collective-permute-done.5.inner, ...), custom_call_target="tpu_custom_call" | custom-call | flops 1200000000 | bytes 1048576 | tf_op jit(solution)/shard_map/pallas_call | solution.py:380
  73.4 10.3 %all-to-all-done.1.got = bf16[16,3,8,256]{3,2,1,0:T(8,128)(2,1)S(1)} async-done(((bf16[16,3,8,256]{3,2,1,0:T(8,128)(2,1)}), bf16[16,3,8,256]{3,2,1,0:T(8,128)(2,1)S(1)}, u32[]{:S(2)}, u32[]{:S(2)}) %all-to-all-start.1) | async-done | bytes 196640 | tf_op jit(solution)/shard_map/all_to_all | solution.py:325
  83.7 0.6 shard_map.106
  84.3 5.5 %collective-permute-start.7 = (f32[16,256]{1,0:T(8,128)S(1)}, f32[16,256]{1,0:T(8,128)S(1)}, u32[]{:S(2)}, u32[]{:S(2)}) collective-permute-start(f32[16,256]{1,0:T(8,128)S(1)} %get-tuple-element.45.mine), channel_id=1, source_target_pairs={{0,4},{4,0},{1,5},{5,1},{2,6},{6,2},{3,7},{7,3},{8,12},{12,8},{9,1... | collective-permute-start | bytes 49160 | tf_op jit(solution)/shard_map/ppermute | solution.py:390
  89.9 0.8 collective-permute-done.7.other
  90.7 0.6 shard_map.107
  (16 shorter events, 0.0 us)
Async XLA Ops:
  0.6 17.5 %copy-start.1 = (bf16[1024,256]{1,0:T(8,128)(2,1)S(1)}, bf16[1024,256]{1,0:T(8,128)(2,1)}, u32[]{:S(2)}) copy-start(bf16[1024,256]{1,0:T(8,128)(2,1)} %gate.3) | copy-start | bytes 1572868
  0.6 17.5 %copy-start = (bf16[1024,256]{1,0:T(8,128)(2,1)S(1)}, bf16[1024,256]{1,0:T(8,128)(2,1)}, u32[]{:S(2)}) copy-start(bf16[1024,256]{1,0:T(8,128)(2,1)} %value.3) | copy-start | bytes 1572868
  0.7 17.5 %copy-start.5 = (bf16[31,256]{1,0:T(8,128)(2,1)S(1)}, bf16[31,256]{1,0:T(8,128)(2,1)}, u32[]{:S(2)}) copy-start(bf16[31,256]{1,0:T(8,128)(2,1)} %taps.3) | copy-start | bytes 47620
  0.7 17.5 %copy-start.3 = (f32[256]{0:T(256)S(1)}, f32[256]{0:T(256)}, u32[]{:S(2)}) copy-start(f32[256]{0:T(256)} %param.9) | copy-start | bytes 3076
  0.7 22.7 %collective-permute-start.3 = (bf16[1024,256]{1,0:T(8,128)(2,1)}, bf16[1024,256]{1,0:T(8,128)(2,1)S(1)}, u32[]{:S(2)}, u32[]{:S(2)}) collective-permute-start(bf16[1024,256]{1,0:T(8,128)(2,1)} %own.1), channel_id=1, source_target_pairs={{0,1},{1,2},{2,3},{3,0},{4,5},{5,6},{6,7},{7,4},{8,9},{9,10},{10,1... | collective-permute-start | bytes 1572872 | tf_op jit(solution)/shard_map/ppermute | solution.py:337
  2.7 20.7 %collective-permute-start.4 = (bf16[1024,256]{1,0:T(8,128)(2,1)}, bf16[1024,256]{1,0:T(8,128)(2,1)S(1)}, u32[]{:S(2)}, u32[]{:S(2)}) collective-permute-start(bf16[1024,256]{1,0:T(8,128)(2,1)} %own.1), channel_id=1, source_target_pairs={{0,3},{1,0},{2,1},{3,2},{4,7},{5,4},{6,5},{7,6},{8,11},{9,8},{10,9... | collective-permute-start | bytes 1572872 | tf_op jit(solution)/shard_map/ppermute | solution.py:338
  6.1 23.5 %collective-permute-start = (bf16[1024,256]{1,0:T(8,128)(2,1)}, bf16[1024,256]{1,0:T(8,128)(2,1)S(1)}, u32[]{:S(2)}, u32[]{:S(2)}) collective-permute-start(bf16[1024,256]{1,0:T(8,128)(2,1)} %own.1), channel_id=1, source_target_pairs={{0,2},{1,3},{2,0},{3,1},{4,6},{5,7},{6,4},{7,5},{8,10},{9,11},{10,... | collective-permute-start | bytes 1572872 | tf_op jit(solution)/shard_map/ppermute | solution.py:341
  10.3 6.4 %collective-permute-start.2 = (bf16[32,256]{1,0:T(8,128)(2,1)}, bf16[32,256]{1,0:T(8,128)(2,1)S(1)}, u32[]{:S(2)}, u32[]{:S(2)}) collective-permute-start(bf16[32,256]{1,0:T(8,128)(2,1)} %edges.1), channel_id=1, source_target_pairs={{4,8},{12,16},{20,24},{28,32},{36,40},{44,48},{52,56},{60,64},{68,... | collective-permute-start | bytes 49160 | tf_op jit(solution)/shard_map/ppermute | solution.py:340
  14.9 3.3 %collective-permute-start.1 = (bf16[32,256]{1,0:T(8,128)(2,1)}, bf16[32,256]{1,0:T(8,128)(2,1)S(1)}, u32[]{:S(2)}, u32[]{:S(2)}) collective-permute-start(bf16[32,256]{1,0:T(8,128)(2,1)} %edges.1), channel_id=1, source_target_pairs={{0,4},{4,0},{8,12},{12,8},{16,20},{20,16},{24,28},{28,24},{32,36},... | collective-permute-start | bytes 49160 | tf_op jit(solution)/shard_map/ppermute | solution.py:339
  18.2 5.3 %copy-start.2 = (bf16[1024,256]{1,0:T(8,128)(2,1)S(1)}, bf16[1024,256]{1,0:T(8,128)(2,1)}, u32[]{:S(2)}) copy-start(bf16[1024,256]{1,0:T(8,128)(2,1)} %weight.3) | copy-start | bytes 1572868
  18.2 5.3 %copy-start.4 = (bf16[1024,256]{1,0:T(8,128)(2,1)S(1)}, bf16[1024,256]{1,0:T(8,128)(2,1)}, u32[]{:S(2)}) copy-start(bf16[1024,256]{1,0:T(8,128)(2,1)} %own.1) | copy-start | bytes 1572868
  35.8 18.1 %all-to-all-start = ((bf16[8,18,8,256]{3,2,1,0:T(8,128)(2,1)}), bf16[8,18,8,256]{3,2,1,0:T(8,128)(2,1)S(1)}, u32[]{:S(2)}, u32[]{:S(2)}) async-start(bf16[8,18,8,256]{3,2,1,0:T(8,128)(2,1)} %get-tuple-element.34), calls=%async_computation | async-start | bytes 1179648 | tf_op jit(solution)/shard_map/all_to_all | solution.py:325
  43.9 9.8 %collective-permute-start.6 = (f32[32,256]{1,0:T(8,128)S(1)}, f32[32,256]{1,0:T(8,128)S(1)}, u32[]{:S(2)}, u32[]{:S(2)}) collective-permute-start(f32[32,256]{1,0:T(8,128)S(1)} %get-tuple-element.35), channel_id=1, source_target_pairs={{4,8},{12,16},{20,24},{28,32},{36,40},{44,48},{52,56},{60,64},{68,... | collective-permute-start | bytes 98312 | tf_op jit(solution)/shard_map/ppermute | solution.py:375
  47.4 6.2 %collective-permute-start.5 = (f32[32,256]{1,0:T(8,128)S(1)}, f32[32,256]{1,0:T(8,128)S(1)}, u32[]{:S(2)}, u32[]{:S(2)}) collective-permute-start(f32[32,256]{1,0:T(8,128)S(1)} %get-tuple-element.35), channel_id=1, source_target_pairs={{0,4},{4,0},{8,12},{12,8},{16,20},{20,16},{24,28},{28,24},{32,36},... | collective-permute-start | bytes 98312 | tf_op jit(solution)/shard_map/ppermute | solution.py:374
  54.7 29.0 %all-to-all-start.1 = ((bf16[16,3,8,256]{3,2,1,0:T(8,128)(2,1)}), bf16[16,3,8,256]{3,2,1,0:T(8,128)(2,1)S(1)}, u32[]{:S(2)}, u32[]{:S(2)}) async-start(bf16[16,3,8,256]{3,2,1,0:T(8,128)(2,1)} %shard_map.104), calls=%async_computation.1 | async-start | bytes 393216 | tf_op jit(solution)/shard_map/all_to_all | solution.py:325
  84.3 6.4 %collective-permute-start.7 = (f32[16,256]{1,0:T(8,128)S(1)}, f32[16,256]{1,0:T(8,128)S(1)}, u32[]{:S(2)}, u32[]{:S(2)}) collective-permute-start(f32[16,256]{1,0:T(8,128)S(1)} %get-tuple-element.45.mine), channel_id=1, source_target_pairs={{0,4},{4,0},{1,5},{5,1},{2,6},{6,2},{3,7},{7,3},{8,12},{12,8},{9,1... | collective-permute-start | bytes 49160 | tf_op jit(solution)/shard_map/ppermute | solution.py:390

commit v5 on v4

--- a/solution.py
+++ b/solution.py
@@ -126,7 +126,7 @@
     lax.fori_loop(0, ROWS // CHUNK, norm_rows, 0)
 
 
-def early_kernel(own, left, right, weight, normed, partial, wgrad):
+def early_kernel(own, left, right, weight, normed, partial, kept, given):
     y = lax.axis_index("tp")
     blocks = ((own, lax.rem(y, 4)), (left, lax.rem(y + 3, 4)), (right, lax.rem(y + 1, 4)))
     weights = [weight[pl.ds(pl.multiple_of(at * CH, CH), CH), :] for _, at in blocks]
@@ -145,18 +145,14 @@
         grads = lax.dot_general(
             ref[...], normed[...], (((0,), (0,)), ((), ())), preferred_element_type=F32
         )
-        put_weight(wgrad, d, grads)
-
-
-def put_weight(out, d, grads):
-    pieces = grads.reshape(4, 8, 8, CH).astype(BF16)
-    for near in range(4):
-        for peer in range(8):
-            out[peer, d * 4 + near] = pieces[near, peer]
+        pieces = grads.reshape(4, 8, 8, CH).astype(BF16)
+        for m in range(2):
+            even, odd = pieces[2 * m], pieces[2 * m + 1]
+            kept[:, d * 2 + m], given[:, d * 2 + m] = sides(is_second(), odd, even)
 
 
 def late_kernel(
-    far, weight, normed, partial, unit, inv, slope, gain, wide, begun, grad, ends, sums
+    far, weight, normed, partial, unit, inv, slope, gain, wide, kept, taken, grad, ends, sums
 ):
     y = lax.axis_index("tp")
     w = weight[pl.ds(pl.multiple_of(lax.rem(y + 2, 4) * CH, CH), CH), :]
@@ -185,15 +181,12 @@
         ends[0:PAD, cols] = grad[b, 0:PAD, :]
         ends[PAD : 2 * PAD, cols] = grad[b, ROWS - PAD : ROWS, :]
 
-    for peer in range(8):
-        sums[peer, 0:12] = begun[peer]
-    put_weight(
-        sums,
-        3,
-        lax.dot_general(
-            far[...], normed[...], (((0,), (0,)), ((), ())), preferred_element_type=F32
-        ),
-    )
+    sums[:, 0:6] = (kept[...].astype(F32) + taken[...].astype(F32)).astype(BF16)
+    pieces = lax.dot_general(
+        far[...], normed[...], (((0,), (0,)), ((), ())), preferred_element_type=F32
+    ).reshape(4, 8, 8, CH).astype(BF16)
+    for near in range(4):
+        sums[:, 6 + near] = pieces[near]
 
     halves = []
     for b in range(2):
@@ -224,7 +217,7 @@
     for peer in range(8):
         for part in range(2):
             line = (peer % 2) * 16 + part * 8
-            sums[peer, 16 + part] = taps[line : line + 8]
+            sums[peer, 10 + part] = taps[line : line + 8]
 
 
 def backward_kernel(
@@ -260,18 +253,25 @@
 
 def middle_kernel(late, out):
     y = lax.axis_index("tp")
-    taps = late[0, 16:18].astype(F32)
-    for peer in range(1, 8):
-        taps = taps + late[peer, 16:18].astype(F32)
-    taps = taps.astype(BF16)
+
+    def total(tile, peers):
+        sums = None
+        for peer in peers:
+            part = late[peer, tile].astype(F32)
+            sums = part if sums is None else sums + part
+        return sums.astype(BF16)
+
+    taps = [total(10 + part, range(8)) for part in range(2)]
     for d, at in enumerate((y, y + 3, y + 1, y + 2)):
         home = lax.rem(at, 4)
         for near in range(4):
-            total = late[0, d * 4 + near].astype(F32)
-            for peer in range(1, 8):
-                total = total + late[peer, d * 4 + near].astype(F32)
-            out[home * 4 + near, 0] = total.astype(BF16)
-            out[home * 4 + near, 1:3] = taps
+            if d < 3:
+                rows = total(d * 2 + near // 2, range(near % 2, 8, 2))
+            else:
+                rows = total(6 + near, range(8))
+            out[home * 4 + near, 0] = rows
+            for part in range(2):
+                out[home * 4 + near, 1 + part] = taps[part]
 
 
 def whole_kernel(got, weight, mine):
@@ -354,21 +354,24 @@
         cost(7),
     )(value_rows, gate_rows, inner, outer, conv_taps, gain)
 
-    partial, wgrad = call(
-        early_kernel, (shape(ROWS, CH), shape(8, 12, 8, CH, dtype=BF16)), [VMEM] * 5, (), cost(4)
+    half = shape(8, 6, 8, CH, dtype=BF16)
+    partial, kept, given = call(
+        early_kernel, (shape(ROWS, CH), half, half), [VMEM] * 5, (), cost(4)
     )(out_grad, left, right, point_weight, normed)
+
+    taken = lax.ppermute(given, SP, pairs)
 
     grad, ends, sums = call(
         late_kernel,
         (
             shape(2, ROWS, LANES),
             shape(2 * PAD, CH),
-            shape(8, 18, 8, CH, dtype=BF16),
+            shape(8, 12, 8, CH, dtype=BF16),
         ),
-        [VMEM] * 10,
+        [VMEM] * 11,
         (),
         cost(8),
-    )(far, point_weight, normed, partial, unit, inv, slope, gain, wide, wgrad)
+    )(far, point_weight, normed, partial, unit, inv, slope, gain, wide, kept, taken)
     late = exchange(sums, ("x", "c"))
 
     inner = lax.ppermute(ends, SP, pairs)

time: 91.9 us -> 92.9 us (1.011)
  starting transfers between devices: 49.3 us -> 55.7 us
  waiting for transfers between devices: 20.5 us -> 15.2 us
    ppermute x0 -> x1, starting transfers between devices: none -> 10.1 us  [body(): taken = lax.ppermute(given, SP, pairs)]
    ppermute x1, waiting for transfers between devices: 4.37 us -> 0.01 us  [body(): far = lax.ppermute(out_grad, 'tp', ring(4, 2))]
    all_to_all x2, starting transfers between devices: 22.7 us -> 19.6 us  [exchange(): return lax.all_to_all(array, axis, 0, 0, tiled=True)]
    ppermute x1, waiting for transfers between devices: 3.44 us -> 0.74 us  [body(): outer = lax.ppermute(ends, SP, apart)]
    ppermute x0 -> x1, waiting for transfers between devices: none -> 1.04 us  [body(): taken = lax.ppermute(given, SP, pairs)]
  transfers between devices with their start and end apart: 10 -> 11, of which waited for: 6 -> 7; matrix products, arithmetic and copies ran while one was open for 0% -> 0% of each run, Pallas kernels for 14% -> 13%
where the time goes in v5:
time: 92.9 us; the launch traced here: 92.3 us
  starting transfers between devices  55.7 us (60%)
  Pallas kernels  20.5 us (22%)
  waiting for transfers between devices  15.2 us (16%)
    all_to_all x2, starting transfers between devices, exchange(): return lax.all_to_all(array, axis, 0, 0, tiled=True)  19.6 us
    all_to_all x2, waiting for transfers between devices, exchange(): return lax.all_to_all(array, axis, 0, 0, tiled=True)  11.2 us
    ppermute x1, starting transfers between devices, body(): taken = lax.ppermute(given, SP, pairs)  10.1 us
    pallas_call x1, Pallas kernels, body(): call(late_kernel, (shape(2, ROWS, LANES), shape(2 * PAD, CH), shape(8, 12...  6.11 us
    pallas_call x1, Pallas kernels, body(): call(forward_kernel, (shape(2, HALO, LANES), shape(ROWS, CH), shape(ROWS,...  5.23 us
    ppermute x1, starting transfers between devices, body(): other = lax.ppermute(mine, 'c', ring(2, 1))  5.06 us
    ppermute x1, starting transfers between devices, body(): outer = lax.ppermute(edges, SP, apart)  4.51 us
    pallas_call x1, Pallas kernels, body(): call(backward_kernel, (shape(ROWS, CH, dtype=BF16), shape(ROWS, CH, dtype...  4.08 us
  transfers between devices with their start and end apart: 11, of which 7 were waited for; matrix products, arithmetic and copies ran while one was open for 0% of the time, Pallas kernels for 13%

profile of v5, /device:TPU:57, one launch (start us, length us, event | category | flops | bytes accessed | tf_op | source)
XLA Modules:
  0.0 92.3 jit_solution(5826394654414158261)
XLA Ops:
  0.7 2.1 %collective-permute-start.3 = (bf16[1024,256]{1,0:T(8,128)(2,1)}, bf16[1024,256]{1,0:T(8,128)(2,1)S(1)}, u32[]{:S(2)}, u32[]{:S(2)}) collective-permute-start(bf16[1024,256]{1,0:T(8,128)(2,1)} %own.1), channel_id=1, source_target_pairs={{0,1},{1,2},{2,3},{3,0},{4,5},{5,6},{6,7},{7,4},{8,9},{9,10},{10,1... | collective-permute-start | bytes 1572872 | tf_op jit(solution)/shard_map/ppermute | solution.py:337
  2.7 3.4 %collective-permute-start.4 = (bf16[1024,256]{1,0:T(8,128)(2,1)}, bf16[1024,256]{1,0:T(8,128)(2,1)S(1)}, u32[]{:S(2)}, u32[]{:S(2)}) collective-permute-start(bf16[1024,256]{1,0:T(8,128)(2,1)} %own.1), channel_id=1, source_target_pairs={{0,3},{1,0},{2,1},{3,2},{4,7},{5,4},{6,5},{7,6},{8,11},{9,8},{10,9... | collective-permute-start | bytes 1572872 | tf_op jit(solution)/shard_map/ppermute | solution.py:338
  6.1 2.9 %collective-permute-start = (bf16[1024,256]{1,0:T(8,128)(2,1)}, bf16[1024,256]{1,0:T(8,128)(2,1)S(1)}, u32[]{:S(2)}, u32[]{:S(2)}) collective-permute-start(bf16[1024,256]{1,0:T(8,128)(2,1)} %own.1), channel_id=1, source_target_pairs={{0,2},{1,3},{2,0},{3,1},{4,6},{5,7},{6,4},{7,5},{8,10},{9,11},{10,... | collective-permute-start | bytes 1572872 | tf_op jit(solution)/shard_map/ppermute | solution.py:341
  9.0 1.4 %edges.1 = bf16[32,256]{1,0:T(8,128)(2,1)} custom-call(bf16[1024,256]{1,0:T(8,128)(2,1)} %value.3, bf16[1024,256]{1,0:T(8,128)(2,1)} %gate.3, bf16[1024,256]{1,0:T(8,128)(2,1)} %value.3, bf16[1024,256]{1,0:T(8,128)(2,1)} %gate.3), custom_call_target="tpu_custom_call" | custom-call | tf_op jit(solution)/shard_map/edges/pallas_call | solution.py:329
  10.3 4.5 %collective-permute-start.2 = (bf16[32,256]{1,0:T(8,128)(2,1)}, bf16[32,256]{1,0:T(8,128)(2,1)S(1)}, u32[]{:S(2)}, u32[]{:S(2)}) collective-permute-start(bf16[32,256]{1,0:T(8,128)(2,1)} %edges.1), channel_id=1, source_target_pairs={{4,8},{12,16},{20,24},{28,32},{36,40},{44,48},{52,56},{60,64},{68,... | collective-permute-start | bytes 49160 | tf_op jit(solution)/shard_map/ppermute | solution.py:340
  14.9 1.9 %collective-permute-start.1 = (bf16[32,256]{1,0:T(8,128)(2,1)}, bf16[32,256]{1,0:T(8,128)(2,1)S(1)}, u32[]{:S(2)}, u32[]{:S(2)}) collective-permute-start(bf16[32,256]{1,0:T(8,128)(2,1)} %edges.1), channel_id=1, source_target_pairs={{0,4},{4,0},{8,12},{12,8},{16,20},{20,16},{24,28},{28,24},{32,36},... | collective-permute-start | bytes 49160 | tf_op jit(solution)/shard_map/ppermute | solution.py:339
  16.8 1.3 %collective-permute-done.1.inner = bf16[32,256]{1,0:T(8,128)(2,1)S(1)} collective-permute-done((bf16[32,256]{1,0:T(8,128)(2,1)}, bf16[32,256]{1,0:T(8,128)(2,1)S(1)}, u32[]{:S(2)}, u32[]{:S(2)}) %collective-permute-start.1) | collective-permute-done | bytes 16416 | tf_op jit(solution)/shard_map/ppermute | solution.py:339
  18.2 5.2 %shard_map.101 = (f32[2,1056,128]{2,1,0:T(8,128)S(1)}, f32[1024,256]{1,0:T(8,128)S(1)}, f32[1024,256]{1,0:T(8,128)S(1)}, f32[1024,256]{1,0:T(8,128)S(1)}, bf16[1024,256]{1,0:T(8,128)(2,1)S(1)}) custom-call(bf16[1024,256]{1,0:T(8,128)(2,1)S(1)} %copy-done, bf16[1024,256]{1,0:T(8,128)(2,1)S(1)} %copy-done.1, bf16[32,256]{1,0:T(8,128)(2,1)S(1)} %collective-permute-done.1.inner, ...), custom_call_target="tpu_custom_call" | custom-call | flops 1400000000 | bytes 1048576 | tf_op jit(solution)/shard_map/pallas_call | solution.py:343
  23.5 1.8 %shard_map.102 = (f32[1024,256]{1,0:T(8,128)S(1)}, bf16[8,6,8,256]{3,2,1,0:T(8,128)(2,1)S(1)}, bf16[8,6,8,256]{3,2,1,0:T(8,128)(2,1)S(1)}) custom-call(bf16[1024,256]{1,0:T(8,128)(2,1)S(1)} %copy-done.4, bf16[1024,256]{1,0:T(8,128)(2,1)S(1)} %collective-permute-done.3.left, bf16[1024,256]{1,0:T(8,128)(2,1)S(1)} %collective-permute-done.4.right, ...), custom_call_target="tpu_custom_call" | custom-call | flops 800000000 | bytes 1048576 | tf_op jit(solution)/shard_map/pallas_call | solution.py:358
  25.2 10.1 %collective-permute-start.5 = (bf16[8,6,8,256]{3,2,1,0:T(8,128)(2,1)S(1)}, bf16[8,6,8,256]{3,2,1,0:T(8,128)(2,1)S(1)}, u32[]{:S(2)}, u32[]{:S(2)}) collective-permute-start(bf16[8,6,8,256]{3,2,1,0:T(8,128)(2,1)S(1)} %get-tuple-element.35), channel_id=1, source_target_pairs={{0,4},{4,0},{8,12},{12,8},{16,20},{20,16},{24,28},{28,24},{32,36},... | collective-permute-start | bytes 589832 | tf_op jit(solution)/shard_map/ppermute | solution.py:362
  35.3 1.0 %collective-permute-done.5.taken = bf16[8,6,8,256]{3,2,1,0:T(8,128)(2,1)S(1)} collective-permute-done((bf16[8,6,8,256]{3,2,1,0:T(8,128)(2,1)S(1)}, bf16[8,6,8,256]{3,2,1,0:T(8,128)(2,1)S(1)}, u32[]{:S(2)}, u32[]{:S(2)}) %collective-permute-start.5) | collective-permute-done | bytes 196640 | tf_op jit(solution)/shard_map/ppermute | solution.py:362
  36.4 6.1 %shard_map.103 = (f32[2,1024,128]{2,1,0:T(8,128)S(1)}, f32[32,256]{1,0:T(8,128)S(1)}, bf16[8,12,8,256]{3,2,1,0:T(8,128)(2,1)}) custom-call(bf16[1024,256]{1,0:T(8,128)(2,1)S(1)} %collective-permute-done.far, bf16[1024,256]{1,0:T(8,128)(2,1)S(1)} %copy-done.2, bf16[1024,256]{1,0:T(8,128)(2,1)S(1)} %get-tuple-element.28.normed, ...), custom_call_target="tpu_custom_call" | custom-call | flops 1600000000 | bytes 1048576 | tf_op jit(solution)/shard_map/pallas_call | solution.py:364
  42.5 4.7 %all-to-all-start = ((bf16[8,12,8,256]{3,2,1,0:T(8,128)(2,1)}), bf16[8,12,8,256]{3,2,1,0:T(8,128)(2,1)S(1)}, u32[]{:S(2)}, u32[]{:S(2)}) async-start(bf16[8,12,8,256]{3,2,1,0:T(8,128)(2,1)} %get-tuple-element.36), calls=%async_computation | async-start | bytes 786432 | tf_op jit(solution)/shard_map/all_to_all | solution.py:325
  47.1 3.5 %collective-permute-start.7 = (f32[32,256]{1,0:T(8,128)S(1)}, f32[32,256]{1,0:T(8,128)S(1)}, u32[]{:S(2)}, u32[]{:S(2)}) collective-permute-start(f32[32,256]{1,0:T(8,128)S(1)} %get-tuple-element.37), channel_id=1, source_target_pairs={{4,8},{12,16},{20,24},{28,32},{36,40},{44,48},{52,56},{60,64},{68,... | collective-permute-start | bytes 98312 | tf_op jit(solution)/shard_map/ppermute | solution.py:378
  50.7 2.8 %collective-permute-start.6 = (f32[32,256]{1,0:T(8,128)S(1)}, f32[32,256]{1,0:T(8,128)S(1)}, u32[]{:S(2)}, u32[]{:S(2)}) collective-permute-start(f32[32,256]{1,0:T(8,128)S(1)} %get-tuple-element.37), channel_id=1, source_target_pairs={{0,4},{4,0},{8,12},{12,8},{16,20},{20,16},{24,28},{28,24},{32,36},... | collective-permute-start | bytes 98312 | tf_op jit(solution)/shard_map/ppermute | solution.py:377
  53.5 0.7 collective-permute-done.7.outer
  54.9 0.7 shard_map.104
  55.6 14.9 %all-to-all-start.1 = ((bf16[16,3,8,256]{3,2,1,0:T(8,128)(2,1)}), bf16[16,3,8,256]{3,2,1,0:T(8,128)(2,1)S(1)}, u32[]{:S(2)}, u32[]{:S(2)}) async-start(bf16[16,3,8,256]{3,2,1,0:T(8,128)(2,1)} %shard_map.104), calls=%async_computation.1 | async-start | bytes 393216 | tf_op jit(solution)/shard_map/all_to_all | solution.py:325
  70.6 4.1 %shard_map.105 = (bf16[1024,256]{1,0:T(8,128)(2,1)}, bf16[1024,256]{1,0:T(8,128)(2,1)}) custom-call(bf16[1024,256]{1,0:T(8,128)(2,1)S(1)} %copy-done, bf16[1024,256]{1,0:T(8,128)(2,1)S(1)} %copy-done.1, f32[2,1024,128]{2,1,0:T(8,128)S(1)} %get-tuple-element.39.grad, f32[32,256]{1,0:T(8,128)S(1)} %collective-permute-done.6.inner, ...), custom_call_target="tpu_custom_call" | custom-call | flops 1200000000 | bytes 1048576 | tf_op jit(solution)/shard_map/pallas_call | solution.py:383
  74.6 10.6 %all-to-all-done.1.got = bf16[16,3,8,256]{3,2,1,0:T(8,128)(2,1)S(1)} async-done(((bf16[16,3,8,256]{3,2,1,0:T(8,128)(2,1)}), bf16[16,3,8,256]{3,2,1,0:T(8,128)(2,1)S(1)}, u32[]{:S(2)}, u32[]{:S(2)}) %all-to-all-start.1) | async-done | bytes 196640 | tf_op jit(solution)/shard_map/all_to_all | solution.py:325
  85.2 0.6 shard_map.106
  85.8 5.1 %collective-permute-start.8 = (f32[16,256]{1,0:T(8,128)S(1)}, f32[16,256]{1,0:T(8,128)S(1)}, u32[]{:S(2)}, u32[]{:S(2)}) collective-permute-start(f32[16,256]{1,0:T(8,128)S(1)} %get-tuple-element.47.mine), channel_id=1, source_target_pairs={{0,4},{4,0},{1,5},{5,1},{2,6},{6,2},{3,7},{7,3},{8,12},{12,8},{9,1... | collective-permute-start | bytes 49160 | tf_op jit(solution)/shard_map/ppermute | solution.py:393
  90.9 0.8 collective-permute-done.8.other
  91.7 0.6 shard_map.107
  (18 shorter events, 0.7 us)
Async XLA Ops:
  0.6 17.5 %copy-start.1 = (bf16[1024,256]{1,0:T(8,128)(2,1)S(1)}, bf16[1024,256]{1,0:T(8,128)(2,1)}, u32[]{:S(2)}) copy-start(bf16[1024,256]{1,0:T(8,128)(2,1)} %gate.3) | copy-start | bytes 1572868
  0.6 17.5 %copy-start = (bf16[1024,256]{1,0:T(8,128)(2,1)S(1)}, bf16[1024,256]{1,0:T(8,128)(2,1)}, u32[]{:S(2)}) copy-start(bf16[1024,256]{1,0:T(8,128)(2,1)} %value.3) | copy-start | bytes 1572868
  0.7 17.5 %copy-start.5 = (bf16[31,256]{1,0:T(8,128)(2,1)S(1)}, bf16[31,256]{1,0:T(8,128)(2,1)}, u32[]{:S(2)}) copy-start(bf16[31,256]{1,0:T(8,128)(2,1)} %taps.3) | copy-start | bytes 47620
  0.7 17.5 %copy-start.3 = (f32[256]{0:T(256)S(1)}, f32[256]{0:T(256)}, u32[]{:S(2)}) copy-start(f32[256]{0:T(256)} %param.9) | copy-start | bytes 3076
  0.7 22.8 %collective-permute-start.3 = (bf16[1024,256]{1,0:T(8,128)(2,1)}, bf16[1024,256]{1,0:T(8,128)(2,1)S(1)}, u32[]{:S(2)}, u32[]{:S(2)}) collective-permute-start(bf16[1024,256]{1,0:T(8,128)(2,1)} %own.1), channel_id=1, source_target_pairs={{0,1},{1,2},{2,3},{3,0},{4,5},{5,6},{6,7},{7,4},{8,9},{9,10},{10,1... | collective-permute-start | bytes 1572872 | tf_op jit(solution)/shard_map/ppermute | solution.py:337
  2.7 20.7 %collective-permute-start.4 = (bf16[1024,256]{1,0:T(8,128)(2,1)}, bf16[1024,256]{1,0:T(8,128)(2,1)S(1)}, u32[]{:S(2)}, u32[]{:S(2)}) collective-permute-start(bf16[1024,256]{1,0:T(8,128)(2,1)} %own.1), channel_id=1, source_target_pairs={{0,3},{1,0},{2,1},{3,2},{4,7},{5,4},{6,5},{7,6},{8,11},{9,8},{10,9... | collective-permute-start | bytes 1572872 | tf_op jit(solution)/shard_map/ppermute | solution.py:338
  6.1 29.2 %collective-permute-start = (bf16[1024,256]{1,0:T(8,128)(2,1)}, bf16[1024,256]{1,0:T(8,128)(2,1)S(1)}, u32[]{:S(2)}, u32[]{:S(2)}) collective-permute-start(bf16[1024,256]{1,0:T(8,128)(2,1)} %own.1), channel_id=1, source_target_pairs={{0,2},{1,3},{2,0},{3,1},{4,6},{5,7},{6,4},{7,5},{8,10},{9,11},{10,... | collective-permute-start | bytes 1572872 | tf_op jit(solution)/shard_map/ppermute | solution.py:341
  10.3 6.4 %collective-permute-start.2 = (bf16[32,256]{1,0:T(8,128)(2,1)}, bf16[32,256]{1,0:T(8,128)(2,1)S(1)}, u32[]{:S(2)}, u32[]{:S(2)}) collective-permute-start(bf16[32,256]{1,0:T(8,128)(2,1)} %edges.1), channel_id=1, source_target_pairs={{4,8},{12,16},{20,24},{28,32},{36,40},{44,48},{52,56},{60,64},{68,... | collective-permute-start | bytes 49160 | tf_op jit(solution)/shard_map/ppermute | solution.py:340
  14.9 3.3 %collective-permute-start.1 = (bf16[32,256]{1,0:T(8,128)(2,1)}, bf16[32,256]{1,0:T(8,128)(2,1)S(1)}, u32[]{:S(2)}, u32[]{:S(2)}) collective-permute-start(bf16[32,256]{1,0:T(8,128)(2,1)} %edges.1), channel_id=1, source_target_pairs={{0,4},{4,0},{8,12},{12,8},{16,20},{20,16},{24,28},{28,24},{32,36},... | collective-permute-start | bytes 49160 | tf_op jit(solution)/shard_map/ppermute | solution.py:339
  18.2 5.3 %copy-start.2 = (bf16[1024,256]{1,0:T(8,128)(2,1)S(1)}, bf16[1024,256]{1,0:T(8,128)(2,1)}, u32[]{:S(2)}) copy-start(bf16[1024,256]{1,0:T(8,128)(2,1)} %weight.3) | copy-start | bytes 1572868
  18.2 5.3 %copy-start.4 = (bf16[1024,256]{1,0:T(8,128)(2,1)S(1)}, bf16[1024,256]{1,0:T(8,128)(2,1)}, u32[]{:S(2)}) copy-start(bf16[1024,256]{1,0:T(8,128)(2,1)} %own.1) | copy-start | bytes 1572868
  25.2 11.1 %collective-permute-start.5 = (bf16[8,6,8,256]{3,2,1,0:T(8,128)(2,1)S(1)}, bf16[8,6,8,256]{3,2,1,0:T(8,128)(2,1)S(1)}, u32[]{:S(2)}, u32[]{:S(2)}) collective-permute-start(bf16[8,6,8,256]{3,2,1,0:T(8,128)(2,1)S(1)} %get-tuple-element.35), channel_id=1, source_target_pairs={{0,4},{4,0},{8,12},{12,8},{16,20},{20,16},{24,28},{28,24},{32,36},... | collective-permute-start | bytes 589832 | tf_op jit(solution)/shard_map/ppermute | solution.py:362
  42.5 12.4 %all-to-all-start = ((bf16[8,12,8,256]{3,2,1,0:T(8,128)(2,1)}), bf16[8,12,8,256]{3,2,1,0:T(8,128)(2,1)S(1)}, u32[]{:S(2)}, u32[]{:S(2)}) async-start(bf16[8,12,8,256]{3,2,1,0:T(8,128)(2,1)} %get-tuple-element.36), calls=%async_computation | async-start | bytes 786432 | tf_op jit(solution)/shard_map/all_to_all | solution.py:325
  47.1 7.1 %collective-permute-start.7 = (f32[32,256]{1,0:T(8,128)S(1)}, f32[32,256]{1,0:T(8,128)S(1)}, u32[]{:S(2)}, u32[]{:S(2)}) collective-permute-start(f32[32,256]{1,0:T(8,128)S(1)} %get-tuple-element.37), channel_id=1, source_target_pairs={{4,8},{12,16},{20,24},{28,32},{36,40},{44,48},{52,56},{60,64},{68,... | collective-permute-start | bytes 98312 | tf_op jit(solution)/shard_map/ppermute | solution.py:378
  50.7 3.6 %collective-permute-start.6 = (f32[32,256]{1,0:T(8,128)S(1)}, f32[32,256]{1,0:T(8,128)S(1)}, u32[]{:S(2)}, u32[]{:S(2)}) collective-permute-start(f32[32,256]{1,0:T(8,128)S(1)} %get-tuple-element.37), channel_id=1, source_target_pairs={{0,4},{4,0},{8,12},{12,8},{16,20},{20,16},{24,28},{28,24},{32,36},... | collective-permute-start | bytes 98312 | tf_op jit(solution)/shard_map/ppermute | solution.py:377
  55.6 29.6 %all-to-all-start.1 = ((bf16[16,3,8,256]{3,2,1,0:T(8,128)(2,1)}), bf16[16,3,8,256]{3,2,1,0:T(8,128)(2,1)S(1)}, u32[]{:S(2)}, u32[]{:S(2)}) async-start(bf16[16,3,8,256]{3,2,1,0:T(8,128)(2,1)} %shard_map.104), calls=%async_computation.1 | async-start | bytes 393216 | tf_op jit(solution)/shard_map/all_to_all | solution.py:325
  85.8 5.9 %collective-permute-start.8 = (f32[16,256]{1,0:T(8,128)S(1)}, f32[16,256]{1,0:T(8,128)S(1)}, u32[]{:S(2)}, u32[]{:S(2)}) collective-permute-start(f32[16,256]{1,0:T(8,128)S(1)} %get-tuple-element.47.mine), channel_id=1, source_target_pairs={{0,4},{4,0},{1,5},{5,1},{2,6},{6,2},{3,7},{7,3},{8,12},{12,8},{9,1... | collective-permute-start | bytes 49160 | tf_op jit(solution)/shard_map/ppermute | solution.py:393

commit v6 on v5

--- a/solution.py
+++ b/solution.py
@@ -1,3 +1,5 @@
+import functools
+
 import jax
 import jax.numpy as jnp
 from jax import lax
@@ -13,6 +15,7 @@
 ROWS = 1024
 CH = 256
 LANES = 128
+HALF = 512
 PAD = 16
 HALO = ROWS + 2 * PAD
 KW = 31
@@ -126,9 +129,13 @@
     lax.fori_loop(0, ROWS // CHUNK, norm_rows, 0)
 
 
+def homes(y):
+    return y, lax.bitwise_xor(y, 1), 3 - y, lax.bitwise_xor(y, 2)
+
+
 def early_kernel(own, left, right, weight, normed, partial, kept, given):
     y = lax.axis_index("tp")
-    blocks = ((own, lax.rem(y, 4)), (left, lax.rem(y + 3, 4)), (right, lax.rem(y + 1, 4)))
+    blocks = tuple(zip((own, left, right), homes(y)))
     weights = [weight[pl.ds(pl.multiple_of(at * CH, CH), CH), :] for _, at in blocks]
 
     def some_rows(step, _):
@@ -152,17 +159,18 @@
 
 
 def late_kernel(
-    far, weight, normed, partial, unit, inv, slope, gain, wide, kept, taken, grad, ends, sums
+    far_top, far_bottom, weight, normed, partial, unit, inv, slope, gain, wide, kept, taken, grad, ends, sums
 ):
     y = lax.axis_index("tp")
-    w = weight[pl.ds(pl.multiple_of(lax.rem(y + 2, 4) * CH, CH), CH), :]
+    w = weight[pl.ds(pl.multiple_of(homes(y)[3] * CH, CH), CH), :]
     avg = averaging()
     gain_row = gain[...]
 
-    def some_rows(step, gain_sum):
+    def some_rows(step, gain_sum, far, base):
         start = pl.multiple_of(step * CHUNK, CHUNK)
-        rows = pl.ds(start, CHUNK)
-        normed_grad = partial[rows, :] + jnp.dot(far[rows, :], w, preferred_element_type=F32)
+        rows = pl.ds(start + base, CHUNK)
+        normed_grad = partial[rows, :] + jnp.dot(
+            far[pl.ds(start, CHUNK), :], w, preferred_element_type=F32)
         u = unit[rows, :]
         act = normed_grad * slope[rows, :]
         au = act * u
@@ -175,7 +183,11 @@
             grad[b, rows, :] = rows_grad[:, b * LANES : (b + 1) * LANES]
         return gain_sum + jnp.sum(au.reshape(CHUNK // 8, 8, CH), axis=0)
 
-    gain_sum = lax.fori_loop(0, ROWS // CHUNK, some_rows, jnp.zeros((8, CH), F32))
+    gain_sum = jnp.zeros((8, CH), F32)
+    for far, base in ((far_top, 0), (far_bottom, HALF)):
+        gain_sum = lax.fori_loop(
+            0, HALF // CHUNK, functools.partial(some_rows, far=far, base=base), gain_sum
+        )
     for b in range(2):
         cols = slice(b * LANES, (b + 1) * LANES)
         ends[0:PAD, cols] = grad[b, 0:PAD, :]
@@ -183,8 +195,11 @@
 
     sums[:, 0:6] = (kept[...].astype(F32) + taken[...].astype(F32)).astype(BF16)
     pieces = lax.dot_general(
-        far[...], normed[...], (((0,), (0,)), ((), ())), preferred_element_type=F32
-    ).reshape(4, 8, 8, CH).astype(BF16)
+        far_top[...], normed[0:HALF, :], (((0,), (0,)), ((), ())), preferred_element_type=F32
+    ) + lax.dot_general(
+        far_bottom[...], normed[HALF:ROWS, :], (((0,), (0,)), ((), ())), preferred_element_type=F32
+    )
+    pieces = pieces.reshape(4, 8, 8, CH).astype(BF16)
     for near in range(4):
         sums[:, 6 + near] = pieces[near]
 
@@ -262,8 +277,7 @@
         return sums.astype(BF16)
 
     taps = [total(10 + part, range(8)) for part in range(2)]
-    for d, at in enumerate((y, y + 3, y + 1, y + 2)):
-        home = lax.rem(at, 4)
+    for d, home in enumerate(homes(y)):
         for near in range(4):
             if d < 3:
                 rows = total(d * 2 + near // 2, range(near % 2, 8, 2))
@@ -334,11 +348,14 @@
         out_specs=pl.BlockSpec((2 * PAD, CH), lambda i: (0, 0)),
         name="edges",
     )(value_rows, gate_rows, value_rows, gate_rows)
-    left = lax.ppermute(out_grad, "tp", ring(4, 1))
-    right = lax.ppermute(out_grad, "tp", ring(4, 3))
+    beside = [(i, i ^ 1) for i in range(4)]
+    around = [(i, 3 - i) for i in range(4)]
+    left = lax.ppermute(out_grad, "tp", beside)
+    right = lax.ppermute(out_grad, "tp", around)
     inner = lax.ppermute(edges, SP, pairs)
     outer = lax.ppermute(edges, SP, apart)
-    far = lax.ppermute(out_grad, "tp", ring(4, 2))
+    far_top = lax.ppermute(left[:HALF], "tp", around)
+    far_bottom = lax.ppermute(right[HALF:], "tp", beside)
 
     wide, unit, inv, slope, normed = call(
         forward_kernel,
@@ -368,10 +385,10 @@
             shape(2 * PAD, CH),
             shape(8, 12, 8, CH, dtype=BF16),
         ),
-        [VMEM] * 11,
+        [VMEM] * 12,
         (),
         cost(8),
-    )(far, point_weight, normed, partial, unit, inv, slope, gain, wide, kept, taken)
+    )(far_top, far_bottom, point_weight, normed, partial, unit, inv, slope, gain, wide, kept, taken)
     late = exchange(sums, ("x", "c"))
 
     inner = lax.ppermute(ends, SP, pairs)

time: 92.9 us -> 92.5 us (level)
  the two profiles are of different devices: /device:TPU:57 before, /device:TPU:1 now
where the time goes in v6:
time: 92.5 us; the launch traced here: 91.9 us
  starting transfers between devices  55.5 us (60%)
  Pallas kernels  20.5 us (22%)
  waiting for transfers between devices  15 us (16%)
    all_to_all x2, starting transfers between devices, exchange(): return lax.all_to_all(array, axis, 0, 0, tiled=True)  20.3 us
    all_to_all x2, waiting for transfers between devices, exchange(): return lax.all_to_all(array, axis, 0, 0, tiled=True)  9.09 us
    ppermute x1, starting transfers between devices, body(): other = lax.ppermute(mine, 'c', ring(2, 1))  6.61 us
    pallas_call x1, Pallas kernels, body(): call(late_kernel, (shape(2, ROWS, LANES), shape(2 * PAD, CH), shape(8, 12...  6.1 us
    pallas_call x1, Pallas kernels, body(): call(forward_kernel, (shape(2, HALO, LANES), shape(ROWS, CH), shape(ROWS,...  5.21 us
    ppermute x1, starting transfers between devices, body(): outer = lax.ppermute(edges, SP, apart)  4.23 us
    ppermute x1, starting transfers between devices, body(): left = lax.ppermute(out_grad, 'tp', beside)  4.16 us
    pallas_call x1, Pallas kernels, body(): call(backward_kernel, (shape(ROWS, CH, dtype=BF16), shape(ROWS, CH, dtype...  4.08 us
  transfers between devices with their start and end apart: 12, of which 7 were waited for; matrix products, arithmetic and copies ran while one was open for 0% of the time, Pallas kernels for 14%

profile of v6, /device:TPU:1, one launch (start us, length us, event | category | flops | bytes accessed | tf_op | source)
XLA Modules:
  0.0 91.9 jit_solution(8645100213243456041)
XLA Ops:
  0.7 4.2 %collective-permute-start = (bf16[1024,256]{1,0:T(8,128)(2,1)}, bf16[1024,256]{1,0:T(8,128)(2,1)S(1)}, u32[]{:S(2)}, u32[]{:S(2)}) collective-permute-start(bf16[1024,256]{1,0:T(8,128)(2,1)} %own.1), channel_id=1, source_target_pairs={{0,1},{1,0},{2,3},{3,2},{4,5},{5,4},{6,7},{7,6},{8,9},{9,8},{10,11... | collective-permute-start | bytes 1572872 | tf_op jit(solution)/shard_map/ppermute | solution.py:353
  4.8 3.8 %collective-permute-start.2 = (bf16[1024,256]{1,0:T(8,128)(2,1)}, bf16[1024,256]{1,0:T(8,128)(2,1)S(1)}, u32[]{:S(2)}, u32[]{:S(2)}) collective-permute-start(bf16[1024,256]{1,0:T(8,128)(2,1)} %own.1), channel_id=1, source_target_pairs={{0,3},{1,2},{2,1},{3,0},{4,7},{5,6},{6,5},{7,4},{8,11},{9,10},{10,... | collective-permute-start | bytes 1572872 | tf_op jit(solution)/shard_map/ppermute | solution.py:354
  8.7 1.4 %edges.1 = bf16[32,256]{1,0:T(8,128)(2,1)} custom-call(bf16[1024,256]{1,0:T(8,128)(2,1)} %value.3, bf16[1024,256]{1,0:T(8,128)(2,1)} %gate.3, bf16[1024,256]{1,0:T(8,128)(2,1)} %value.3, bf16[1024,256]{1,0:T(8,128)(2,1)} %gate.3), custom_call_target="tpu_custom_call" | custom-call | tf_op jit(solution)/shard_map/edges/pallas_call | solution.py:343
  10.0 4.2 %collective-permute-start.5 = (bf16[32,256]{1,0:T(8,128)(2,1)}, bf16[32,256]{1,0:T(8,128)(2,1)S(1)}, u32[]{:S(2)}, u32[]{:S(2)}) collective-permute-start(bf16[32,256]{1,0:T(8,128)(2,1)} %edges.1), channel_id=1, source_target_pairs={{4,8},{12,16},{20,24},{28,32},{36,40},{44,48},{52,56},{60,64},{68,... | collective-permute-start | bytes 49160 | tf_op jit(solution)/shard_map/ppermute | solution.py:356
  14.3 1.9 %collective-permute-start.4 = (bf16[32,256]{1,0:T(8,128)(2,1)}, bf16[32,256]{1,0:T(8,128)(2,1)S(1)}, u32[]{:S(2)}, u32[]{:S(2)}) collective-permute-start(bf16[32,256]{1,0:T(8,128)(2,1)} %edges.1), channel_id=1, source_target_pairs={{0,4},{4,0},{8,12},{12,8},{16,20},{20,16},{24,28},{28,24},{32,36},... | collective-permute-start | bytes 49160 | tf_op jit(solution)/shard_map/ppermute | solution.py:355
  16.2 1.3 %collective-permute-done.4.inner = bf16[32,256]{1,0:T(8,128)(2,1)S(1)} collective-permute-done((bf16[32,256]{1,0:T(8,128)(2,1)}, bf16[32,256]{1,0:T(8,128)(2,1)S(1)}, u32[]{:S(2)}, u32[]{:S(2)}) %collective-permute-start.4) | collective-permute-done | bytes 16416 | tf_op jit(solution)/shard_map/ppermute | solution.py:355
  17.6 5.2 %shard_map.101 = (f32[2,1056,128]{2,1,0:T(8,128)S(1)}, f32[1024,256]{1,0:T(8,128)S(1)}, f32[1024,256]{1,0:T(8,128)S(1)}, f32[1024,256]{1,0:T(8,128)S(1)}, bf16[1024,256]{1,0:T(8,128)(2,1)S(1)}) custom-call(bf16[1024,256]{1,0:T(8,128)(2,1)S(1)} %copy-done, bf16[1024,256]{1,0:T(8,128)(2,1)S(1)} %copy-done.1, bf16[32,256]{1,0:T(8,128)(2,1)S(1)} %collective-permute-done.4.inner, ...), custom_call_target="tpu_custom_call" | custom-call | flops 1400000000 | bytes 1048576 | tf_op jit(solution)/shard_map/pallas_call | solution.py:360
  22.8 3.8 %collective-permute-start.1 = (bf16[512,256]{1,0:T(8,128)(2,1)S(1)}, bf16[512,256]{1,0:T(8,128)(2,1)S(1)}, u32[]{:S(2)}, u32[]{:S(2)}) collective-permute-start(bf16[512,256]{1,0:T(8,128)(2,1)S(1)} %slice.8), channel_id=1, source_target_pairs={{0,3},{1,2},{2,1},{3,0},{4,7},{5,6},{6,5},{7,4},{8,11},{9,10},{10,... | collective-permute-start | bytes 786440 | tf_op jit(solution)/shard_map/ppermute | solution.py:357
  26.7 2.4 %collective-permute-start.3 = (bf16[512,256]{1,0:T(8,128)(2,1)S(1)}, bf16[512,256]{1,0:T(8,128)(2,1)S(1)}, u32[]{:S(2)}, u32[]{:S(2)}) collective-permute-start(bf16[512,256]{1,0:T(8,128)(2,1)S(1)} %slice.9), channel_id=1, source_target_pairs={{0,1},{1,0},{2,3},{3,2},{4,5},{5,4},{6,7},{7,6},{8,9},{9,8},{10,11... | collective-permute-start | bytes 786440 | tf_op jit(solution)/shard_map/ppermute | solution.py:358
  29.1 1.8 %shard_map.102 = (f32[1024,256]{1,0:T(8,128)S(1)}, bf16[8,6,8,256]{3,2,1,0:T(8,128)(2,1)S(1)}, bf16[8,6,8,256]{3,2,1,0:T(8,128)(2,1)S(1)}) custom-call(bf16[1024,256]{1,0:T(8,128)(2,1)S(1)} %copy-done.4, bf16[1024,256]{1,0:T(8,128)(2,1)S(1)} %collective-permute-done.left, bf16[1024,256]{1,0:T(8,128)(2,1)S(1)} %collective-permute-done.2.right, ...), custom_call_target="tpu_custom_call" | custom-call | flops 800000000 | bytes 1048576 | tf_op jit(solution)/shard_map/pallas_call | solution.py:375
  30.9 2.8 %collective-permute-start.6 = (bf16[8,6,8,256]{3,2,1,0:T(8,128)(2,1)S(1)}, bf16[8,6,8,256]{3,2,1,0:T(8,128)(2,1)S(1)}, u32[]{:S(2)}, u32[]{:S(2)}) collective-permute-start(bf16[8,6,8,256]{3,2,1,0:T(8,128)(2,1)S(1)} %get-tuple-element.35), channel_id=1, source_target_pairs={{0,4},{4,0},{8,12},{12,8},{16,20},{20,16},{24,28},{28,24},{32,36},... | collective-permute-start | bytes 589832 | tf_op jit(solution)/shard_map/ppermute | solution.py:379
  33.7 1.0 %collective-permute-done.6.taken = bf16[8,6,8,256]{3,2,1,0:T(8,128)(2,1)S(1)} collective-permute-done((bf16[8,6,8,256]{3,2,1,0:T(8,128)(2,1)S(1)}, bf16[8,6,8,256]{3,2,1,0:T(8,128)(2,1)S(1)}, u32[]{:S(2)}, u32[]{:S(2)}) %collective-permute-start.6) | collective-permute-done | bytes 196640 | tf_op jit(solution)/shard_map/ppermute | solution.py:379
  34.8 1.0 %collective-permute-done.3.far_bottom = bf16[512,256]{1,0:T(8,128)(2,1)S(1)} collective-permute-done((bf16[512,256]{1,0:T(8,128)(2,1)S(1)}, bf16[512,256]{1,0:T(8,128)(2,1)S(1)}, u32[]{:S(2)}, u32[]{:S(2)}) %collective-permute-start.3) | collective-permute-done | bytes 262176 | tf_op jit(solution)/shard_map/ppermute | solution.py:358
  35.8 6.1 %shard_map.103 = (f32[2,1024,128]{2,1,0:T(8,128)S(1)}, f32[32,256]{1,0:T(8,128)S(1)}, bf16[8,12,8,256]{3,2,1,0:T(8,128)(2,1)}) custom-call(bf16[512,256]{1,0:T(8,128)(2,1)S(1)} %collective-permute-done.1.far_top, bf16[512,256]{1,0:T(8,128)(2,1)S(1)} %collective-permute-done.3.far_bottom, bf16[1024,256]{1,0:T(8,128)(2,1)S(1)} %copy-done.2, ...), custom_call_target="tpu_custom_call" | custom-call | flops 1600000000 | bytes 1048576 | tf_op jit(solution)/shard_map/pallas_call | solution.py:381
  41.9 4.8 %all-to-all-start = ((bf16[8,12,8,256]{3,2,1,0:T(8,128)(2,1)}), bf16[8,12,8,256]{3,2,1,0:T(8,128)(2,1)S(1)}, u32[]{:S(2)}, u32[]{:S(2)}) async-start(bf16[8,12,8,256]{3,2,1,0:T(8,128)(2,1)} %get-tuple-element.36), calls=%async_computation | async-start | bytes 786432 | tf_op jit(solution)/shard_map/all_to_all | solution.py:339
  46.7 3.5 %collective-permute-start.8 = (f32[32,256]{1,0:T(8,128)S(1)}, f32[32,256]{1,0:T(8,128)S(1)}, u32[]{:S(2)}, u32[]{:S(2)}) collective-permute-start(f32[32,256]{1,0:T(8,128)S(1)} %get-tuple-element.37), channel_id=1, source_target_pairs={{4,8},{12,16},{20,24},{28,32},{36,40},{44,48},{52,56},{60,64},{68,... | collective-permute-start | bytes 98312 | tf_op jit(solution)/shard_map/ppermute | solution.py:395
  50.3 1.9 %collective-permute-start.7 = (f32[32,256]{1,0:T(8,128)S(1)}, f32[32,256]{1,0:T(8,128)S(1)}, u32[]{:S(2)}, u32[]{:S(2)}) collective-permute-start(f32[32,256]{1,0:T(8,128)S(1)} %get-tuple-element.37), channel_id=1, source_target_pairs={{0,4},{4,0},{8,12},{12,8},{16,20},{20,16},{24,28},{28,24},{32,36},... | collective-permute-start | bytes 98312 | tf_op jit(solution)/shard_map/ppermute | solution.py:394
  52.2 1.6 %collective-permute-done.8.outer = f32[32,256]{1,0:T(8,128)S(1)} collective-permute-done((f32[32,256]{1,0:T(8,128)S(1)}, f32[32,256]{1,0:T(8,128)S(1)}, u32[]{:S(2)}, u32[]{:S(2)}) %collective-permute-start.8) | collective-permute-done | bytes 32800 | tf_op jit(solution)/shard_map/ppermute | solution.py:395
  54.5 0.7 shard_map.104
  55.2 15.5 %all-to-all-start.1 = ((bf16[16,3,8,256]{3,2,1,0:T(8,128)(2,1)}), bf16[16,3,8,256]{3,2,1,0:T(8,128)(2,1)S(1)}, u32[]{:S(2)}, u32[]{:S(2)}) async-start(bf16[16,3,8,256]{3,2,1,0:T(8,128)(2,1)} %shard_map.104), calls=%async_computation.1 | async-start | bytes 393216 | tf_op jit(solution)/shard_map/all_to_all | solution.py:339
  70.7 4.1 %shard_map.105 = (bf16[1024,256]{1,0:T(8,128)(2,1)}, bf16[1024,256]{1,0:T(8,128)(2,1)}) custom-call(bf16[1024,256]{1,0:T(8,128)(2,1)S(1)} %copy-done, bf16[1024,256]{1,0:T(8,128)(2,1)S(1)} %copy-done.1, f32[2,1024,128]{2,1,0:T(8,128)S(1)} %get-tuple-element.39.grad, f32[32,256]{1,0:T(8,128)S(1)} %collective-permute-done.7.inner, ...), custom_call_target="tpu_custom_call" | custom-call | flops 1200000000 | bytes 1048576 | tf_op jit(solution)/shard_map/pallas_call | solution.py:400
  74.8 8.4 %all-to-all-done.1.got = bf16[16,3,8,256]{3,2,1,0:T(8,128)(2,1)S(1)} async-done(((bf16[16,3,8,256]{3,2,1,0:T(8,128)(2,1)}), bf16[16,3,8,256]{3,2,1,0:T(8,128)(2,1)S(1)}, u32[]{:S(2)}, u32[]{:S(2)}) %all-to-all-start.1) | async-done | bytes 196640 | tf_op jit(solution)/shard_map/all_to_all | solution.py:339
  83.8 6.6 %collective-permute-start.9 = (f32[16,256]{1,0:T(8,128)S(1)}, f32[16,256]{1,0:T(8,128)S(1)}, u32[]{:S(2)}, u32[]{:S(2)}) collective-permute-start(f32[16,256]{1,0:T(8,128)S(1)} %get-tuple-element.47.mine), channel_id=1, source_target_pairs={{0,4},{4,0},{1,5},{5,1},{2,6},{6,2},{3,7},{7,3},{8,12},{12,8},{9,1... | collective-permute-start | bytes 49160 | tf_op jit(solution)/shard_map/ppermute | solution.py:410
  90.4 0.8 collective-permute-done.9.other
  (22 shorter events, 2.0 us)
Async XLA Ops:
  0.6 16.9 %copy-start.1 = (bf16[1024,256]{1,0:T(8,128)(2,1)S(1)}, bf16[1024,256]{1,0:T(8,128)(2,1)}, u32[]{:S(2)}) copy-start(bf16[1024,256]{1,0:T(8,128)(2,1)} %gate.3) | copy-start | bytes 1572868
  0.6 16.9 %copy-start = (bf16[1024,256]{1,0:T(8,128)(2,1)S(1)}, bf16[1024,256]{1,0:T(8,128)(2,1)}, u32[]{:S(2)}) copy-start(bf16[1024,256]{1,0:T(8,128)(2,1)} %value.3) | copy-start | bytes 1572868
  0.7 16.9 %copy-start.5 = (bf16[31,256]{1,0:T(8,128)(2,1)S(1)}, bf16[31,256]{1,0:T(8,128)(2,1)}, u32[]{:S(2)}) copy-start(bf16[31,256]{1,0:T(8,128)(2,1)} %taps.3) | copy-start | bytes 47620
  0.7 16.9 %copy-start.3 = (f32[256]{0:T(256)S(1)}, f32[256]{0:T(256)}, u32[]{:S(2)}) copy-start(f32[256]{0:T(256)} %param.9) | copy-start | bytes 3076
  0.7 22.1 %collective-permute-start = (bf16[1024,256]{1,0:T(8,128)(2,1)}, bf16[1024,256]{1,0:T(8,128)(2,1)S(1)}, u32[]{:S(2)}, u32[]{:S(2)}) collective-permute-start(bf16[1024,256]{1,0:T(8,128)(2,1)} %own.1), channel_id=1, source_target_pairs={{0,1},{1,0},{2,3},{3,2},{4,5},{5,4},{6,7},{7,6},{8,9},{9,8},{10,11... | collective-permute-start | bytes 1572872 | tf_op jit(solution)/shard_map/ppermute | solution.py:353
  4.8 21.8 %collective-permute-start.2 = (bf16[1024,256]{1,0:T(8,128)(2,1)}, bf16[1024,256]{1,0:T(8,128)(2,1)S(1)}, u32[]{:S(2)}, u32[]{:S(2)}) collective-permute-start(bf16[1024,256]{1,0:T(8,128)(2,1)} %own.1), channel_id=1, source_target_pairs={{0,3},{1,2},{2,1},{3,0},{4,7},{5,6},{6,5},{7,4},{8,11},{9,10},{10,... | collective-permute-start | bytes 1572872 | tf_op jit(solution)/shard_map/ppermute | solution.py:354
  10.0 6.2 %collective-permute-start.5 = (bf16[32,256]{1,0:T(8,128)(2,1)}, bf16[32,256]{1,0:T(8,128)(2,1)S(1)}, u32[]{:S(2)}, u32[]{:S(2)}) collective-permute-start(bf16[32,256]{1,0:T(8,128)(2,1)} %edges.1), channel_id=1, source_target_pairs={{4,8},{12,16},{20,24},{28,32},{36,40},{44,48},{52,56},{60,64},{68,... | collective-permute-start | bytes 49160 | tf_op jit(solution)/shard_map/ppermute | solution.py:356
  14.3 3.3 %collective-permute-start.4 = (bf16[32,256]{1,0:T(8,128)(2,1)}, bf16[32,256]{1,0:T(8,128)(2,1)S(1)}, u32[]{:S(2)}, u32[]{:S(2)}) collective-permute-start(bf16[32,256]{1,0:T(8,128)(2,1)} %edges.1), channel_id=1, source_target_pairs={{0,4},{4,0},{8,12},{12,8},{16,20},{20,16},{24,28},{28,24},{32,36},... | collective-permute-start | bytes 49160 | tf_op jit(solution)/shard_map/ppermute | solution.py:355
  17.6 11.5 %copy-start.2 = (bf16[1024,256]{1,0:T(8,128)(2,1)S(1)}, bf16[1024,256]{1,0:T(8,128)(2,1)}, u32[]{:S(2)}) copy-start(bf16[1024,256]{1,0:T(8,128)(2,1)} %weight.3) | copy-start | bytes 1572868
  17.6 11.5 %copy-start.4 = (bf16[1024,256]{1,0:T(8,128)(2,1)S(1)}, bf16[1024,256]{1,0:T(8,128)(2,1)}, u32[]{:S(2)}) copy-start(bf16[1024,256]{1,0:T(8,128)(2,1)} %own.1) | copy-start | bytes 1572868
  22.8 11.9 %collective-permute-start.1 = (bf16[512,256]{1,0:T(8,128)(2,1)S(1)}, bf16[512,256]{1,0:T(8,128)(2,1)S(1)}, u32[]{:S(2)}, u32[]{:S(2)}) collective-permute-start(bf16[512,256]{1,0:T(8,128)(2,1)S(1)} %slice.8), channel_id=1, source_target_pairs={{0,3},{1,2},{2,1},{3,0},{4,7},{5,6},{6,5},{7,4},{8,11},{9,10},{10,... | collective-permute-start | bytes 786440 | tf_op jit(solution)/shard_map/ppermute | solution.py:357
  26.7 9.1 %collective-permute-start.3 = (bf16[512,256]{1,0:T(8,128)(2,1)S(1)}, bf16[512,256]{1,0:T(8,128)(2,1)S(1)}, u32[]{:S(2)}, u32[]{:S(2)}) collective-permute-start(bf16[512,256]{1,0:T(8,128)(2,1)S(1)} %slice.9), channel_id=1, source_target_pairs={{0,1},{1,0},{2,3},{3,2},{4,5},{5,4},{6,7},{7,6},{8,9},{9,8},{10,11... | collective-permute-start | bytes 786440 | tf_op jit(solution)/shard_map/ppermute | solution.py:358
  30.9 3.9 %collective-permute-start.6 = (bf16[8,6,8,256]{3,2,1,0:T(8,128)(2,1)S(1)}, bf16[8,6,8,256]{3,2,1,0:T(8,128)(2,1)S(1)}, u32[]{:S(2)}, u32[]{:S(2)}) collective-permute-start(bf16[8,6,8,256]{3,2,1,0:T(8,128)(2,1)S(1)} %get-tuple-element.35), channel_id=1, source_target_pairs={{0,4},{4,0},{8,12},{12,8},{16,20},{20,16},{24,28},{28,24},{32,36},... | collective-permute-start | bytes 589832 | tf_op jit(solution)/shard_map/ppermute | solution.py:379
  41.9 12.6 %all-to-all-start = ((bf16[8,12,8,256]{3,2,1,0:T(8,128)(2,1)}), bf16[8,12,8,256]{3,2,1,0:T(8,128)(2,1)S(1)}, u32[]{:S(2)}, u32[]{:S(2)}) async-start(bf16[8,12,8,256]{3,2,1,0:T(8,128)(2,1)} %get-tuple-element.36), calls=%async_computation | async-start | bytes 786432 | tf_op jit(solution)/shard_map/all_to_all | solution.py:339
  46.7 7.1 %collective-permute-start.8 = (f32[32,256]{1,0:T(8,128)S(1)}, f32[32,256]{1,0:T(8,128)S(1)}, u32[]{:S(2)}, u32[]{:S(2)}) collective-permute-start(f32[32,256]{1,0:T(8,128)S(1)} %get-tuple-element.37), channel_id=1, source_target_pairs={{4,8},{12,16},{20,24},{28,32},{36,40},{44,48},{52,56},{60,64},{68,... | collective-permute-start | bytes 98312 | tf_op jit(solution)/shard_map/ppermute | solution.py:395
  50.3 3.5 %collective-permute-start.7 = (f32[32,256]{1,0:T(8,128)S(1)}, f32[32,256]{1,0:T(8,128)S(1)}, u32[]{:S(2)}, u32[]{:S(2)}) collective-permute-start(f32[32,256]{1,0:T(8,128)S(1)} %get-tuple-element.37), channel_id=1, source_target_pairs={{0,4},{4,0},{8,12},{12,8},{16,20},{20,16},{24,28},{28,24},{32,36},... | collective-permute-start | bytes 98312 | tf_op jit(solution)/shard_map/ppermute | solution.py:394
  55.2 28.0 %all-to-all-start.1 = ((bf16[16,3,8,256]{3,2,1,0:T(8,128)(2,1)}), bf16[16,3,8,256]{3,2,1,0:T(8,128)(2,1)S(1)}, u32[]{:S(2)}, u32[]{:S(2)}) async-start(bf16[16,3,8,256]{3,2,1,0:T(8,128)(2,1)} %shard_map.104), calls=%async_computation.1 | async-start | bytes 393216 | tf_op jit(solution)/shard_map/all_to_all | solution.py:339
  83.8 7.4 %collective-permute-start.9 = (f32[16,256]{1,0:T(8,128)S(1)}, f32[16,256]{1,0:T(8,128)S(1)}, u32[]{:S(2)}, u32[]{:S(2)}) collective-permute-start(f32[16,256]{1,0:T(8,128)S(1)} %get-tuple-element.47.mine), channel_id=1, source_target_pairs={{0,4},{4,0},{1,5},{5,1},{2,6},{6,2},{3,7},{7,3},{8,12},{12,8},{9,1... | collective-permute-start | bytes 49160 | tf_op jit(solution)/shard_map/ppermute | solution.py:410

commit v7 on v5

--- a/solution.py
+++ b/solution.py
@@ -126,9 +126,13 @@
     lax.fori_loop(0, ROWS // CHUNK, norm_rows, 0)
 
 
+def homes(y):
+    return y, lax.bitwise_xor(y, 1), 3 - y, lax.bitwise_xor(y, 2)
+
+
 def early_kernel(own, left, right, weight, normed, partial, kept, given):
     y = lax.axis_index("tp")
-    blocks = ((own, lax.rem(y, 4)), (left, lax.rem(y + 3, 4)), (right, lax.rem(y + 1, 4)))
+    blocks = tuple(zip((own, left, right), homes(y)))
     weights = [weight[pl.ds(pl.multiple_of(at * CH, CH), CH), :] for _, at in blocks]
 
     def some_rows(step, _):
@@ -155,7 +159,7 @@
     far, weight, normed, partial, unit, inv, slope, gain, wide, kept, taken, grad, ends, sums
 ):
     y = lax.axis_index("tp")
-    w = weight[pl.ds(pl.multiple_of(lax.rem(y + 2, 4) * CH, CH), CH), :]
+    w = weight[pl.ds(pl.multiple_of(homes(y)[3] * CH, CH), CH), :]
     avg = averaging()
     gain_row = gain[...]
 
@@ -262,8 +266,7 @@
         return sums.astype(BF16)
 
     taps = [total(10 + part, range(8)) for part in range(2)]
-    for d, at in enumerate((y, y + 3, y + 1, y + 2)):
-        home = lax.rem(at, 4)
+    for d, home in enumerate(homes(y)):
         for near in range(4):
             if d < 3:
                 rows = total(d * 2 + near // 2, range(near % 2, 8, 2))
@@ -334,11 +337,11 @@
         out_specs=pl.BlockSpec((2 * PAD, CH), lambda i: (0, 0)),
         name="edges",
     )(value_rows, gate_rows, value_rows, gate_rows)
-    left = lax.ppermute(out_grad, "tp", ring(4, 1))
-    right = lax.ppermute(out_grad, "tp", ring(4, 3))
+    left = lax.ppermute(out_grad, "tp", [(i, i ^ 1) for i in range(4)])
+    right = lax.ppermute(out_grad, "tp", [(i, 3 - i) for i in range(4)])
     inner = lax.ppermute(edges, SP, pairs)
     outer = lax.ppermute(edges, SP, apart)
-    far = lax.ppermute(out_grad, "tp", ring(4, 2))
+    far = lax.ppermute(out_grad, "tp", [(i, i ^ 2) for i in range(4)])
 
     wide, unit, inv, slope, normed = call(
         forward_kernel,

time: 92.9 us -> 94.9 us (1.022)
  the two profiles are of different devices: /device:TPU:57 before, /device:TPU:1 now
where the time goes in v7:
time: 94.9 us; the launch traced here: 94.3 us
  starting transfers between devices  59.5 us (63%)
  Pallas kernels  20.5 us (22%)
  waiting for transfers between devices  13.4 us (14%)
    all_to_all x2, starting transfers between devices, exchange(): return lax.all_to_all(array, axis, 0, 0, tiled=True)  19.9 us
    all_to_all x2, waiting for transfers between devices, exchange(): return lax.all_to_all(array, axis, 0, 0, tiled=True)  8.88 us
    ppermute x1, starting transfers between devices, body(): taken = lax.ppermute(given, SP, pairs)  7.85 us
    ppermute x1, starting transfers between devices, body(): other = lax.ppermute(mine, 'c', ring(2, 1))  6.99 us
    pallas_call x1, Pallas kernels, body(): call(late_kernel, (shape(2, ROWS, LANES), shape(2 * PAD, CH), shape(8, 12...  6.11 us
    pallas_call x1, Pallas kernels, body(): call(forward_kernel, (shape(2, HALO, LANES), shape(ROWS, CH), shape(ROWS,...  5.23 us
    ppermute x1, starting transfers between devices, body(): inner = lax.ppermute(edges, SP, pairs)  4.52 us
    ppermute x1, starting transfers between devices, body(): outer = lax.ppermute(edges, SP, apart)  4.23 us
  transfers between devices with their start and end apart: 11, of which 6 were waited for; matrix products, arithmetic and copies ran while one was open for 0% of the time, Pallas kernels for 13%

profile of v7, /device:TPU:1, one launch (start us, length us, event | category | flops | bytes accessed | tf_op | source)
XLA Modules:
  0.0 94.3 jit_solution(12016874469248327373)
XLA Ops:
  0.7 4.2 %collective-permute-start.3 = (bf16[1024,256]{1,0:T(8,128)(2,1)}, bf16[1024,256]{1,0:T(8,128)(2,1)S(1)}, u32[]{:S(2)}, u32[]{:S(2)}) collective-permute-start(bf16[1024,256]{1,0:T(8,128)(2,1)} %own.1), channel_id=1, source_target_pairs={{0,1},{1,0},{2,3},{3,2},{4,5},{5,4},{6,7},{7,6},{8,9},{9,8},{10,11... | collective-permute-start | bytes 1572872 | tf_op jit(solution)/shard_map/ppermute | solution.py:340
  4.8 3.8 %collective-permute-start.4 = (bf16[1024,256]{1,0:T(8,128)(2,1)}, bf16[1024,256]{1,0:T(8,128)(2,1)S(1)}, u32[]{:S(2)}, u32[]{:S(2)}) collective-permute-start(bf16[1024,256]{1,0:T(8,128)(2,1)} %own.1), channel_id=1, source_target_pairs={{0,3},{1,2},{2,1},{3,0},{4,7},{5,6},{6,5},{7,4},{8,11},{9,10},{10,... | collective-permute-start | bytes 1572872 | tf_op jit(solution)/shard_map/ppermute | solution.py:341
  8.7 2.6 %collective-permute-start = (bf16[1024,256]{1,0:T(8,128)(2,1)}, bf16[1024,256]{1,0:T(8,128)(2,1)S(1)}, u32[]{:S(2)}, u32[]{:S(2)}) collective-permute-start(bf16[1024,256]{1,0:T(8,128)(2,1)} %own.1), channel_id=1, source_target_pairs={{0,2},{1,3},{2,0},{3,1},{4,6},{5,7},{6,4},{7,5},{8,10},{9,11},{10,... | collective-permute-start | bytes 1572872 | tf_op jit(solution)/shard_map/ppermute | solution.py:344
  11.3 1.4 %edges.1 = bf16[32,256]{1,0:T(8,128)(2,1)} custom-call(bf16[1024,256]{1,0:T(8,128)(2,1)} %value.3, bf16[1024,256]{1,0:T(8,128)(2,1)} %gate.3, bf16[1024,256]{1,0:T(8,128)(2,1)} %value.3, bf16[1024,256]{1,0:T(8,128)(2,1)} %gate.3), custom_call_target="tpu_custom_call" | custom-call | tf_op jit(solution)/shard_map/edges/pallas_call | solution.py:332
  12.7 4.2 %collective-permute-start.2 = (bf16[32,256]{1,0:T(8,128)(2,1)}, bf16[32,256]{1,0:T(8,128)(2,1)S(1)}, u32[]{:S(2)}, u32[]{:S(2)}) collective-permute-start(bf16[32,256]{1,0:T(8,128)(2,1)} %edges.1), channel_id=1, source_target_pairs={{4,8},{12,16},{20,24},{28,32},{36,40},{44,48},{52,56},{60,64},{68,... | collective-permute-start | bytes 49160 | tf_op jit(solution)/shard_map/ppermute | solution.py:343
  16.9 4.5 %collective-permute-start.1 = (bf16[32,256]{1,0:T(8,128)(2,1)}, bf16[32,256]{1,0:T(8,128)(2,1)S(1)}, u32[]{:S(2)}, u32[]{:S(2)}) collective-permute-start(bf16[32,256]{1,0:T(8,128)(2,1)} %edges.1), channel_id=1, source_target_pairs={{0,4},{4,0},{8,12},{12,8},{16,20},{20,16},{24,28},{28,24},{32,36},... | collective-permute-start | bytes 49160 | tf_op jit(solution)/shard_map/ppermute | solution.py:342
  21.4 1.0 %collective-permute-done.1.inner = bf16[32,256]{1,0:T(8,128)(2,1)S(1)} collective-permute-done((bf16[32,256]{1,0:T(8,128)(2,1)}, bf16[32,256]{1,0:T(8,128)(2,1)S(1)}, u32[]{:S(2)}, u32[]{:S(2)}) %collective-permute-start.1) | collective-permute-done | bytes 16416 | tf_op jit(solution)/shard_map/ppermute | solution.py:342
  22.5 5.2 %shard_map.101 = (f32[2,1056,128]{2,1,0:T(8,128)S(1)}, f32[1024,256]{1,0:T(8,128)S(1)}, f32[1024,256]{1,0:T(8,128)S(1)}, f32[1024,256]{1,0:T(8,128)S(1)}, bf16[1024,256]{1,0:T(8,128)(2,1)S(1)}) custom-call(bf16[1024,256]{1,0:T(8,128)(2,1)S(1)} %copy-done, bf16[1024,256]{1,0:T(8,128)(2,1)S(1)} %copy-done.1, bf16[32,256]{1,0:T(8,128)(2,1)S(1)} %collective-permute-done.1.inner, ...), custom_call_target="tpu_custom_call" | custom-call | flops 1400000000 | bytes 1048576 | tf_op jit(solution)/shard_map/pallas_call | solution.py:346
  27.8 1.8 %shard_map.102 = (f32[1024,256]{1,0:T(8,128)S(1)}, bf16[8,6,8,256]{3,2,1,0:T(8,128)(2,1)S(1)}, bf16[8,6,8,256]{3,2,1,0:T(8,128)(2,1)S(1)}) custom-call(bf16[1024,256]{1,0:T(8,128)(2,1)S(1)} %copy-done.4, bf16[1024,256]{1,0:T(8,128)(2,1)S(1)} %collective-permute-done.3.left, bf16[1024,256]{1,0:T(8,128)(2,1)S(1)} %collective-permute-done.4.right, ...), custom_call_target="tpu_custom_call" | custom-call | flops 800000000 | bytes 1048576 | tf_op jit(solution)/shard_map/pallas_call | solution.py:361
  29.5 7.9 %collective-permute-start.5 = (bf16[8,6,8,256]{3,2,1,0:T(8,128)(2,1)S(1)}, bf16[8,6,8,256]{3,2,1,0:T(8,128)(2,1)S(1)}, u32[]{:S(2)}, u32[]{:S(2)}) collective-permute-start(bf16[8,6,8,256]{3,2,1,0:T(8,128)(2,1)S(1)} %get-tuple-element.35), channel_id=1, source_target_pairs={{0,4},{4,0},{8,12},{12,8},{16,20},{20,16},{24,28},{28,24},{32,36},... | collective-permute-start | bytes 589832 | tf_op jit(solution)/shard_map/ppermute | solution.py:365
  37.4 1.0 %collective-permute-done.5.taken = bf16[8,6,8,256]{3,2,1,0:T(8,128)(2,1)S(1)} collective-permute-done((bf16[8,6,8,256]{3,2,1,0:T(8,128)(2,1)S(1)}, bf16[8,6,8,256]{3,2,1,0:T(8,128)(2,1)S(1)}, u32[]{:S(2)}, u32[]{:S(2)}) %collective-permute-start.5) | collective-permute-done | bytes 196640 | tf_op jit(solution)/shard_map/ppermute | solution.py:365
  38.5 6.1 %shard_map.103 = (f32[2,1024,128]{2,1,0:T(8,128)S(1)}, f32[32,256]{1,0:T(8,128)S(1)}, bf16[8,12,8,256]{3,2,1,0:T(8,128)(2,1)}) custom-call(bf16[1024,256]{1,0:T(8,128)(2,1)S(1)} %collective-permute-done.far, bf16[1024,256]{1,0:T(8,128)(2,1)S(1)} %copy-done.2, bf16[1024,256]{1,0:T(8,128)(2,1)S(1)} %get-tuple-element.28.normed, ...), custom_call_target="tpu_custom_call" | custom-call | flops 1600000000 | bytes 1048576 | tf_op jit(solution)/shard_map/pallas_call | solution.py:367
  44.6 4.7 %all-to-all-start = ((bf16[8,12,8,256]{3,2,1,0:T(8,128)(2,1)}), bf16[8,12,8,256]{3,2,1,0:T(8,128)(2,1)S(1)}, u32[]{:S(2)}, u32[]{:S(2)}) async-start(bf16[8,12,8,256]{3,2,1,0:T(8,128)(2,1)} %get-tuple-element.36), calls=%async_computation | async-start | bytes 786432 | tf_op jit(solution)/shard_map/all_to_all | solution.py:328
  49.2 3.5 %collective-permute-start.7 = (f32[32,256]{1,0:T(8,128)S(1)}, f32[32,256]{1,0:T(8,128)S(1)}, u32[]{:S(2)}, u32[]{:S(2)}) collective-permute-start(f32[32,256]{1,0:T(8,128)S(1)} %get-tuple-element.37), channel_id=1, source_target_pairs={{4,8},{12,16},{20,24},{28,32},{36,40},{44,48},{52,56},{60,64},{68,... | collective-permute-start | bytes 98312 | tf_op jit(solution)/shard_map/ppermute | solution.py:381
  52.8 1.9 %collective-permute-start.6 = (f32[32,256]{1,0:T(8,128)S(1)}, f32[32,256]{1,0:T(8,128)S(1)}, u32[]{:S(2)}, u32[]{:S(2)}) collective-permute-start(f32[32,256]{1,0:T(8,128)S(1)} %get-tuple-element.37), channel_id=1, source_target_pairs={{0,4},{4,0},{8,12},{12,8},{16,20},{20,16},{24,28},{28,24},{32,36},... | collective-permute-start | bytes 98312 | tf_op jit(solution)/shard_map/ppermute | solution.py:380
  54.7 1.6 %collective-permute-done.7.outer = f32[32,256]{1,0:T(8,128)S(1)} collective-permute-done((f32[32,256]{1,0:T(8,128)S(1)}, f32[32,256]{1,0:T(8,128)S(1)}, u32[]{:S(2)}, u32[]{:S(2)}) %collective-permute-start.7) | collective-permute-done | bytes 32800 | tf_op jit(solution)/shard_map/ppermute | solution.py:381
  56.3 0.7 all-to-all-done.late
  57.0 0.7 shard_map.104
  57.7 15.2 %all-to-all-start.1 = ((bf16[16,3,8,256]{3,2,1,0:T(8,128)(2,1)}), bf16[16,3,8,256]{3,2,1,0:T(8,128)(2,1)S(1)}, u32[]{:S(2)}, u32[]{:S(2)}) async-start(bf16[16,3,8,256]{3,2,1,0:T(8,128)(2,1)} %shard_map.104), calls=%async_computation.1 | async-start | bytes 393216 | tf_op jit(solution)/shard_map/all_to_all | solution.py:328
  72.9 4.1 %shard_map.105 = (bf16[1024,256]{1,0:T(8,128)(2,1)}, bf16[1024,256]{1,0:T(8,128)(2,1)}) custom-call(bf16[1024,256]{1,0:T(8,128)(2,1)S(1)} %copy-done, bf16[1024,256]{1,0:T(8,128)(2,1)S(1)} %copy-done.1, f32[2,1024,128]{2,1,0:T(8,128)S(1)} %get-tuple-element.39.grad, f32[32,256]{1,0:T(8,128)S(1)} %collective-permute-done.6.inner, ...), custom_call_target="tpu_custom_call" | custom-call | flops 1200000000 | bytes 1048576 | tf_op jit(solution)/shard_map/pallas_call | solution.py:386
  77.0 8.2 %all-to-all-done.1.got = bf16[16,3,8,256]{3,2,1,0:T(8,128)(2,1)S(1)} async-done(((bf16[16,3,8,256]{3,2,1,0:T(8,128)(2,1)}), bf16[16,3,8,256]{3,2,1,0:T(8,128)(2,1)S(1)}, u32[]{:S(2)}, u32[]{:S(2)}) %all-to-all-start.1) | async-done | bytes 196640 | tf_op jit(solution)/shard_map/all_to_all | solution.py:328
  85.8 7.0 %collective-permute-start.8 = (f32[16,256]{1,0:T(8,128)S(1)}, f32[16,256]{1,0:T(8,128)S(1)}, u32[]{:S(2)}, u32[]{:S(2)}) collective-permute-start(f32[16,256]{1,0:T(8,128)S(1)} %get-tuple-element.47.mine), channel_id=1, source_target_pairs={{0,4},{4,0},{1,5},{5,1},{2,6},{6,2},{3,7},{7,3},{8,12},{12,8},{9,1... | collective-permute-start | bytes 49160 | tf_op jit(solution)/shard_map/ppermute | solution.py:396
  92.8 0.8 collective-permute-done.8.other
  93.7 0.6 shard_map.107
  (18 shorter events, 0.7 us)
Async XLA Ops:
  0.6 21.8 %copy-start.1 = (bf16[1024,256]{1,0:T(8,128)(2,1)S(1)}, bf16[1024,256]{1,0:T(8,128)(2,1)}, u32[]{:S(2)}) copy-start(bf16[1024,256]{1,0:T(8,128)(2,1)} %gate.3) | copy-start | bytes 1572868
  0.6 21.8 %copy-start = (bf16[1024,256]{1,0:T(8,128)(2,1)S(1)}, bf16[1024,256]{1,0:T(8,128)(2,1)}, u32[]{:S(2)}) copy-start(bf16[1024,256]{1,0:T(8,128)(2,1)} %value.3) | copy-start | bytes 1572868
  0.7 21.8 %copy-start.5 = (bf16[31,256]{1,0:T(8,128)(2,1)S(1)}, bf16[31,256]{1,0:T(8,128)(2,1)}, u32[]{:S(2)}) copy-start(bf16[31,256]{1,0:T(8,128)(2,1)} %taps.3) | copy-start | bytes 47620
  0.7 21.8 %copy-start.3 = (f32[256]{0:T(256)S(1)}, f32[256]{0:T(256)}, u32[]{:S(2)}) copy-start(f32[256]{0:T(256)} %param.9) | copy-start | bytes 3076
  0.7 27.1 %collective-permute-start.3 = (bf16[1024,256]{1,0:T(8,128)(2,1)}, bf16[1024,256]{1,0:T(8,128)(2,1)S(1)}, u32[]{:S(2)}, u32[]{:S(2)}) collective-permute-start(bf16[1024,256]{1,0:T(8,128)(2,1)} %own.1), channel_id=1, source_target_pairs={{0,1},{1,0},{2,3},{3,2},{4,5},{5,4},{6,7},{7,6},{8,9},{9,8},{10,11... | collective-permute-start | bytes 1572872 | tf_op jit(solution)/shard_map/ppermute | solution.py:340
  4.8 22.9 %collective-permute-start.4 = (bf16[1024,256]{1,0:T(8,128)(2,1)}, bf16[1024,256]{1,0:T(8,128)(2,1)S(1)}, u32[]{:S(2)}, u32[]{:S(2)}) collective-permute-start(bf16[1024,256]{1,0:T(8,128)(2,1)} %own.1), channel_id=1, source_target_pairs={{0,3},{1,2},{2,1},{3,0},{4,7},{5,6},{6,5},{7,4},{8,11},{9,10},{10,... | collective-permute-start | bytes 1572872 | tf_op jit(solution)/shard_map/ppermute | solution.py:341
  8.7 28.8 %collective-permute-start = (bf16[1024,256]{1,0:T(8,128)(2,1)}, bf16[1024,256]{1,0:T(8,128)(2,1)S(1)}, u32[]{:S(2)}, u32[]{:S(2)}) collective-permute-start(bf16[1024,256]{1,0:T(8,128)(2,1)} %own.1), channel_id=1, source_target_pairs={{0,2},{1,3},{2,0},{3,1},{4,6},{5,7},{6,4},{7,5},{8,10},{9,11},{10,... | collective-permute-start | bytes 1572872 | tf_op jit(solution)/shard_map/ppermute | solution.py:344
  12.7 8.8 %collective-permute-start.2 = (bf16[32,256]{1,0:T(8,128)(2,1)}, bf16[32,256]{1,0:T(8,128)(2,1)S(1)}, u32[]{:S(2)}, u32[]{:S(2)}) collective-permute-start(bf16[32,256]{1,0:T(8,128)(2,1)} %edges.1), channel_id=1, source_target_pairs={{4,8},{12,16},{20,24},{28,32},{36,40},{44,48},{52,56},{60,64},{68,... | collective-permute-start | bytes 49160 | tf_op jit(solution)/shard_map/ppermute | solution.py:343
  16.9 5.6 %collective-permute-start.1 = (bf16[32,256]{1,0:T(8,128)(2,1)}, bf16[32,256]{1,0:T(8,128)(2,1)S(1)}, u32[]{:S(2)}, u32[]{:S(2)}) collective-permute-start(bf16[32,256]{1,0:T(8,128)(2,1)} %edges.1), channel_id=1, source_target_pairs={{0,4},{4,0},{8,12},{12,8},{16,20},{20,16},{24,28},{28,24},{32,36},... | collective-permute-start | bytes 49160 | tf_op jit(solution)/shard_map/ppermute | solution.py:342
  22.5 5.3 %copy-start.2 = (bf16[1024,256]{1,0:T(8,128)(2,1)S(1)}, bf16[1024,256]{1,0:T(8,128)(2,1)}, u32[]{:S(2)}) copy-start(bf16[1024,256]{1,0:T(8,128)(2,1)} %weight.3) | copy-start | bytes 1572868
  22.5 5.3 %copy-start.4 = (bf16[1024,256]{1,0:T(8,128)(2,1)S(1)}, bf16[1024,256]{1,0:T(8,128)(2,1)}, u32[]{:S(2)}) copy-start(bf16[1024,256]{1,0:T(8,128)(2,1)} %own.1) | copy-start | bytes 1572868
  29.5 8.9 %collective-permute-start.5 = (bf16[8,6,8,256]{3,2,1,0:T(8,128)(2,1)S(1)}, bf16[8,6,8,256]{3,2,1,0:T(8,128)(2,1)S(1)}, u32[]{:S(2)}, u32[]{:S(2)}) collective-permute-start(bf16[8,6,8,256]{3,2,1,0:T(8,128)(2,1)S(1)} %get-tuple-element.35), channel_id=1, source_target_pairs={{0,4},{4,0},{8,12},{12,8},{16,20},{20,16},{24,28},{28,24},{32,36},... | collective-permute-start | bytes 589832 | tf_op jit(solution)/shard_map/ppermute | solution.py:365
  44.6 12.4 %all-to-all-start = ((bf16[8,12,8,256]{3,2,1,0:T(8,128)(2,1)}), bf16[8,12,8,256]{3,2,1,0:T(8,128)(2,1)S(1)}, u32[]{:S(2)}, u32[]{:S(2)}) async-start(bf16[8,12,8,256]{3,2,1,0:T(8,128)(2,1)} %get-tuple-element.36), calls=%async_computation | async-start | bytes 786432 | tf_op jit(solution)/shard_map/all_to_all | solution.py:328
  49.2 7.1 %collective-permute-start.7 = (f32[32,256]{1,0:T(8,128)S(1)}, f32[32,256]{1,0:T(8,128)S(1)}, u32[]{:S(2)}, u32[]{:S(2)}) collective-permute-start(f32[32,256]{1,0:T(8,128)S(1)} %get-tuple-element.37), channel_id=1, source_target_pairs={{4,8},{12,16},{20,24},{28,32},{36,40},{44,48},{52,56},{60,64},{68,... | collective-permute-start | bytes 98312 | tf_op jit(solution)/shard_map/ppermute | solution.py:381
  52.8 3.5 %collective-permute-start.6 = (f32[32,256]{1,0:T(8,128)S(1)}, f32[32,256]{1,0:T(8,128)S(1)}, u32[]{:S(2)}, u32[]{:S(2)}) collective-permute-start(f32[32,256]{1,0:T(8,128)S(1)} %get-tuple-element.37), channel_id=1, source_target_pairs={{0,4},{4,0},{8,12},{12,8},{16,20},{20,16},{24,28},{28,24},{32,36},... | collective-permute-start | bytes 98312 | tf_op jit(solution)/shard_map/ppermute | solution.py:380
  57.7 27.5 %all-to-all-start.1 = ((bf16[16,3,8,256]{3,2,1,0:T(8,128)(2,1)}), bf16[16,3,8,256]{3,2,1,0:T(8,128)(2,1)S(1)}, u32[]{:S(2)}, u32[]{:S(2)}) async-start(bf16[16,3,8,256]{3,2,1,0:T(8,128)(2,1)} %shard_map.104), calls=%async_computation.1 | async-start | bytes 393216 | tf_op jit(solution)/shard_map/all_to_all | solution.py:328
  85.8 7.8 %collective-permute-start.8 = (f32[16,256]{1,0:T(8,128)S(1)}, f32[16,256]{1,0:T(8,128)S(1)}, u32[]{:S(2)}, u32[]{:S(2)}) collective-permute-start(f32[16,256]{1,0:T(8,128)S(1)} %get-tuple-element.47.mine), channel_id=1, source_target_pairs={{0,4},{4,0},{1,5},{5,1},{2,6},{6,2},{3,7},{7,3},{8,12},{12,8},{9,1... | collective-permute-start | bytes 49160 | tf_op jit(solution)/shard_map/ppermute | solution.py:396

commit v8 on v6

--- a/solution.py
+++ b/solution.py
@@ -33,6 +33,10 @@
     )
 
 
+def rounded_mean(x, avg):
+    return jnp.dot(x.astype(BF16), avg, preferred_element_type=F32)
+
+
 def averaging():
     rows = lax.broadcasted_iota(jnp.int32, (CH, CH), 0) // GROUP
     cols = lax.broadcasted_iota(jnp.int32, (CH, CH), 1) // GROUP
@@ -116,7 +120,7 @@
         rows = pl.ds(pl.multiple_of(step * CHUNK, CHUNK), CHUNK)
         raw = conv[rows, :]
         centred = raw - group_mean(raw, avg)
-        scale = lax.rsqrt(group_mean(centred * centred, avg) + EPS)
+        scale = lax.rsqrt(rounded_mean(centred * centred, avg) + EPS)
         unit_rows = centred * scale
         pre = unit_rows * gain_row
         s = jax.nn.sigmoid(pre)
@@ -133,51 +137,27 @@
     return y, lax.bitwise_xor(y, 1), 3 - y, lax.bitwise_xor(y, 2)
 
 
-def early_kernel(own, left, right, weight, normed, partial, kept, given):
-    y = lax.axis_index("tp")
-    blocks = tuple(zip((own, left, right), homes(y)))
-    weights = [weight[pl.ds(pl.multiple_of(at * CH, CH), CH), :] for _, at in blocks]
-
-    def some_rows(step, _):
-        rows = pl.ds(pl.multiple_of(step * CHUNK, CHUNK), CHUNK)
-        total = None
-        for (ref, _), w in zip(blocks, weights):
-            part = jnp.dot(ref[rows, :], w, preferred_element_type=F32)
-            total = part if total is None else total + part
-        partial[rows, :] = total
-        return 0
-
-    lax.fori_loop(0, ROWS // CHUNK, some_rows, 0)
-    for d, (ref, _) in enumerate(blocks):
-        grads = lax.dot_general(
-            ref[...], normed[...], (((0,), (0,)), ((), ())), preferred_element_type=F32
-        )
-        pieces = grads.reshape(4, 8, 8, CH).astype(BF16)
-        for m in range(2):
-            even, odd = pieces[2 * m], pieces[2 * m + 1]
-            kept[:, d * 2 + m], given[:, d * 2 + m] = sides(is_second(), odd, even)
-
-
 def late_kernel(
-    far_top, far_bottom, weight, normed, partial, unit, inv, slope, gain, wide, kept, taken, grad, ends, sums
+    own, left, right, far_top, far_bottom, weight, normed, unit, inv, slope, gain, wide, grad, ends, sums
 ):
     y = lax.axis_index("tp")
-    w = weight[pl.ds(pl.multiple_of(homes(y)[3] * CH, CH), CH), :]
+    weights = [weight[pl.ds(pl.multiple_of(at * CH, CH), CH), :] for at in homes(y)]
     avg = averaging()
     gain_row = gain[...]
 
     def some_rows(step, gain_sum, far, base):
         start = pl.multiple_of(step * CHUNK, CHUNK)
         rows = pl.ds(start + base, CHUNK)
-        normed_grad = partial[rows, :] + jnp.dot(
-            far[pl.ds(start, CHUNK), :], w, preferred_element_type=F32)
+        normed_grad = jnp.dot(far[pl.ds(start, CHUNK), :], weights[3], preferred_element_type=F32)
+        for ref, w in zip((own, left, right), weights):
+            normed_grad = normed_grad + jnp.dot(ref[rows, :], w, preferred_element_type=F32)
         u = unit[rows, :]
         act = normed_grad * slope[rows, :]
         au = act * u
         hat = act * gain_row
         hat_unit = au * gain_row
         rows_grad = inv[rows, :] * (
-            hat - group_mean(hat, avg) - u * group_mean(hat_unit, avg)
+            hat - group_mean(hat, avg) - u * rounded_mean(hat_unit, avg)
         )
         for b in range(2):
             grad[b, rows, :] = rows_grad[:, b * LANES : (b + 1) * LANES]
@@ -193,15 +173,22 @@
         ends[0:PAD, cols] = grad[b, 0:PAD, :]
         ends[PAD : 2 * PAD, cols] = grad[b, ROWS - PAD : ROWS, :]
 
-    sums[:, 0:6] = (kept[...].astype(F32) + taken[...].astype(F32)).astype(BF16)
-    pieces = lax.dot_general(
-        far_top[...], normed[0:HALF, :], (((0,), (0,)), ((), ())), preferred_element_type=F32
-    ) + lax.dot_general(
-        far_bottom[...], normed[HALF:ROWS, :], (((0,), (0,)), ((), ())), preferred_element_type=F32
-    )
-    pieces = pieces.reshape(4, 8, 8, CH).astype(BF16)
-    for near in range(4):
-        sums[:, 6 + near] = pieces[near]
+    def against(block, start, size):
+        return lax.dot_general(
+            block[...],
+            normed[start : start + size, :],
+            (((0,), (0,)), ((), ())),
+            preferred_element_type=F32,
+        )
+
+    for d, block in enumerate((own, left, right, None)):
+        if block is None:
+            grads = against(far_top, 0, HALF) + against(far_bottom, HALF, HALF)
+        else:
+            grads = against(block, 0, ROWS)
+        pieces = grads.reshape(4, 8, 8, CH).astype(BF16)
+        for near in range(4):
+            sums[:, d * 4 + near] = pieces[near]
 
     halves = []
     for b in range(2):
@@ -232,7 +219,7 @@
     for peer in range(8):
         for part in range(2):
             line = (peer % 2) * 16 + part * 8
-            sums[peer, 10 + part] = taps[line : line + 8]
+            sums[peer, 16 + part] = taps[line : line + 8]
 
 
 def backward_kernel(
@@ -269,21 +256,16 @@
 def middle_kernel(late, out):
     y = lax.axis_index("tp")
 
-    def total(tile, peers):
-        sums = None
-        for peer in peers:
-            part = late[peer, tile].astype(F32)
-            sums = part if sums is None else sums + part
+    def total(tile):
+        sums = late[0, tile].astype(F32)
+        for peer in range(1, 8):
+            sums = sums + late[peer, tile].astype(F32)
         return sums.astype(BF16)
 
-    taps = [total(10 + part, range(8)) for part in range(2)]
+    taps = [total(16 + part) for part in range(2)]
     for d, home in enumerate(homes(y)):
         for near in range(4):
-            if d < 3:
-                rows = total(d * 2 + near // 2, range(near % 2, 8, 2))
-            else:
-                rows = total(6 + near, range(8))
-            out[home * 4 + near, 0] = rows
+            out[home * 4 + near, 0] = total(d * 4 + near)
             for part in range(2):
                 out[home * 4 + near, 1 + part] = taps[part]
 
@@ -371,24 +353,30 @@
         cost(7),
     )(value_rows, gate_rows, inner, outer, conv_taps, gain)
 
-    half = shape(8, 6, 8, CH, dtype=BF16)
-    partial, kept, given = call(
-        early_kernel, (shape(ROWS, CH), half, half), [VMEM] * 5, (), cost(4)
-    )(out_grad, left, right, point_weight, normed)
-
-    taken = lax.ppermute(given, SP, pairs)
-
     grad, ends, sums = call(
         late_kernel,
         (
             shape(2, ROWS, LANES),
             shape(2 * PAD, CH),
-            shape(8, 12, 8, CH, dtype=BF16),
+            shape(8, 18, 8, CH, dtype=BF16),
         ),
         [VMEM] * 12,
         (),
         cost(8),
-    )(far_top, far_bottom, point_weight, normed, partial, unit, inv, slope, gain, wide, kept, taken)
+    )(
+        out_grad,
+        left,
+        right,
+        far_top,
+        far_bottom,
+        point_weight,
+        normed,
+        unit,
+        inv,
+        slope,
+        gain,
+        wide,
+    )
     late = exchange(sums, ("x", "c"))
 
     inner = lax.ppermute(ends, SP, pairs)

time: 92.5 us -> 99.6 us (1.077)
  starting transfers between devices: 55.5 us -> 59.3 us
  waiting for transfers between devices: 15 us -> 18.3 us
  local copies, waits for them, and re-layouts: 0.07 us -> 1.08 us
  Pallas kernels: 20.5 us -> 19.5 us
    ppermute x1, starting transfers between devices: 3.77 us -> 9.23 us  [body(): far_top = lax.ppermute(left[:HALF], 'tp', around)]
    ppermute x1, waiting for transfers between devices: 0.01 us -> 3.3 us  [body(): left = lax.ppermute(out_grad, 'tp', beside)]
    ppermute x1 -> x0, starting transfers between devices: 2.82 us -> none  [body(): taken = lax.ppermute(given, SP, pairs)]
    ppermute x1, waiting for transfers between devices: 1.61 us -> 4.3 us  [body(): outer = lax.ppermute(ends, SP, apart)]
    ppermute x1 -> x0, waiting for transfers between devices: 1.05 us -> none  [body(): taken = lax.ppermute(given, SP, pairs)]
    ppermute x1, waiting for transfers between devices: 1.02 us -> 0.01 us  [body(): far_bottom = lax.ppermute(right[HALF:], 'tp', beside)]
    unnamed x12 -> x16, local copies, waits for them, and re-layouts: 0.03 us -> 1.04 us
    pallas_call x2 -> x1, Pallas kernels: 7.86 us -> 7.26 us  [body(): call(late_kernel, (shape(2, ROWS, LANES), shape(2 * PAD, CH), shape(8, 18...]
  transfers between devices with their start and end apart: 12 -> 11, of which waited for: 7 -> 6; matrix products, arithmetic and copies ran while one was open for 0% -> 0% of each run, Pallas kernels for 14% -> 10%
where the time goes in v8:
time: 99.6 us; the launch traced here: 99.1 us
  starting transfers between devices  59.3 us (60%)
  Pallas kernels  19.5 us (20%)
  waiting for transfers between devices  18.3 us (18%)
  local copies, waits for them, and re-layouts  1.08 us (1%)
    all_to_all x2, starting transfers between devices, exchange(): return lax.all_to_all(array, axis, 0, 0, tiled=True)  20.8 us
    ppermute x1, starting transfers between devices, body(): far_top = lax.ppermute(left[:HALF], 'tp', around)  9.23 us
    all_to_all x2, waiting for transfers between devices, exchange(): return lax.all_to_all(array, axis, 0, 0, tiled=True)  8.48 us
    pallas_call x1, Pallas kernels, body(): call(late_kernel, (shape(2, ROWS, LANES), shape(2 * PAD, CH), shape(8, 18...  7.26 us
    ppermute x1, starting transfers between devices, body(): other = lax.ppermute(mine, 'c', ring(2, 1))  7.12 us
    ppermute x1, starting transfers between devices, body(): outer = lax.ppermute(edges, SP, apart)  4.93 us
    pallas_call x1, Pallas kernels, body(): call(forward_kernel, (shape(2, HALO, LANES), shape(ROWS, CH), shape(ROWS,...  4.83 us
    ppermute x1, waiting for transfers between devices, body(): outer = lax.ppermute(ends, SP, apart)  4.3 us
  transfers between devices with their start and end apart: 11, of which 6 were waited for; matrix products, arithmetic and copies ran while one was open for 0% of the time, Pallas kernels for 10%

profile of v8, /device:TPU:1, one launch (start us, length us, event | category | flops | bytes accessed | tf_op | source)
XLA Modules:
  0.0 99.1 jit_solution(5812626709560255985)
XLA Ops:
  0.6 4.0 %collective-permute-start = (bf16[1024,256]{1,0:T(8,128)(2,1)}, bf16[1024,256]{1,0:T(8,128)(2,1)S(1)}, u32[]{:S(2)}, u32[]{:S(2)}) collective-permute-start(bf16[1024,256]{1,0:T(8,128)(2,1)} %own.1), channel_id=1, source_target_pairs={{0,1},{1,0},{2,3},{3,2},{4,5},{5,4},{6,7},{7,6},{8,9},{9,8},{10,11... | collective-permute-start | bytes 1572872 | tf_op jit(solution)/shard_map/ppermute | solution.py:335
  4.7 3.8 %collective-permute-start.1 = (bf16[1024,256]{1,0:T(8,128)(2,1)}, bf16[1024,256]{1,0:T(8,128)(2,1)S(1)}, u32[]{:S(2)}, u32[]{:S(2)}) collective-permute-start(bf16[1024,256]{1,0:T(8,128)(2,1)} %own.1), channel_id=1, source_target_pairs={{0,3},{1,2},{2,1},{3,0},{4,7},{5,6},{6,5},{7,4},{8,11},{9,10},{10,... | collective-permute-start | bytes 1572872 | tf_op jit(solution)/shard_map/ppermute | solution.py:336
  8.5 3.3 %collective-permute-done.left = bf16[1024,256]{1,0:T(8,128)(2,1)S(1)} collective-permute-done((bf16[1024,256]{1,0:T(8,128)(2,1)}, bf16[1024,256]{1,0:T(8,128)(2,1)S(1)}, u32[]{:S(2)}, u32[]{:S(2)}) %collective-permute-start) | collective-permute-done | bytes 524320 | tf_op jit(solution)/shard_map/ppermute | solution.py:335
  11.8 9.2 %collective-permute-start.2 = (bf16[512,256]{1,0:T(8,128)(2,1)S(1)}, bf16[512,256]{1,0:T(8,128)(2,1)S(1)}, u32[]{:S(2)}, u32[]{:S(2)}) collective-permute-start(bf16[512,256]{1,0:T(8,128)(2,1)S(1)} %slice.8), channel_id=1, source_target_pairs={{0,3},{1,2},{2,1},{3,0},{4,7},{5,6},{6,5},{7,4},{8,11},{9,10},{10,... | collective-permute-start | bytes 786440 | tf_op jit(solution)/shard_map/ppermute | solution.py:339
  21.1 2.1 %collective-permute-start.3 = (bf16[512,256]{1,0:T(8,128)(2,1)S(1)}, bf16[512,256]{1,0:T(8,128)(2,1)S(1)}, u32[]{:S(2)}, u32[]{:S(2)}) collective-permute-start(bf16[512,256]{1,0:T(8,128)(2,1)S(1)} %slice.9), channel_id=1, source_target_pairs={{0,1},{1,0},{2,3},{3,2},{4,5},{5,4},{6,7},{7,6},{8,9},{9,8},{10,11... | collective-permute-start | bytes 786440 | tf_op jit(solution)/shard_map/ppermute | solution.py:340
  23.2 1.4 %edges.1 = bf16[32,256]{1,0:T(8,128)(2,1)} custom-call(bf16[1024,256]{1,0:T(8,128)(2,1)} %value.3, bf16[1024,256]{1,0:T(8,128)(2,1)} %gate.3, bf16[1024,256]{1,0:T(8,128)(2,1)} %value.3, bf16[1024,256]{1,0:T(8,128)(2,1)} %gate.3), custom_call_target="tpu_custom_call" | custom-call | tf_op jit(solution)/shard_map/edges/pallas_call | solution.py:325
  24.6 4.9 %collective-permute-start.5 = (bf16[32,256]{1,0:T(8,128)(2,1)}, bf16[32,256]{1,0:T(8,128)(2,1)S(1)}, u32[]{:S(2)}, u32[]{:S(2)}) collective-permute-start(bf16[32,256]{1,0:T(8,128)(2,1)} %edges.1), channel_id=1, source_target_pairs={{4,8},{12,16},{20,24},{28,32},{36,40},{44,48},{52,56},{60,64},{68,... | collective-permute-start | bytes 49160 | tf_op jit(solution)/shard_map/ppermute | solution.py:338
  29.5 1.9 %collective-permute-start.4 = (bf16[32,256]{1,0:T(8,128)(2,1)}, bf16[32,256]{1,0:T(8,128)(2,1)S(1)}, u32[]{:S(2)}, u32[]{:S(2)}) collective-permute-start(bf16[32,256]{1,0:T(8,128)(2,1)} %edges.1), channel_id=1, source_target_pairs={{0,4},{4,0},{8,12},{12,8},{16,20},{20,16},{24,28},{28,24},{32,36},... | collective-permute-start | bytes 49160 | tf_op jit(solution)/shard_map/ppermute | solution.py:337
  31.4 1.3 %collective-permute-done.4.inner = bf16[32,256]{1,0:T(8,128)(2,1)S(1)} collective-permute-done((bf16[32,256]{1,0:T(8,128)(2,1)}, bf16[32,256]{1,0:T(8,128)(2,1)S(1)}, u32[]{:S(2)}, u32[]{:S(2)}) %collective-permute-start.4) | collective-permute-done | bytes 16416 | tf_op jit(solution)/shard_map/ppermute | solution.py:337
  32.8 4.8 %shard_map.101 = (f32[2,1056,128]{2,1,0:T(8,128)S(1)}, f32[1024,256]{1,0:T(8,128)S(1)}, f32[1024,256]{1,0:T(8,128)S(1)}, f32[1024,256]{1,0:T(8,128)S(1)}, bf16[1024,256]{1,0:T(8,128)(2,1)S(1)}) custom-call(bf16[1024,256]{1,0:T(8,128)(2,1)S(1)} %copy-done, bf16[1024,256]{1,0:T(8,128)(2,1)S(1)} %copy-done.1, bf16[32,256]{1,0:T(8,128)(2,1)S(1)} %collective-permute-done.4.inner, ...), custom_call_target="tpu_custom_call" | custom-call | flops 1400000000 | bytes 1048576 | tf_op jit(solution)/shard_map/pallas_call | solution.py:342
  37.7 7.3 %shard_map.102 = (f32[2,1024,128]{2,1,0:T(8,128)S(1)}, f32[32,256]{1,0:T(8,128)S(1)}, bf16[8,18,8,256]{3,2,1,0:T(8,128)(2,1)}) custom-call(bf16[1024,256]{1,0:T(8,128)(2,1)S(1)} %copy-done.2, bf16[1024,256]{1,0:T(8,128)(2,1)S(1)} %collective-permute-done.left, bf16[1024,256]{1,0:T(8,128)(2,1)S(1)} %collective-permute-done.1.right, ...), custom_call_target="tpu_custom_call" | custom-call | flops 1600000000 | bytes 1048576 | tf_op jit(solution)/shard_map/pallas_call | solution.py:356
  45.0 1.0 %copy-done.5 = f32[2,1024,128]{2,1,0:T(8,128)} copy-done((f32[2,1024,128]{2,1,0:T(8,128)}, f32[2,1024,128]{2,1,0:T(8,128)S(1)}, u32[]{:S(2)}) %copy-start.5) | copy-done | bytes 1048600
  46.0 4.7 %all-to-all-start = ((bf16[8,18,8,256]{3,2,1,0:T(8,128)(2,1)}), bf16[8,18,8,256]{3,2,1,0:T(8,128)(2,1)S(1)}, u32[]{:S(2)}, u32[]{:S(2)}) async-start(bf16[8,18,8,256]{3,2,1,0:T(8,128)(2,1)} %get-tuple-element.30), calls=%async_computation | async-start | bytes 1179648 | tf_op jit(solution)/shard_map/all_to_all | solution.py:321
  50.6 3.5 %collective-permute-start.7 = (f32[32,256]{1,0:T(8,128)S(1)}, f32[32,256]{1,0:T(8,128)S(1)}, u32[]{:S(2)}, u32[]{:S(2)}) collective-permute-start(f32[32,256]{1,0:T(8,128)S(1)} %get-tuple-element.31), channel_id=1, source_target_pairs={{4,8},{12,16},{20,24},{28,32},{36,40},{44,48},{52,56},{60,64},{68,... | collective-permute-start | bytes 98312 | tf_op jit(solution)/shard_map/ppermute | solution.py:383
  54.2 1.9 %collective-permute-start.6 = (f32[32,256]{1,0:T(8,128)S(1)}, f32[32,256]{1,0:T(8,128)S(1)}, u32[]{:S(2)}, u32[]{:S(2)}) collective-permute-start(f32[32,256]{1,0:T(8,128)S(1)} %get-tuple-element.31), channel_id=1, source_target_pairs={{0,4},{4,0},{8,12},{12,8},{16,20},{20,16},{24,28},{28,24},{32,36},... | collective-permute-start | bytes 98312 | tf_op jit(solution)/shard_map/ppermute | solution.py:382
  56.1 4.3 %collective-permute-done.7.outer = f32[32,256]{1,0:T(8,128)S(1)} collective-permute-done((f32[32,256]{1,0:T(8,128)S(1)}, f32[32,256]{1,0:T(8,128)S(1)}, u32[]{:S(2)}, u32[]{:S(2)}) %collective-permute-start.7) | collective-permute-done | bytes 32800 | tf_op jit(solution)/shard_map/ppermute | solution.py:383
  60.7 0.7 shard_map.103
  61.4 16.2 %all-to-all-start.1 = ((bf16[16,3,8,256]{3,2,1,0:T(8,128)(2,1)}), bf16[16,3,8,256]{3,2,1,0:T(8,128)(2,1)S(1)}, u32[]{:S(2)}, u32[]{:S(2)}) async-start(bf16[16,3,8,256]{3,2,1,0:T(8,128)(2,1)} %shard_map.103), calls=%async_computation.1 | async-start | bytes 393216 | tf_op jit(solution)/shard_map/all_to_all | solution.py:321
  77.6 4.1 %shard_map.104 = (bf16[1024,256]{1,0:T(8,128)(2,1)}, bf16[1024,256]{1,0:T(8,128)(2,1)}) custom-call(bf16[1024,256]{1,0:T(8,128)(2,1)S(1)} %copy-done, bf16[1024,256]{1,0:T(8,128)(2,1)S(1)} %copy-done.1, f32[2,1024,128]{2,1,0:T(8,128)S(1)} %copy-done.6, f32[32,256]{1,0:T(8,128)S(1)} %collective-permute-done.6.inner, ...), custom_call_target="tpu_custom_call" | custom-call | flops 1200000000 | bytes 1048576 | tf_op jit(solution)/shard_map/pallas_call | solution.py:388
  81.7 8.2 %all-to-all-done.1.got = bf16[16,3,8,256]{3,2,1,0:T(8,128)(2,1)S(1)} async-done(((bf16[16,3,8,256]{3,2,1,0:T(8,128)(2,1)}), bf16[16,3,8,256]{3,2,1,0:T(8,128)(2,1)S(1)}, u32[]{:S(2)}, u32[]{:S(2)}) %all-to-all-start.1) | async-done | bytes 196640 | tf_op jit(solution)/shard_map/all_to_all | solution.py:321
  89.9 0.6 shard_map.105
  90.5 7.1 %collective-permute-start.8 = (f32[16,256]{1,0:T(8,128)S(1)}, f32[16,256]{1,0:T(8,128)S(1)}, u32[]{:S(2)}, u32[]{:S(2)}) collective-permute-start(f32[16,256]{1,0:T(8,128)S(1)} %get-tuple-element.41.mine), channel_id=1, source_target_pairs={{0,4},{4,0},{1,5},{5,1},{2,6},{6,2},{3,7},{7,3},{8,12},{12,8},{9,1... | collective-permute-start | bytes 49160 | tf_op jit(solution)/shard_map/ppermute | solution.py:398
  97.6 0.8 collective-permute-done.8.other
  98.5 0.6 shard_map.106
  (23 shorter events, 0.4 us)
Async XLA Ops:
  0.6 11.1 %collective-permute-start = (bf16[1024,256]{1,0:T(8,128)(2,1)}, bf16[1024,256]{1,0:T(8,128)(2,1)S(1)}, u32[]{:S(2)}, u32[]{:S(2)}) collective-permute-start(bf16[1024,256]{1,0:T(8,128)(2,1)} %own.1), channel_id=1, source_target_pairs={{0,1},{1,0},{2,3},{3,2},{4,5},{5,4},{6,7},{7,6},{8,9},{9,8},{10,11... | collective-permute-start | bytes 1572872 | tf_op jit(solution)/shard_map/ppermute | solution.py:335
  4.7 16.4 %collective-permute-start.1 = (bf16[1024,256]{1,0:T(8,128)(2,1)}, bf16[1024,256]{1,0:T(8,128)(2,1)S(1)}, u32[]{:S(2)}, u32[]{:S(2)}) collective-permute-start(bf16[1024,256]{1,0:T(8,128)(2,1)} %own.1), channel_id=1, source_target_pairs={{0,3},{1,2},{2,1},{3,0},{4,7},{5,6},{6,5},{7,4},{8,11},{9,10},{10,... | collective-permute-start | bytes 1572872 | tf_op jit(solution)/shard_map/ppermute | solution.py:336
  11.8 25.9 %collective-permute-start.2 = (bf16[512,256]{1,0:T(8,128)(2,1)S(1)}, bf16[512,256]{1,0:T(8,128)(2,1)S(1)}, u32[]{:S(2)}, u32[]{:S(2)}) collective-permute-start(bf16[512,256]{1,0:T(8,128)(2,1)S(1)} %slice.8), channel_id=1, source_target_pairs={{0,3},{1,2},{2,1},{3,0},{4,7},{5,6},{6,5},{7,4},{8,11},{9,10},{10,... | collective-permute-start | bytes 786440 | tf_op jit(solution)/shard_map/ppermute | solution.py:339
  21.1 11.7 %copy-start = (bf16[1024,256]{1,0:T(8,128)(2,1)S(1)}, bf16[1024,256]{1,0:T(8,128)(2,1)}, u32[]{:S(2)}) copy-start(bf16[1024,256]{1,0:T(8,128)(2,1)} %value.3) | copy-start | bytes 1572868
  21.1 11.7 %copy-start.1 = (bf16[1024,256]{1,0:T(8,128)(2,1)S(1)}, bf16[1024,256]{1,0:T(8,128)(2,1)}, u32[]{:S(2)}) copy-start(bf16[1024,256]{1,0:T(8,128)(2,1)} %gate.3) | copy-start | bytes 1572868
  21.1 11.7 %copy-start.4 = (f32[256]{0:T(256)S(1)}, f32[256]{0:T(256)}, u32[]{:S(2)}) copy-start(f32[256]{0:T(256)} %param.9) | copy-start | bytes 3076
  21.1 11.7 %copy-start.7 = (bf16[31,256]{1,0:T(8,128)(2,1)S(1)}, bf16[31,256]{1,0:T(8,128)(2,1)}, u32[]{:S(2)}) copy-start(bf16[31,256]{1,0:T(8,128)(2,1)} %taps.3) | copy-start | bytes 47620
  21.1 16.6 %collective-permute-start.3 = (bf16[512,256]{1,0:T(8,128)(2,1)S(1)}, bf16[512,256]{1,0:T(8,128)(2,1)S(1)}, u32[]{:S(2)}, u32[]{:S(2)}) collective-permute-start(bf16[512,256]{1,0:T(8,128)(2,1)S(1)} %slice.9), channel_id=1, source_target_pairs={{0,1},{1,0},{2,3},{3,2},{4,5},{5,4},{6,7},{7,6},{8,9},{9,8},{10,11... | collective-permute-start | bytes 786440 | tf_op jit(solution)/shard_map/ppermute | solution.py:340
  24.6 6.9 %collective-permute-start.5 = (bf16[32,256]{1,0:T(8,128)(2,1)}, bf16[32,256]{1,0:T(8,128)(2,1)S(1)}, u32[]{:S(2)}, u32[]{:S(2)}) collective-permute-start(bf16[32,256]{1,0:T(8,128)(2,1)} %edges.1), channel_id=1, source_target_pairs={{4,8},{12,16},{20,24},{28,32},{36,40},{44,48},{52,56},{60,64},{68,... | collective-permute-start | bytes 49160 | tf_op jit(solution)/shard_map/ppermute | solution.py:338
  29.5 3.3 %collective-permute-start.4 = (bf16[32,256]{1,0:T(8,128)(2,1)}, bf16[32,256]{1,0:T(8,128)(2,1)S(1)}, u32[]{:S(2)}, u32[]{:S(2)}) collective-permute-start(bf16[32,256]{1,0:T(8,128)(2,1)} %edges.1), channel_id=1, source_target_pairs={{0,4},{4,0},{8,12},{12,8},{16,20},{20,16},{24,28},{28,24},{32,36},... | collective-permute-start | bytes 49160 | tf_op jit(solution)/shard_map/ppermute | solution.py:337
  32.8 4.9 %copy-start.2 = (bf16[1024,256]{1,0:T(8,128)(2,1)S(1)}, bf16[1024,256]{1,0:T(8,128)(2,1)}, u32[]{:S(2)}) copy-start(bf16[1024,256]{1,0:T(8,128)(2,1)} %own.1) | copy-start | bytes 1572868
  32.8 4.9 %copy-start.3 = (bf16[1024,256]{1,0:T(8,128)(2,1)S(1)}, bf16[1024,256]{1,0:T(8,128)(2,1)}, u32[]{:S(2)}) copy-start(bf16[1024,256]{1,0:T(8,128)(2,1)} %weight.1) | copy-start | bytes 1572868
  45.0 1.0 %copy-start.5 = (f32[2,1024,128]{2,1,0:T(8,128)}, f32[2,1024,128]{2,1,0:T(8,128)S(1)}, u32[]{:S(2)}) copy-start(f32[2,1024,128]{2,1,0:T(8,128)S(1)} %get-tuple-element.33.grad) | copy-start | bytes 3145732
  46.0 31.6 %copy-start.6 = (f32[2,1024,128]{2,1,0:T(8,128)S(1)}, f32[2,1024,128]{2,1,0:T(8,128)}, u32[]{:S(2)}) copy-start(f32[2,1024,128]{2,1,0:T(8,128)} %copy-done.5) | copy-start | bytes 3145732
  46.0 14.7 %all-to-all-start = ((bf16[8,18,8,256]{3,2,1,0:T(8,128)(2,1)}), bf16[8,18,8,256]{3,2,1,0:T(8,128)(2,1)S(1)}, u32[]{:S(2)}, u32[]{:S(2)}) async-start(bf16[8,18,8,256]{3,2,1,0:T(8,128)(2,1)} %get-tuple-element.30), calls=%async_computation | async-start | bytes 1179648 | tf_op jit(solution)/shard_map/all_to_all | solution.py:321
  50.6 9.8 %collective-permute-start.7 = (f32[32,256]{1,0:T(8,128)S(1)}, f32[32,256]{1,0:T(8,128)S(1)}, u32[]{:S(2)}, u32[]{:S(2)}) collective-permute-start(f32[32,256]{1,0:T(8,128)S(1)} %get-tuple-element.31), channel_id=1, source_target_pairs={{4,8},{12,16},{20,24},{28,32},{36,40},{44,48},{52,56},{60,64},{68,... | collective-permute-start | bytes 98312 | tf_op jit(solution)/shard_map/ppermute | solution.py:383
  54.2 6.2 %collective-permute-start.6 = (f32[32,256]{1,0:T(8,128)S(1)}, f32[32,256]{1,0:T(8,128)S(1)}, u32[]{:S(2)}, u32[]{:S(2)}) collective-permute-start(f32[32,256]{1,0:T(8,128)S(1)} %get-tuple-element.31), channel_id=1, source_target_pairs={{0,4},{4,0},{8,12},{12,8},{16,20},{20,16},{24,28},{28,24},{32,36},... | collective-permute-start | bytes 98312 | tf_op jit(solution)/shard_map/ppermute | solution.py:382
  61.4 28.5 %all-to-all-start.1 = ((bf16[16,3,8,256]{3,2,1,0:T(8,128)(2,1)}), bf16[16,3,8,256]{3,2,1,0:T(8,128)(2,1)S(1)}, u32[]{:S(2)}, u32[]{:S(2)}) async-start(bf16[16,3,8,256]{3,2,1,0:T(8,128)(2,1)} %shard_map.103), calls=%async_computation.1 | async-start | bytes 393216 | tf_op jit(solution)/shard_map/all_to_all | solution.py:321
  90.5 7.9 %collective-permute-start.8 = (f32[16,256]{1,0:T(8,128)S(1)}, f32[16,256]{1,0:T(8,128)S(1)}, u32[]{:S(2)}, u32[]{:S(2)}) collective-permute-start(f32[16,256]{1,0:T(8,128)S(1)} %get-tuple-element.41.mine), channel_id=1, source_target_pairs={{0,4},{4,0},{1,5},{5,1},{2,6},{6,2},{3,7},{7,3},{8,12},{12,8},{9,1... | collective-permute-start | bytes 49160 | tf_op jit(solution)/shard_map/ppermute | solution.py:398

commit v9 on v6

--- a/solution.py
+++ b/solution.py
@@ -133,7 +133,7 @@
     return y, lax.bitwise_xor(y, 1), 3 - y, lax.bitwise_xor(y, 2)
 
 
-def early_kernel(own, left, right, weight, normed, partial, kept, given):
+def early_kernel(own, left, right, weight, normed, partial, wgrad):
     y = lax.axis_index("tp")
     blocks = tuple(zip((own, left, right), homes(y)))
     weights = [weight[pl.ds(pl.multiple_of(at * CH, CH), CH), :] for _, at in blocks]
@@ -153,13 +153,12 @@
             ref[...], normed[...], (((0,), (0,)), ((), ())), preferred_element_type=F32
         )
         pieces = grads.reshape(4, 8, 8, CH).astype(BF16)
-        for m in range(2):
-            even, odd = pieces[2 * m], pieces[2 * m + 1]
-            kept[:, d * 2 + m], given[:, d * 2 + m] = sides(is_second(), odd, even)
+        for near in range(4):
+            wgrad[:, d * 4 + near] = pieces[near]
 
 
 def late_kernel(
-    far_top, far_bottom, weight, normed, partial, unit, inv, slope, gain, wide, kept, taken, grad, ends, sums
+    far_top, far_bottom, weight, normed, partial, unit, inv, slope, gain, wide, begun, grad, ends, sums
 ):
     y = lax.axis_index("tp")
     w = weight[pl.ds(pl.multiple_of(homes(y)[3] * CH, CH), CH), :]
@@ -193,7 +192,7 @@
         ends[0:PAD, cols] = grad[b, 0:PAD, :]
         ends[PAD : 2 * PAD, cols] = grad[b, ROWS - PAD : ROWS, :]
 
-    sums[:, 0:6] = (kept[...].astype(F32) + taken[...].astype(F32)).astype(BF16)
+    sums[:, 0:12] = begun[...]
     pieces = lax.dot_general(
         far_top[...], normed[0:HALF, :], (((0,), (0,)), ((), ())), preferred_element_type=F32
     ) + lax.dot_general(
@@ -201,7 +200,7 @@
     )
     pieces = pieces.reshape(4, 8, 8, CH).astype(BF16)
     for near in range(4):
-        sums[:, 6 + near] = pieces[near]
+        sums[:, 12 + near] = pieces[near]
 
     halves = []
     for b in range(2):
@@ -232,7 +231,7 @@
     for peer in range(8):
         for part in range(2):
             line = (peer % 2) * 16 + part * 8
-            sums[peer, 10 + part] = taps[line : line + 8]
+            sums[peer, 16 + part] = taps[line : line + 8]
 
 
 def backward_kernel(
@@ -269,21 +268,16 @@
 def middle_kernel(late, out):
     y = lax.axis_index("tp")
 
-    def total(tile, peers):
-        sums = None
-        for peer in peers:
-            part = late[peer, tile].astype(F32)
-            sums = part if sums is None else sums + part
+    def total(tile):
+        sums = late[0, tile].astype(F32)
+        for peer in range(1, 8):
+            sums = sums + late[peer, tile].astype(F32)
         return sums.astype(BF16)
 
-    taps = [total(10 + part, range(8)) for part in range(2)]
+    taps = [total(16 + part) for part in range(2)]
     for d, home in enumerate(homes(y)):
         for near in range(4):
-            if d < 3:
-                rows = total(d * 2 + near // 2, range(near % 2, 8, 2))
-            else:
-                rows = total(6 + near, range(8))
-            out[home * 4 + near, 0] = rows
+            out[home * 4 + near, 0] = total(d * 4 + near)
             for part in range(2):
                 out[home * 4 + near, 1 + part] = taps[part]
 
@@ -371,32 +365,28 @@
         cost(7),
     )(value_rows, gate_rows, inner, outer, conv_taps, gain)
 
-    half = shape(8, 6, 8, CH, dtype=BF16)
-    partial, kept, given = call(
-        early_kernel, (shape(ROWS, CH), half, half), [VMEM] * 5, (), cost(4)
+    partial, wgrad = call(
+        early_kernel, (shape(ROWS, CH), shape(8, 12, 8, CH, dtype=BF16)), [VMEM] * 5, (), cost(4)
     )(out_grad, left, right, point_weight, normed)
-
-    taken = lax.ppermute(given, SP, pairs)
 
     grad, ends, sums = call(
         late_kernel,
         (
             shape(2, ROWS, LANES),
             shape(2 * PAD, CH),
-            shape(8, 12, 8, CH, dtype=BF16),
+            shape(8, 18, 8, CH, dtype=BF16),
         ),
-        [VMEM] * 12,
+        [VMEM] * 11,
         (),
         cost(8),
-    )(far_top, far_bottom, point_weight, normed, partial, unit, inv, slope, gain, wide, kept, taken)
+    )(far_top, far_bottom, point_weight, normed, partial, unit, inv, slope, gain, wide, wgrad)
     late = exchange(sums, ("x", "c"))
+
+    sent = call(middle_kernel, shape(16, 3, 8, CH, dtype=BF16), [VMEM], (), cost(1))(late)
+    got = exchange(sent, "z")
 
     inner = lax.ppermute(ends, SP, pairs)
     outer = lax.ppermute(ends, SP, apart)
-    late, inner, outer = lax.optimization_barrier((late, inner, outer))
-    sent = call(middle_kernel, shape(16, 3, 8, CH, dtype=BF16), [VMEM], (), cost(1))(late)
-    got = exchange(sent, "z")
-
     value_grad, gate_grad = call(
         backward_kernel,
         (shape(ROWS, CH, dtype=BF16), shape(ROWS, CH, dtype=BF16)),

time: 92.5 us -> 97.6 us (1.055)
  blocking collectives: 0 us -> 14.6 us
  waiting for transfers between devices: 15 us -> 8.69 us
  starting transfers between devices: 55.5 us -> 53.2 us
    all_to_all x0 -> x1, blocking collectives: none -> 14.6 us  [exchange(): return lax.all_to_all(array, axis, 0, 0, tiled=True)]
    all_to_all x2 -> x1, waiting for transfers between devices: 9.09 us -> 2.04 us  [exchange(): return lax.all_to_all(array, axis, 0, 0, tiled=True)]
    ppermute x1, starting transfers between devices: 3.77 us -> 9.23 us  [body(): far_top = lax.ppermute(left[:HALF], 'tp', around)]
    all_to_all x2 -> x1, starting transfers between devices: 20.3 us -> 15.3 us  [exchange(): return lax.all_to_all(array, axis, 0, 0, tiled=True)]
    ppermute x1, waiting for transfers between devices: 0.01 us -> 3.3 us  [body(): left = lax.ppermute(out_grad, 'tp', beside)]
    ppermute x1 -> x0, starting transfers between devices: 2.82 us -> none  [body(): taken = lax.ppermute(given, SP, pairs)]
    ppermute x1, waiting for transfers between devices: 1.61 us -> 0.48 us  [body(): outer = lax.ppermute(ends, SP, apart)]
    ppermute x1 -> x0, waiting for transfers between devices: 1.05 us -> none  [body(): taken = lax.ppermute(given, SP, pairs)]
  transfers between devices with their start and end apart: 12 -> 10, of which waited for: 7 -> 6; matrix products, arithmetic and copies ran while one was open for 0% -> 0% of each run, Pallas kernels for 14% -> 13%
where the time goes in v9:
time: 97.6 us; the launch traced here: 97 us
  starting transfers between devices  53.2 us (55%)
  Pallas kernels  19.6 us (20%)
  blocking collectives  14.6 us (15%)
  waiting for transfers between devices  8.69 us (9%)
    all_to_all x1, starting transfers between devices, exchange(): return lax.all_to_all(array, axis, 0, 0, tiled=True)  15.3 us
    all_to_all x1, blocking collectives, exchange(): return lax.all_to_all(array, axis, 0, 0, tiled=True)  14.6 us
    ppermute x1, starting transfers between devices, body(): far_top = lax.ppermute(left[:HALF], 'tp', around)  9.23 us
    ppermute x1, starting transfers between devices, body(): other = lax.ppermute(mine, 'c', ring(2, 1))  6.89 us
    pallas_call x1, Pallas kernels, body(): call(late_kernel, (shape(2, ROWS, LANES), shape(2 * PAD, CH), shape(8, 18...  5.24 us
    pallas_call x1, Pallas kernels, body(): call(forward_kernel, (shape(2, HALO, LANES), shape(ROWS, CH), shape(ROWS,...  5.18 us
    ppermute x1, starting transfers between devices, body(): outer = lax.ppermute(edges, SP, apart)  4.93 us
    pallas_call x1, Pallas kernels, body(): call(backward_kernel, (shape(ROWS, CH, dtype=BF16), shape(ROWS, CH, dtype...  4.08 us
  transfers between devices with their start and end apart: 10, of which 6 were waited for; matrix products, arithmetic and copies ran while one was open for 0% of the time, Pallas kernels for 13%

profile of v9, /device:TPU:1, one launch (start us, length us, event | category | flops | bytes accessed | tf_op | source)
XLA Modules:
  0.0 97.0 jit_solution(15357437421333248561)
XLA Ops:
  0.6 4.0 %collective-permute-start = (bf16[1024,256]{1,0:T(8,128)(2,1)}, bf16[1024,256]{1,0:T(8,128)(2,1)S(1)}, u32[]{:S(2)}, u32[]{:S(2)}) collective-permute-start(bf16[1024,256]{1,0:T(8,128)(2,1)} %own.1), channel_id=1, source_target_pairs={{0,1},{1,0},{2,3},{3,2},{4,5},{5,4},{6,7},{7,6},{8,9},{9,8},{10,11... | collective-permute-start | bytes 1572872 | tf_op jit(solution)/shard_map/ppermute | solution.py:347
  4.7 3.8 %collective-permute-start.2 = (bf16[1024,256]{1,0:T(8,128)(2,1)}, bf16[1024,256]{1,0:T(8,128)(2,1)S(1)}, u32[]{:S(2)}, u32[]{:S(2)}) collective-permute-start(bf16[1024,256]{1,0:T(8,128)(2,1)} %own.1), channel_id=1, source_target_pairs={{0,3},{1,2},{2,1},{3,0},{4,7},{5,6},{6,5},{7,4},{8,11},{9,10},{10,... | collective-permute-start | bytes 1572872 | tf_op jit(solution)/shard_map/ppermute | solution.py:348
  8.5 3.3 %collective-permute-done.left = bf16[1024,256]{1,0:T(8,128)(2,1)S(1)} collective-permute-done((bf16[1024,256]{1,0:T(8,128)(2,1)}, bf16[1024,256]{1,0:T(8,128)(2,1)S(1)}, u32[]{:S(2)}, u32[]{:S(2)}) %collective-permute-start) | collective-permute-done | bytes 524320 | tf_op jit(solution)/shard_map/ppermute | solution.py:347
  11.8 9.2 %collective-permute-start.1 = (bf16[512,256]{1,0:T(8,128)(2,1)S(1)}, bf16[512,256]{1,0:T(8,128)(2,1)S(1)}, u32[]{:S(2)}, u32[]{:S(2)}) collective-permute-start(bf16[512,256]{1,0:T(8,128)(2,1)S(1)} %slice.8), channel_id=1, source_target_pairs={{0,3},{1,2},{2,1},{3,0},{4,7},{5,6},{6,5},{7,4},{8,11},{9,10},{10,... | collective-permute-start | bytes 786440 | tf_op jit(solution)/shard_map/ppermute | solution.py:351
  21.1 2.1 %collective-permute-start.3 = (bf16[512,256]{1,0:T(8,128)(2,1)S(1)}, bf16[512,256]{1,0:T(8,128)(2,1)S(1)}, u32[]{:S(2)}, u32[]{:S(2)}) collective-permute-start(bf16[512,256]{1,0:T(8,128)(2,1)S(1)} %slice.9), channel_id=1, source_target_pairs={{0,1},{1,0},{2,3},{3,2},{4,5},{5,4},{6,7},{7,6},{8,9},{9,8},{10,11... | collective-permute-start | bytes 786440 | tf_op jit(solution)/shard_map/ppermute | solution.py:352
  23.2 1.4 %edges.1 = bf16[32,256]{1,0:T(8,128)(2,1)} custom-call(bf16[1024,256]{1,0:T(8,128)(2,1)} %value.3, bf16[1024,256]{1,0:T(8,128)(2,1)} %gate.3, bf16[1024,256]{1,0:T(8,128)(2,1)} %value.3, bf16[1024,256]{1,0:T(8,128)(2,1)} %gate.3), custom_call_target="tpu_custom_call" | custom-call | tf_op jit(solution)/shard_map/edges/pallas_call | solution.py:337
  24.6 4.9 %collective-permute-start.5 = (bf16[32,256]{1,0:T(8,128)(2,1)}, bf16[32,256]{1,0:T(8,128)(2,1)S(1)}, u32[]{:S(2)}, u32[]{:S(2)}) collective-permute-start(bf16[32,256]{1,0:T(8,128)(2,1)} %edges.1), channel_id=1, source_target_pairs={{4,8},{12,16},{20,24},{28,32},{36,40},{44,48},{52,56},{60,64},{68,... | collective-permute-start | bytes 49160 | tf_op jit(solution)/shard_map/ppermute | solution.py:350
  29.5 1.9 %collective-permute-start.4 = (bf16[32,256]{1,0:T(8,128)(2,1)}, bf16[32,256]{1,0:T(8,128)(2,1)S(1)}, u32[]{:S(2)}, u32[]{:S(2)}) collective-permute-start(bf16[32,256]{1,0:T(8,128)(2,1)} %edges.1), channel_id=1, source_target_pairs={{0,4},{4,0},{8,12},{12,8},{16,20},{20,16},{24,28},{28,24},{32,36},... | collective-permute-start | bytes 49160 | tf_op jit(solution)/shard_map/ppermute | solution.py:349
  31.4 1.3 %collective-permute-done.4.inner = bf16[32,256]{1,0:T(8,128)(2,1)S(1)} collective-permute-done((bf16[32,256]{1,0:T(8,128)(2,1)}, bf16[32,256]{1,0:T(8,128)(2,1)S(1)}, u32[]{:S(2)}, u32[]{:S(2)}) %collective-permute-start.4) | collective-permute-done | bytes 16416 | tf_op jit(solution)/shard_map/ppermute | solution.py:349
  32.8 5.2 %shard_map.101 = (f32[2,1056,128]{2,1,0:T(8,128)S(1)}, f32[1024,256]{1,0:T(8,128)S(1)}, f32[1024,256]{1,0:T(8,128)S(1)}, f32[1024,256]{1,0:T(8,128)S(1)}, bf16[1024,256]{1,0:T(8,128)(2,1)S(1)}) custom-call(bf16[1024,256]{1,0:T(8,128)(2,1)S(1)} %copy-done, bf16[1024,256]{1,0:T(8,128)(2,1)S(1)} %copy-done.1, bf16[32,256]{1,0:T(8,128)(2,1)S(1)} %collective-permute-done.4.inner, ...), custom_call_target="tpu_custom_call" | custom-call | flops 1400000000 | bytes 1048576 | tf_op jit(solution)/shard_map/pallas_call | solution.py:354
  38.0 1.8 %shard_map.102 = (f32[1024,256]{1,0:T(8,128)S(1)}, bf16[8,12,8,256]{3,2,1,0:T(8,128)(2,1)S(1)}) custom-call(bf16[1024,256]{1,0:T(8,128)(2,1)S(1)} %copy-done.4, bf16[1024,256]{1,0:T(8,128)(2,1)S(1)} %collective-permute-done.left, bf16[1024,256]{1,0:T(8,128)(2,1)S(1)} %collective-permute-done.2.right, bf16[1024,256]{1,0:T(8,128)(2,1)S(1)} %copy-done.2, ...), custom_call_target="tpu_custom_call" | custom-call | flops 800000000 | bytes 1048576 | tf_op jit(solution)/shard_map/pallas_call | solution.py:368
  39.8 5.2 %shard_map.103 = (f32[2,1024,128]{2,1,0:T(8,128)S(1)}, f32[32,256]{1,0:T(8,128)S(1)}, bf16[8,18,8,256]{3,2,1,0:T(8,128)(2,1)S(1)}) custom-call(bf16[512,256]{1,0:T(8,128)(2,1)S(1)} %collective-permute-done.1.far_top, bf16[512,256]{1,0:T(8,128)(2,1)S(1)} %collective-permute-done.3.far_bottom, bf16[1024,256]{1,0:T(8,128)(2,1)S(1)} %copy-done.2, ...), custom_call_target="tpu_custom_call" | custom-call | flops 1600000000 | bytes 1048576 | tf_op jit(solution)/shard_map/pallas_call | solution.py:372
  45.1 14.6 %all_to_all.10.late = bf16[8,18,8,256]{3,2,1,0:T(8,128)(2,1)S(1)} all-to-all(bf16[8,18,8,256]{3,2,1,0:T(8,128)(2,1)S(1)} %get-tuple-element.31), channel_id=1, replica_groups=mesh['z'=16,'x'=4,'c'=2,'tp'=4] {'x','c'}, dimensions={0} | all-to-all | bytes 1179648 | tf_op jit(solution)/shard_map/all_to_all | solution.py:333
  59.7 0.8 shard_map.104
  60.5 15.3 %all-to-all-start.1 = ((bf16[16,3,8,256]{3,2,1,0:T(8,128)(2,1)}), bf16[16,3,8,256]{3,2,1,0:T(8,128)(2,1)S(1)}, u32[]{:S(2)}, u32[]{:S(2)}) async-start(bf16[16,3,8,256]{3,2,1,0:T(8,128)(2,1)} %shard_map.104), calls=%async_computation.1 | async-start | bytes 393216 | tf_op jit(solution)/shard_map/all_to_all | solution.py:333
  75.7 3.1 %collective-permute-start.7 = (f32[32,256]{1,0:T(8,128)S(1)}, f32[32,256]{1,0:T(8,128)S(1)}, u32[]{:S(2)}, u32[]{:S(2)}) collective-permute-start(f32[32,256]{1,0:T(8,128)S(1)} %get-tuple-element.33), channel_id=1, source_target_pairs={{4,8},{12,16},{20,24},{28,32},{36,40},{44,48},{52,56},{60,64},{68,... | collective-permute-start | bytes 98312 | tf_op jit(solution)/shard_map/ppermute | solution.py:389
  78.8 1.9 %collective-permute-start.6 = (f32[32,256]{1,0:T(8,128)S(1)}, f32[32,256]{1,0:T(8,128)S(1)}, u32[]{:S(2)}, u32[]{:S(2)}) collective-permute-start(f32[32,256]{1,0:T(8,128)S(1)} %get-tuple-element.33), channel_id=1, source_target_pairs={{0,4},{4,0},{8,12},{12,8},{16,20},{20,16},{24,28},{28,24},{32,36},... | collective-permute-start | bytes 98312 | tf_op jit(solution)/shard_map/ppermute | solution.py:388
  81.3 0.7 collective-permute-done.6.inner
  81.9 4.1 %shard_map.105 = (bf16[1024,256]{1,0:T(8,128)(2,1)}, bf16[1024,256]{1,0:T(8,128)(2,1)}) custom-call(bf16[1024,256]{1,0:T(8,128)(2,1)S(1)} %copy-done, bf16[1024,256]{1,0:T(8,128)(2,1)S(1)} %copy-done.1, f32[2,1024,128]{2,1,0:T(8,128)S(1)} %get-tuple-element.32.grad, f32[32,256]{1,0:T(8,128)S(1)} %collective-permute-done.6.inner, ...), custom_call_target="tpu_custom_call" | custom-call | flops 1200000000 | bytes 1048576 | tf_op jit(solution)/shard_map/pallas_call | solution.py:390
  86.0 2.0 %all-to-all-done.1.got = bf16[16,3,8,256]{3,2,1,0:T(8,128)(2,1)S(1)} async-done(((bf16[16,3,8,256]{3,2,1,0:T(8,128)(2,1)}), bf16[16,3,8,256]{3,2,1,0:T(8,128)(2,1)S(1)}, u32[]{:S(2)}, u32[]{:S(2)}) %all-to-all-start.1) | async-done | bytes 196640 | tf_op jit(solution)/shard_map/all_to_all | solution.py:333
  88.1 0.6 shard_map.106
  88.7 6.9 %collective-permute-start.8 = (f32[16,256]{1,0:T(8,128)S(1)}, f32[16,256]{1,0:T(8,128)S(1)}, u32[]{:S(2)}, u32[]{:S(2)}) collective-permute-start(f32[16,256]{1,0:T(8,128)S(1)} %get-tuple-element.39.mine), channel_id=1, source_target_pairs={{0,4},{4,0},{1,5},{5,1},{2,6},{6,2},{3,7},{7,3},{8,12},{12,8},{9,1... | collective-permute-start | bytes 49160 | tf_op jit(solution)/shard_map/ppermute | solution.py:400
  95.6 0.8 collective-permute-done.8.other
  96.4 0.6 shard_map.107
  (19 shorter events, 0.6 us)
Async XLA Ops:
  0.6 11.1 %collective-permute-start = (bf16[1024,256]{1,0:T(8,128)(2,1)}, bf16[1024,256]{1,0:T(8,128)(2,1)S(1)}, u32[]{:S(2)}, u32[]{:S(2)}) collective-permute-start(bf16[1024,256]{1,0:T(8,128)(2,1)} %own.1), channel_id=1, source_target_pairs={{0,1},{1,0},{2,3},{3,2},{4,5},{5,4},{6,7},{7,6},{8,9},{9,8},{10,11... | collective-permute-start | bytes 1572872 | tf_op jit(solution)/shard_map/ppermute | solution.py:347
  4.7 16.4 %collective-permute-start.2 = (bf16[1024,256]{1,0:T(8,128)(2,1)}, bf16[1024,256]{1,0:T(8,128)(2,1)S(1)}, u32[]{:S(2)}, u32[]{:S(2)}) collective-permute-start(bf16[1024,256]{1,0:T(8,128)(2,1)} %own.1), channel_id=1, source_target_pairs={{0,3},{1,2},{2,1},{3,0},{4,7},{5,6},{6,5},{7,4},{8,11},{9,10},{10,... | collective-permute-start | bytes 1572872 | tf_op jit(solution)/shard_map/ppermute | solution.py:348
  11.8 28.0 %collective-permute-start.1 = (bf16[512,256]{1,0:T(8,128)(2,1)S(1)}, bf16[512,256]{1,0:T(8,128)(2,1)S(1)}, u32[]{:S(2)}, u32[]{:S(2)}) collective-permute-start(bf16[512,256]{1,0:T(8,128)(2,1)S(1)} %slice.8), channel_id=1, source_target_pairs={{0,3},{1,2},{2,1},{3,0},{4,7},{5,6},{6,5},{7,4},{8,11},{9,10},{10,... | collective-permute-start | bytes 786440 | tf_op jit(solution)/shard_map/ppermute | solution.py:351
  21.1 11.7 %copy-start = (bf16[1024,256]{1,0:T(8,128)(2,1)S(1)}, bf16[1024,256]{1,0:T(8,128)(2,1)}, u32[]{:S(2)}) copy-start(bf16[1024,256]{1,0:T(8,128)(2,1)} %value.3) | copy-start | bytes 1572868
  21.1 11.7 %copy-start.1 = (bf16[1024,256]{1,0:T(8,128)(2,1)S(1)}, bf16[1024,256]{1,0:T(8,128)(2,1)}, u32[]{:S(2)}) copy-start(bf16[1024,256]{1,0:T(8,128)(2,1)} %gate.3) | copy-start | bytes 1572868
  21.1 11.7 %copy-start.3 = (f32[256]{0:T(256)S(1)}, f32[256]{0:T(256)}, u32[]{:S(2)}) copy-start(f32[256]{0:T(256)} %param.9) | copy-start | bytes 3076
  21.1 11.7 %copy-start.5 = (bf16[31,256]{1,0:T(8,128)(2,1)S(1)}, bf16[31,256]{1,0:T(8,128)(2,1)}, u32[]{:S(2)}) copy-start(bf16[31,256]{1,0:T(8,128)(2,1)} %taps.3) | copy-start | bytes 47620
  21.1 18.7 %collective-permute-start.3 = (bf16[512,256]{1,0:T(8,128)(2,1)S(1)}, bf16[512,256]{1,0:T(8,128)(2,1)S(1)}, u32[]{:S(2)}, u32[]{:S(2)}) collective-permute-start(bf16[512,256]{1,0:T(8,128)(2,1)S(1)} %slice.9), channel_id=1, source_target_pairs={{0,1},{1,0},{2,3},{3,2},{4,5},{5,4},{6,7},{7,6},{8,9},{9,8},{10,11... | collective-permute-start | bytes 786440 | tf_op jit(solution)/shard_map/ppermute | solution.py:352
  24.6 6.9 %collective-permute-start.5 = (bf16[32,256]{1,0:T(8,128)(2,1)}, bf16[32,256]{1,0:T(8,128)(2,1)S(1)}, u32[]{:S(2)}, u32[]{:S(2)}) collective-permute-start(bf16[32,256]{1,0:T(8,128)(2,1)} %edges.1), channel_id=1, source_target_pairs={{4,8},{12,16},{20,24},{28,32},{36,40},{44,48},{52,56},{60,64},{68,... | collective-permute-start | bytes 49160 | tf_op jit(solution)/shard_map/ppermute | solution.py:350
  29.5 3.3 %collective-permute-start.4 = (bf16[32,256]{1,0:T(8,128)(2,1)}, bf16[32,256]{1,0:T(8,128)(2,1)S(1)}, u32[]{:S(2)}, u32[]{:S(2)}) collective-permute-start(bf16[32,256]{1,0:T(8,128)(2,1)} %edges.1), channel_id=1, source_target_pairs={{0,4},{4,0},{8,12},{12,8},{16,20},{20,16},{24,28},{28,24},{32,36},... | collective-permute-start | bytes 49160 | tf_op jit(solution)/shard_map/ppermute | solution.py:349
  32.8 5.2 %copy-start.2 = (bf16[1024,256]{1,0:T(8,128)(2,1)S(1)}, bf16[1024,256]{1,0:T(8,128)(2,1)}, u32[]{:S(2)}) copy-start(bf16[1024,256]{1,0:T(8,128)(2,1)} %weight.3) | copy-start | bytes 1572868
  32.8 5.2 %copy-start.4 = (bf16[1024,256]{1,0:T(8,128)(2,1)S(1)}, bf16[1024,256]{1,0:T(8,128)(2,1)}, u32[]{:S(2)}) copy-start(bf16[1024,256]{1,0:T(8,128)(2,1)} %own.1) | copy-start | bytes 1572868
  60.5 27.6 %all-to-all-start.1 = ((bf16[16,3,8,256]{3,2,1,0:T(8,128)(2,1)}), bf16[16,3,8,256]{3,2,1,0:T(8,128)(2,1)S(1)}, u32[]{:S(2)}, u32[]{:S(2)}) async-start(bf16[16,3,8,256]{3,2,1,0:T(8,128)(2,1)} %shard_map.104), calls=%async_computation.1 | async-start | bytes 393216 | tf_op jit(solution)/shard_map/all_to_all | solution.py:333
  75.7 5.5 %collective-permute-start.7 = (f32[32,256]{1,0:T(8,128)S(1)}, f32[32,256]{1,0:T(8,128)S(1)}, u32[]{:S(2)}, u32[]{:S(2)}) collective-permute-start(f32[32,256]{1,0:T(8,128)S(1)} %get-tuple-element.33), channel_id=1, source_target_pairs={{4,8},{12,16},{20,24},{28,32},{36,40},{44,48},{52,56},{60,64},{68,... | collective-permute-start | bytes 98312 | tf_op jit(solution)/shard_map/ppermute | solution.py:389
  78.8 3.1 %collective-permute-start.6 = (f32[32,256]{1,0:T(8,128)S(1)}, f32[32,256]{1,0:T(8,128)S(1)}, u32[]{:S(2)}, u32[]{:S(2)}) collective-permute-start(f32[32,256]{1,0:T(8,128)S(1)} %get-tuple-element.33), channel_id=1, source_target_pairs={{0,4},{4,0},{8,12},{12,8},{16,20},{20,16},{24,28},{28,24},{32,36},... | collective-permute-start | bytes 98312 | tf_op jit(solution)/shard_map/ppermute | solution.py:388
  88.7 7.7 %collective-permute-start.8 = (f32[16,256]{1,0:T(8,128)S(1)}, f32[16,256]{1,0:T(8,128)S(1)}, u32[]{:S(2)}, u32[]{:S(2)}) collective-permute-start(f32[16,256]{1,0:T(8,128)S(1)} %get-tuple-element.39.mine), channel_id=1, source_target_pairs={{0,4},{4,0},{1,5},{5,1},{2,6},{6,2},{3,7},{7,3},{8,12},{12,8},{9,1... | collective-permute-start | bytes 49160 | tf_op jit(solution)/shard_map/ppermute | solution.py:400

commit v10 on v9

--- a/solution.py
+++ b/solution.py
@@ -81,14 +81,11 @@
     edges[PAD : 2 * PAD, :] = gated(value_tail, gate_tail)
 
 
-def forward_kernel(
-    value, gate, inner, outer, taps, gain, wide, unit, inv, slope, normed, conv
-):
+def prepare_kernel(value, gate, taps, wide, conv):
     lanes = [slice(b * LANES, (b + 1) * LANES) for b in range(2)]
-    before, after = neighbours(inner, outer)
     for b in range(2):
-        wide[b, 0:PAD, :] = before[:, lanes[b]]
-        wide[b, PAD + ROWS : HALO, :] = after[:, lanes[b]]
+        wide[b, 0:PAD, :] = jnp.zeros((PAD, LANES), F32)
+        wide[b, PAD + ROWS : HALO, :] = jnp.zeros((PAD, LANES), F32)
 
     def gate_rows(step, _):
         start = pl.multiple_of(step * 64, 64)
@@ -109,12 +106,27 @@
     convolve(
         wide, lambda k, b: jnp.broadcast_to(lines[k : k + 1, lanes[b]], (8, LANES)), store
     )
+
+
+def forward_kernel(inner, outer, taps, gain, plain, conv, wide, unit, inv, slope, normed, fixed):
+    lanes = [slice(b * LANES, (b + 1) * LANES) for b in range(2)]
+    lines = taps[...].astype(F32)
+    before, after = neighbours(inner, outer)
+    for b in range(2):
+        wide[b, 0:PAD, :] = before[:, lanes[b]]
+        wide[b, PAD : PAD + ROWS, :] = plain[b, PAD : PAD + ROWS, :]
+        wide[b, PAD + ROWS : HALO, :] = after[:, lanes[b]]
+        for at, start in enumerate((0, 8, ROWS - 16, ROWS - 8)):
+            total = None
+            for k in range(KW):
+                part = wide[b, start + k + 1 : start + k + 9, :] * lines[k : k + 1, lanes[b]]
+                total = part if total is None else total + part
+            fixed[at * 8 : at * 8 + 8, lanes[b]] = total
     avg = averaging()
     gain_row = gain[...]
 
-    def norm_rows(step, _):
-        rows = pl.ds(pl.multiple_of(step * CHUNK, CHUNK), CHUNK)
-        raw = conv[rows, :]
+    def norm_rows(start, raw):
+        rows = pl.ds(start, CHUNK)
         centred = raw - group_mean(raw, avg)
         scale = lax.rsqrt(group_mean(centred * centred, avg) + EPS)
         unit_rows = centred * scale
@@ -124,9 +136,16 @@
         inv[rows, :] = scale
         slope[rows, :] = s * (1.0 + pre * (1.0 - s))
         normed[rows, :] = (pre * s).astype(BF16)
+
+    def middle_rows(step, _):
+        start = pl.multiple_of(step * CHUNK, CHUNK)
+        norm_rows(start, conv[pl.ds(start, CHUNK), :])
         return 0
 
-    lax.fori_loop(0, ROWS // CHUNK, norm_rows, 0)
+    norm_rows(0, jnp.concatenate([fixed[0:16, :], conv[16:CHUNK, :]], axis=0))
+    lax.fori_loop(1, ROWS // CHUNK - 1, middle_rows, 0)
+    last = ROWS - CHUNK
+    norm_rows(last, jnp.concatenate([conv[last : ROWS - 16, :], fixed[16:32, :]], axis=0))
 
 
 def homes(y):
@@ -351,6 +370,9 @@
     far_top = lax.ppermute(left[:HALF], "tp", around)
     far_bottom = lax.ppermute(right[HALF:], "tp", beside)
 
+    plain, conv = call(
+        prepare_kernel, (shape(2, HALO, LANES), shape(ROWS, CH)), [VMEM] * 3, (), cost(4)
+    )(value_rows, gate_rows, conv_taps)
     wide, unit, inv, slope, normed = call(
         forward_kernel,
         (
@@ -361,9 +383,9 @@
             shape(ROWS, CH, dtype=BF16),
         ),
         [VMEM] * 6,
-        [pltpu.VMEM((ROWS, CH), F32)],
-        cost(7),
-    )(value_rows, gate_rows, inner, outer, conv_taps, gain)
+        [pltpu.VMEM((32, CH), F32)],
+        cost(3),
+    )(inner, outer, conv_taps, gain, plain, conv)
 
     partial, wgrad = call(
         early_kernel, (shape(ROWS, CH), shape(8, 12, 8, CH, dtype=BF16)), [VMEM] * 5, (), cost(4)

time: 97.6 us -> 97.2 us (level)
  waiting for transfers between devices: 8.69 us -> 7.55 us
    pallas_call x0 -> x1, Pallas kernels: none -> 3.01 us  [body(): call(prepare_kernel, (shape(2, HALO, LANES), shape(ROWS, CH)), [VMEM] * 3...]
    ppermute x1, waiting for transfers between devices: 0.48 us -> 3.42 us  [body(): outer = lax.ppermute(ends, SP, apart)]
    pallas_call x1, Pallas kernels: 5.18 us -> 2.29 us  [body(): call(forward_kernel, (shape(2, HALO, LANES), shape(ROWS, CH), shape(ROWS,...]
    ppermute x1, starting transfers between devices: 1.92 us -> 3.96 us  [body(): inner = lax.ppermute(edges, SP, pairs)]
    all_to_all x1, waiting for transfers between devices: 2.04 us -> 0.01 us  [exchange(): return lax.all_to_all(array, axis, 0, 0, tiled=True)]
    ppermute x1, starting transfers between devices: 4.93 us -> 3.02 us  [body(): outer = lax.ppermute(edges, SP, apart)]
    ppermute x1, waiting for transfers between devices: 1.35 us -> 0.01 us  [body(): inner = lax.ppermute(edges, SP, pairs)]
    ppermute x1, starting transfers between devices: 3.11 us -> 2.09 us  [body(): outer = lax.ppermute(ends, SP, apart)]
  transfers between devices with their start and end apart: 10 -> 10, of which waited for: 6 -> 3; matrix products, arithmetic and copies ran while one was open for 0% -> 0% of each run, Pallas kernels for 13% -> 13%
where the time goes in v10:
time: 97.2 us; the launch traced here: 96.6 us
  starting transfers between devices  52.7 us (54%)
  Pallas kernels  19.8 us (20%)
  blocking collectives  15.5 us (16%)
  waiting for transfers between devices  7.55 us (8%)
    all_to_all x1, blocking collectives, exchange(): return lax.all_to_all(array, axis, 0, 0, tiled=True)  15.5 us
    all_to_all x1, starting transfers between devices, exchange(): return lax.all_to_all(array, axis, 0, 0, tiled=True)  14.9 us
    ppermute x1, starting transfers between devices, body(): far_top = lax.ppermute(left[:HALF], 'tp', around)  9.23 us
    ppermute x1, starting transfers between devices, body(): other = lax.ppermute(mine, 'c', ring(2, 1))  6.68 us
    pallas_call x1, Pallas kernels, body(): call(late_kernel, (shape(2, ROWS, LANES), shape(2 * PAD, CH), shape(8, 18...  5.34 us
    pallas_call x1, Pallas kernels, body(): call(backward_kernel, (shape(ROWS, CH, dtype=BF16), shape(ROWS, CH, dtype...  4.08 us
    ppermute x1, starting transfers between devices, body(): left = lax.ppermute(out_grad, 'tp', beside)  4.02 us
    ppermute x1, starting transfers between devices, body(): inner = lax.ppermute(edges, SP, pairs)  3.96 us
  transfers between devices with their start and end apart: 10, of which 3 were waited for; matrix products, arithmetic and copies ran while one was open for 0% of the time, Pallas kernels for 13%

profile of v10, /device:TPU:1, one launch (start us, length us, event | category | flops | bytes accessed | tf_op | source)
XLA Modules:
  0.0 96.6 jit_solution(5843385048289532891)
XLA Ops:
  0.6 4.0 %collective-permute-start = (bf16[1024,256]{1,0:T(8,128)(2,1)}, bf16[1024,256]{1,0:T(8,128)(2,1)S(1)}, u32[]{:S(2)}, u32[]{:S(2)}) collective-permute-start(bf16[1024,256]{1,0:T(8,128)(2,1)} %own.1), channel_id=1, source_target_pairs={{0,1},{1,0},{2,3},{3,2},{4,5},{5,4},{6,7},{7,6},{8,9},{9,8},{10,11... | collective-permute-start | bytes 1572872 | tf_op jit(solution)/shard_map/ppermute | solution.py:366
  4.7 3.8 %collective-permute-start.2 = (bf16[1024,256]{1,0:T(8,128)(2,1)}, bf16[1024,256]{1,0:T(8,128)(2,1)S(1)}, u32[]{:S(2)}, u32[]{:S(2)}) collective-permute-start(bf16[1024,256]{1,0:T(8,128)(2,1)} %own.1), channel_id=1, source_target_pairs={{0,3},{1,2},{2,1},{3,0},{4,7},{5,6},{6,5},{7,4},{8,11},{9,10},{10,... | collective-permute-start | bytes 1572872 | tf_op jit(solution)/shard_map/ppermute | solution.py:367
  8.5 3.3 %collective-permute-done.left = bf16[1024,256]{1,0:T(8,128)(2,1)S(1)} collective-permute-done((bf16[1024,256]{1,0:T(8,128)(2,1)}, bf16[1024,256]{1,0:T(8,128)(2,1)S(1)}, u32[]{:S(2)}, u32[]{:S(2)}) %collective-permute-start) | collective-permute-done | bytes 524320 | tf_op jit(solution)/shard_map/ppermute | solution.py:366
  11.8 9.2 %collective-permute-start.1 = (bf16[512,256]{1,0:T(8,128)(2,1)S(1)}, bf16[512,256]{1,0:T(8,128)(2,1)S(1)}, u32[]{:S(2)}, u32[]{:S(2)}) collective-permute-start(bf16[512,256]{1,0:T(8,128)(2,1)S(1)} %slice.8), channel_id=1, source_target_pairs={{0,3},{1,2},{2,1},{3,0},{4,7},{5,6},{6,5},{7,4},{8,11},{9,10},{10,... | collective-permute-start | bytes 786440 | tf_op jit(solution)/shard_map/ppermute | solution.py:370
  21.1 0.0 copy-start
  21.1 2.1 %collective-permute-start.3 = (bf16[512,256]{1,0:T(8,128)(2,1)S(1)}, bf16[512,256]{1,0:T(8,128)(2,1)S(1)}, u32[]{:S(2)}, u32[]{:S(2)}) collective-permute-start(bf16[512,256]{1,0:T(8,128)(2,1)S(1)} %slice.9), channel_id=1, source_target_pairs={{0,1},{1,0},{2,3},{3,2},{4,5},{5,4},{6,7},{7,6},{8,9},{9,8},{10,11... | collective-permute-start | bytes 786440 | tf_op jit(solution)/shard_map/ppermute | solution.py:371
  23.2 1.4 %edges.1 = bf16[32,256]{1,0:T(8,128)(2,1)} custom-call(bf16[1024,256]{1,0:T(8,128)(2,1)} %value.3, bf16[1024,256]{1,0:T(8,128)(2,1)} %gate.3, bf16[1024,256]{1,0:T(8,128)(2,1)} %value.3, bf16[1024,256]{1,0:T(8,128)(2,1)} %gate.3), custom_call_target="tpu_custom_call" | custom-call | tf_op jit(solution)/shard_map/edges/pallas_call | solution.py:356
  24.5 4.0 %collective-permute-start.4 = (bf16[32,256]{1,0:T(8,128)(2,1)}, bf16[32,256]{1,0:T(8,128)(2,1)S(1)}, u32[]{:S(2)}, u32[]{:S(2)}) collective-permute-start(bf16[32,256]{1,0:T(8,128)(2,1)} %edges.1), channel_id=1, source_target_pairs={{0,4},{4,0},{8,12},{12,8},{16,20},{20,16},{24,28},{28,24},{32,36},... | collective-permute-start | bytes 49160 | tf_op jit(solution)/shard_map/ppermute | solution.py:368
  28.5 3.0 %collective-permute-start.5 = (bf16[32,256]{1,0:T(8,128)(2,1)}, bf16[32,256]{1,0:T(8,128)(2,1)S(1)}, u32[]{:S(2)}, u32[]{:S(2)}) collective-permute-start(bf16[32,256]{1,0:T(8,128)(2,1)} %edges.1), channel_id=1, source_target_pairs={{4,8},{12,16},{20,24},{28,32},{36,40},{44,48},{52,56},{60,64},{68,... | collective-permute-start | bytes 49160 | tf_op jit(solution)/shard_map/ppermute | solution.py:369
  31.6 3.0 %shard_map.101 = (f32[2,1056,128]{2,1,0:T(8,128)S(1)}, f32[1024,256]{1,0:T(8,128)S(1)}) custom-call(bf16[1024,256]{1,0:T(8,128)(2,1)S(1)} %copy-done, bf16[1024,256]{1,0:T(8,128)(2,1)S(1)} %copy-done.1, bf16[31,256]{1,0:T(8,128)(2,1)S(1)} %copy-done.5), custom_call_target="tpu_custom_call" | custom-call | flops 800000000 | bytes 1048576 | tf_op jit(solution)/shard_map/pallas_call | solution.py:373
  34.6 2.3 %shard_map.102 = (f32[2,1056,128]{2,1,0:T(8,128)S(1)}, f32[1024,256]{1,0:T(8,128)S(1)}, f32[1024,256]{1,0:T(8,128)S(1)}, f32[1024,256]{1,0:T(8,128)S(1)}, bf16[1024,256]{1,0:T(8,128)(2,1)S(1)}) custom-call(bf16[32,256]{1,0:T(8,128)(2,1)S(1)} %collective-permute-done.4.inner, bf16[32,256]{1,0:T(8,128)(2,1)S(1)} %collective-permute-done.5.outer, ...), custom_call_target="tpu_custom_call" | custom-call | flops 600000000 | bytes 1048576 | tf_op jit(solution)/shard_map/pallas_call | solution.py:376
  37.0 1.8 %shard_map.103 = (f32[1024,256]{1,0:T(8,128)S(1)}, bf16[8,12,8,256]{3,2,1,0:T(8,128)(2,1)S(1)}) custom-call(bf16[1024,256]{1,0:T(8,128)(2,1)S(1)} %copy-done.4, bf16[1024,256]{1,0:T(8,128)(2,1)S(1)} %collective-permute-done.left, bf16[1024,256]{1,0:T(8,128)(2,1)S(1)} %collective-permute-done.2.right, bf16[1024,256]{1,0:T(8,128)(2,1)S(1)} %copy-done.2, ...), custom_call_target="tpu_custom_call" | custom-call | flops 800000000 | bytes 1048576 | tf_op jit(solution)/shard_map/pallas_call | solution.py:390
  38.7 5.3 %shard_map.104 = (f32[2,1024,128]{2,1,0:T(8,128)S(1)}, f32[32,256]{1,0:T(8,128)S(1)}, bf16[8,18,8,256]{3,2,1,0:T(8,128)(2,1)S(1)}) custom-call(bf16[512,256]{1,0:T(8,128)(2,1)S(1)} %collective-permute-done.1.far_top, bf16[512,256]{1,0:T(8,128)(2,1)S(1)} %collective-permute-done.3.far_bottom, bf16[1024,256]{1,0:T(8,128)(2,1)S(1)} %copy-done.2, ...), custom_call_target="tpu_custom_call" | custom-call | flops 1600000000 | bytes 1048576 | tf_op jit(solution)/shard_map/pallas_call | solution.py:394
  44.1 15.5 %all_to_all.10.late = bf16[8,18,8,256]{3,2,1,0:T(8,128)(2,1)S(1)} all-to-all(bf16[8,18,8,256]{3,2,1,0:T(8,128)(2,1)S(1)} %get-tuple-element.35), channel_id=1, replica_groups=mesh['z'=16,'x'=4,'c'=2,'tp'=4] {'x','c'}, dimensions={0} | all-to-all | bytes 1179648 | tf_op jit(solution)/shard_map/all_to_all | solution.py:352
  59.6 0.7 shard_map.105
  60.4 14.9 %all-to-all-start.1 = ((bf16[16,3,8,256]{3,2,1,0:T(8,128)(2,1)}), bf16[16,3,8,256]{3,2,1,0:T(8,128)(2,1)S(1)}, u32[]{:S(2)}, u32[]{:S(2)}) async-start(bf16[16,3,8,256]{3,2,1,0:T(8,128)(2,1)} %shard_map.105), calls=%async_computation.1 | async-start | bytes 393216 | tf_op jit(solution)/shard_map/all_to_all | solution.py:352
  75.3 2.9 %collective-permute-start.6 = (f32[32,256]{1,0:T(8,128)S(1)}, f32[32,256]{1,0:T(8,128)S(1)}, u32[]{:S(2)}, u32[]{:S(2)}) collective-permute-start(f32[32,256]{1,0:T(8,128)S(1)} %get-tuple-element.37), channel_id=1, source_target_pairs={{0,4},{4,0},{8,12},{12,8},{16,20},{20,16},{24,28},{28,24},{32,36},... | collective-permute-start | bytes 98312 | tf_op jit(solution)/shard_map/ppermute | solution.py:410
  78.2 2.1 %collective-permute-start.7 = (f32[32,256]{1,0:T(8,128)S(1)}, f32[32,256]{1,0:T(8,128)S(1)}, u32[]{:S(2)}, u32[]{:S(2)}) collective-permute-start(f32[32,256]{1,0:T(8,128)S(1)} %get-tuple-element.37), channel_id=1, source_target_pairs={{4,8},{12,16},{20,24},{28,32},{36,40},{44,48},{52,56},{60,64},{68,... | collective-permute-start | bytes 98312 | tf_op jit(solution)/shard_map/ppermute | solution.py:411
  80.3 3.4 %collective-permute-done.7.outer = f32[32,256]{1,0:T(8,128)S(1)} collective-permute-done((f32[32,256]{1,0:T(8,128)S(1)}, f32[32,256]{1,0:T(8,128)S(1)}, u32[]{:S(2)}, u32[]{:S(2)}) %collective-permute-start.7) | collective-permute-done | bytes 32800 | tf_op jit(solution)/shard_map/ppermute | solution.py:411
  83.8 4.1 %shard_map.106 = (bf16[1024,256]{1,0:T(8,128)(2,1)}, bf16[1024,256]{1,0:T(8,128)(2,1)}) custom-call(bf16[1024,256]{1,0:T(8,128)(2,1)S(1)} %copy-done, bf16[1024,256]{1,0:T(8,128)(2,1)S(1)} %copy-done.1, f32[2,1024,128]{2,1,0:T(8,128)S(1)} %get-tuple-element.36.grad, f32[32,256]{1,0:T(8,128)S(1)} %collective-permute-done.6.inner, ...), custom_call_target="tpu_custom_call" | custom-call | flops 1200000000 | bytes 1048576 | tf_op jit(solution)/shard_map/pallas_call | solution.py:412
  87.8 0.6 shard_map.107
  88.5 6.7 %collective-permute-start.8 = (f32[16,256]{1,0:T(8,128)S(1)}, f32[16,256]{1,0:T(8,128)S(1)}, u32[]{:S(2)}, u32[]{:S(2)}) collective-permute-start(f32[16,256]{1,0:T(8,128)S(1)} %get-tuple-element.43.mine), channel_id=1, source_target_pairs={{0,4},{4,0},{1,5},{5,1},{2,6},{6,2},{3,7},{7,3},{8,12},{12,8},{9,1... | collective-permute-start | bytes 49160 | tf_op jit(solution)/shard_map/ppermute | solution.py:422
  95.1 0.8 collective-permute-done.8.other
  96.0 0.6 shard_map.108
  (20 shorter events, 0.1 us)
Async XLA Ops:
  0.6 11.1 %collective-permute-start = (bf16[1024,256]{1,0:T(8,128)(2,1)}, bf16[1024,256]{1,0:T(8,128)(2,1)S(1)}, u32[]{:S(2)}, u32[]{:S(2)}) collective-permute-start(bf16[1024,256]{1,0:T(8,128)(2,1)} %own.1), channel_id=1, source_target_pairs={{0,1},{1,0},{2,3},{3,2},{4,5},{5,4},{6,7},{7,6},{8,9},{9,8},{10,11... | collective-permute-start | bytes 1572872 | tf_op jit(solution)/shard_map/ppermute | solution.py:366
  4.7 16.4 %collective-permute-start.2 = (bf16[1024,256]{1,0:T(8,128)(2,1)}, bf16[1024,256]{1,0:T(8,128)(2,1)S(1)}, u32[]{:S(2)}, u32[]{:S(2)}) collective-permute-start(bf16[1024,256]{1,0:T(8,128)(2,1)} %own.1), channel_id=1, source_target_pairs={{0,3},{1,2},{2,1},{3,0},{4,7},{5,6},{6,5},{7,4},{8,11},{9,10},{10,... | collective-permute-start | bytes 1572872 | tf_op jit(solution)/shard_map/ppermute | solution.py:367
  11.8 26.9 %collective-permute-start.1 = (bf16[512,256]{1,0:T(8,128)(2,1)S(1)}, bf16[512,256]{1,0:T(8,128)(2,1)S(1)}, u32[]{:S(2)}, u32[]{:S(2)}) collective-permute-start(bf16[512,256]{1,0:T(8,128)(2,1)S(1)} %slice.8), channel_id=1, source_target_pairs={{0,3},{1,2},{2,1},{3,0},{4,7},{5,6},{6,5},{7,4},{8,11},{9,10},{10,... | collective-permute-start | bytes 786440 | tf_op jit(solution)/shard_map/ppermute | solution.py:370
  21.1 10.5 %copy-start = (bf16[1024,256]{1,0:T(8,128)(2,1)S(1)}, bf16[1024,256]{1,0:T(8,128)(2,1)}, u32[]{:S(2)}) copy-start(bf16[1024,256]{1,0:T(8,128)(2,1)} %value.3) | copy-start | bytes 1572868
  21.1 10.5 %copy-start.1 = (bf16[1024,256]{1,0:T(8,128)(2,1)S(1)}, bf16[1024,256]{1,0:T(8,128)(2,1)}, u32[]{:S(2)}) copy-start(bf16[1024,256]{1,0:T(8,128)(2,1)} %gate.3) | copy-start | bytes 1572868
  21.1 10.5 %copy-start.5 = (bf16[31,256]{1,0:T(8,128)(2,1)S(1)}, bf16[31,256]{1,0:T(8,128)(2,1)}, u32[]{:S(2)}) copy-start(bf16[31,256]{1,0:T(8,128)(2,1)} %taps.5) | copy-start | bytes 47620
  21.1 17.6 %collective-permute-start.3 = (bf16[512,256]{1,0:T(8,128)(2,1)S(1)}, bf16[512,256]{1,0:T(8,128)(2,1)S(1)}, u32[]{:S(2)}, u32[]{:S(2)}) collective-permute-start(bf16[512,256]{1,0:T(8,128)(2,1)S(1)} %slice.9), channel_id=1, source_target_pairs={{0,1},{1,0},{2,3},{3,2},{4,5},{5,4},{6,7},{7,6},{8,9},{9,8},{10,11... | collective-permute-start | bytes 786440 | tf_op jit(solution)/shard_map/ppermute | solution.py:371
  24.5 10.1 %copy-start.3 = (f32[256]{0:T(256)S(1)}, f32[256]{0:T(256)}, u32[]{:S(2)}) copy-start(f32[256]{0:T(256)} %param.9) | copy-start | bytes 3076
  24.5 10.0 %collective-permute-start.4 = (bf16[32,256]{1,0:T(8,128)(2,1)}, bf16[32,256]{1,0:T(8,128)(2,1)S(1)}, u32[]{:S(2)}, u32[]{:S(2)}) collective-permute-start(bf16[32,256]{1,0:T(8,128)(2,1)} %edges.1), channel_id=1, source_target_pairs={{0,4},{4,0},{8,12},{12,8},{16,20},{20,16},{24,28},{28,24},{32,36},... | collective-permute-start | bytes 49160 | tf_op jit(solution)/shard_map/ppermute | solution.py:368
  28.5 6.1 %collective-permute-start.5 = (bf16[32,256]{1,0:T(8,128)(2,1)}, bf16[32,256]{1,0:T(8,128)(2,1)S(1)}, u32[]{:S(2)}, u32[]{:S(2)}) collective-permute-start(bf16[32,256]{1,0:T(8,128)(2,1)} %edges.1), channel_id=1, source_target_pairs={{4,8},{12,16},{20,24},{28,32},{36,40},{44,48},{52,56},{60,64},{68,... | collective-permute-start | bytes 49160 | tf_op jit(solution)/shard_map/ppermute | solution.py:369
  34.6 2.3 %copy-start.2 = (bf16[1024,256]{1,0:T(8,128)(2,1)S(1)}, bf16[1024,256]{1,0:T(8,128)(2,1)}, u32[]{:S(2)}) copy-start(bf16[1024,256]{1,0:T(8,128)(2,1)} %weight.3) | copy-start | bytes 1572868
  34.6 2.3 %copy-start.4 = (bf16[1024,256]{1,0:T(8,128)(2,1)S(1)}, bf16[1024,256]{1,0:T(8,128)(2,1)}, u32[]{:S(2)}) copy-start(bf16[1024,256]{1,0:T(8,128)(2,1)} %own.1) | copy-start | bytes 1572868
  60.4 27.5 %all-to-all-start.1 = ((bf16[16,3,8,256]{3,2,1,0:T(8,128)(2,1)}), bf16[16,3,8,256]{3,2,1,0:T(8,128)(2,1)S(1)}, u32[]{:S(2)}, u32[]{:S(2)}) async-start(bf16[16,3,8,256]{3,2,1,0:T(8,128)(2,1)} %shard_map.105), calls=%async_computation.1 | async-start | bytes 393216 | tf_op jit(solution)/shard_map/all_to_all | solution.py:352
  75.3 5.0 %collective-permute-start.6 = (f32[32,256]{1,0:T(8,128)S(1)}, f32[32,256]{1,0:T(8,128)S(1)}, u32[]{:S(2)}, u32[]{:S(2)}) collective-permute-start(f32[32,256]{1,0:T(8,128)S(1)} %get-tuple-element.37), channel_id=1, source_target_pairs={{0,4},{4,0},{8,12},{12,8},{16,20},{20,16},{24,28},{28,24},{32,36},... | collective-permute-start | bytes 98312 | tf_op jit(solution)/shard_map/ppermute | solution.py:410
  78.2 5.5 %collective-permute-start.7 = (f32[32,256]{1,0:T(8,128)S(1)}, f32[32,256]{1,0:T(8,128)S(1)}, u32[]{:S(2)}, u32[]{:S(2)}) collective-permute-start(f32[32,256]{1,0:T(8,128)S(1)} %get-tuple-element.37), channel_id=1, source_target_pairs={{4,8},{12,16},{20,24},{28,32},{36,40},{44,48},{52,56},{60,64},{68,... | collective-permute-start | bytes 98312 | tf_op jit(solution)/shard_map/ppermute | solution.py:411
  88.5 7.5 %collective-permute-start.8 = (f32[16,256]{1,0:T(8,128)S(1)}, f32[16,256]{1,0:T(8,128)S(1)}, u32[]{:S(2)}, u32[]{:S(2)}) collective-permute-start(f32[16,256]{1,0:T(8,128)S(1)} %get-tuple-element.43.mine), channel_id=1, source_target_pairs={{0,4},{4,0},{1,5},{5,1},{2,6},{6,2},{3,7},{7,3},{8,12},{12,8},{9,1... | collective-permute-start | bytes 49160 | tf_op jit(solution)/shard_map/ppermute | solution.py:422

commit v11 on v10

--- a/solution.py
+++ b/solution.py
@@ -152,7 +152,7 @@
     return y, lax.bitwise_xor(y, 1), 3 - y, lax.bitwise_xor(y, 2)
 
 
-def early_kernel(own, left, right, weight, normed, partial, wgrad):
+def early_kernel(own, left, right, weight, normed, partial, kept, given):
     y = lax.axis_index("tp")
     blocks = tuple(zip((own, left, right), homes(y)))
     weights = [weight[pl.ds(pl.multiple_of(at * CH, CH), CH), :] for _, at in blocks]
@@ -172,12 +172,13 @@
             ref[...], normed[...], (((0,), (0,)), ((), ())), preferred_element_type=F32
         )
         pieces = grads.reshape(4, 8, 8, CH).astype(BF16)
-        for near in range(4):
-            wgrad[:, d * 4 + near] = pieces[near]
+        for m in range(2):
+            even, odd = pieces[2 * m], pieces[2 * m + 1]
+            kept[:, d * 2 + m], given[:, d * 2 + m] = sides(is_second(), odd, even)
 
 
 def late_kernel(
-    far_top, far_bottom, weight, normed, partial, unit, inv, slope, gain, wide, begun, grad, ends, sums
+    far_top, far_bottom, weight, normed, partial, unit, inv, slope, gain, wide, kept, taken, grad, ends, sums
 ):
     y = lax.axis_index("tp")
     w = weight[pl.ds(pl.multiple_of(homes(y)[3] * CH, CH), CH), :]
@@ -211,7 +212,7 @@
         ends[0:PAD, cols] = grad[b, 0:PAD, :]
         ends[PAD : 2 * PAD, cols] = grad[b, ROWS - PAD : ROWS, :]
 
-    sums[:, 0:12] = begun[...]
+    sums[:, 0:6] = (kept[...].astype(F32) + taken[...].astype(F32)).astype(BF16)
     pieces = lax.dot_general(
         far_top[...], normed[0:HALF, :], (((0,), (0,)), ((), ())), preferred_element_type=F32
     ) + lax.dot_general(
@@ -219,7 +220,7 @@
     )
     pieces = pieces.reshape(4, 8, 8, CH).astype(BF16)
     for near in range(4):
-        sums[:, 12 + near] = pieces[near]
+        sums[:, 6 + near] = pieces[near]
 
     halves = []
     for b in range(2):
@@ -250,7 +251,7 @@
     for peer in range(8):
         for part in range(2):
             line = (peer % 2) * 16 + part * 8
-            sums[peer, 16 + part] = taps[line : line + 8]
+            sums[peer, 10 + part] = taps[line : line + 8]
 
 
 def backward_kernel(
@@ -287,16 +288,21 @@
 def middle_kernel(late, out):
     y = lax.axis_index("tp")
 
-    def total(tile):
-        sums = late[0, tile].astype(F32)
-        for peer in range(1, 8):
-            sums = sums + late[peer, tile].astype(F32)
+    def total(tile, peers):
+        sums = None
+        for peer in peers:
+            part = late[peer, tile].astype(F32)
+            sums = part if sums is None else sums + part
         return sums.astype(BF16)
 
-    taps = [total(16 + part) for part in range(2)]
+    taps = [total(10 + part, range(8)) for part in range(2)]
     for d, home in enumerate(homes(y)):
         for near in range(4):
-            out[home * 4 + near, 0] = total(d * 4 + near)
+            if d < 3:
+                rows = total(d * 2 + near // 2, range(near % 2, 8, 2))
+            else:
+                rows = total(6 + near, range(8))
+            out[home * 4 + near, 0] = rows
             for part in range(2):
                 out[home * 4 + near, 1 + part] = taps[part]
 
@@ -387,21 +393,24 @@
         cost(3),
     )(inner, outer, conv_taps, gain, plain, conv)
 
-    partial, wgrad = call(
-        early_kernel, (shape(ROWS, CH), shape(8, 12, 8, CH, dtype=BF16)), [VMEM] * 5, (), cost(4)
+    half = shape(8, 6, 8, CH, dtype=BF16)
+    partial, kept, given = call(
+        early_kernel, (shape(ROWS, CH), half, half), [VMEM] * 5, (), cost(4)
     )(out_grad, left, right, point_weight, normed)
+
+    taken = lax.ppermute(given, SP, pairs)
 
     grad, ends, sums = call(
         late_kernel,
         (
             shape(2, ROWS, LANES),
             shape(2 * PAD, CH),
-            shape(8, 18, 8, CH, dtype=BF16),
+            shape(8, 12, 8, CH, dtype=BF16),
         ),
-        [VMEM] * 11,
+        [VMEM] * 12,
         (),
         cost(8),
-    )(far_top, far_bottom, point_weight, normed, partial, unit, inv, slope, gain, wide, wgrad)
+    )(far_top, far_bottom, point_weight, normed, partial, unit, inv, slope, gain, wide, kept, taken)
     late = exchange(sums, ("x", "c"))
 
     sent = call(middle_kernel, shape(16, 3, 8, CH, dtype=BF16), [VMEM], (), cost(1))(late)

time: 97.2 us -> 89.8 us (0.924)
  blocking collectives: 15.5 us -> 10.4 us
  starting transfers between devices: 52.7 us -> 50.3 us
    all_to_all x1, blocking collectives: 15.5 us -> 10.4 us  [exchange(): return lax.all_to_all(array, axis, 0, 0, tiled=True)]
    ppermute x1, starting transfers between devices: 9.23 us -> 4.85 us  [body(): far_top = lax.ppermute(left[:HALF], 'tp', around)]
    ppermute x1, waiting for transfers between devices: 3.3 us -> 0.01 us  [body(): left = lax.ppermute(out_grad, 'tp', beside)]
    ppermute x0 -> x1, starting transfers between devices: none -> 1.92 us  [body(): taken = lax.ppermute(given, SP, pairs)]
    ppermute x1, waiting for transfers between devices: 0.01 us -> 1.56 us  [body(): far_bottom = lax.ppermute(right[HALF:], 'tp', beside)]
    ppermute x0 -> x1, waiting for transfers between devices: none -> 1.41 us  [body(): taken = lax.ppermute(given, SP, pairs)]
    ppermute x1, starting transfers between devices: 3.02 us -> 1.92 us  [body(): outer = lax.ppermute(edges, SP, apart)]
  transfers between devices with their start and end apart: 10 -> 11, of which waited for: 3 -> 5; matrix products, arithmetic and copies ran while one was open for 0% -> 0% of each run, Pallas kernels for 13% -> 14%
where the time goes in v11:
time: 89.8 us; the launch traced here: 89.2 us
  starting transfers between devices  50.3 us (56%)
  Pallas kernels  19.8 us (22%)
  blocking collectives  10.4 us (12%)
  waiting for transfers between devices  7.85 us (9%)
    all_to_all x1, starting transfers between devices, exchange(): return lax.all_to_all(array, axis, 0, 0, tiled=True)  14.9 us
    all_to_all x1, blocking collectives, exchange(): return lax.all_to_all(array, axis, 0, 0, tiled=True)  10.4 us
    ppermute x1, starting transfers between devices, body(): other = lax.ppermute(mine, 'c', ring(2, 1))  6.52 us
    pallas_call x1, Pallas kernels, body(): call(late_kernel, (shape(2, ROWS, LANES), shape(2 * PAD, CH), shape(8, 12...  5.38 us
    ppermute x1, starting transfers between devices, body(): inner = lax.ppermute(edges, SP, pairs)  4.87 us
    ppermute x1, starting transfers between devices, body(): far_top = lax.ppermute(left[:HALF], 'tp', around)  4.85 us
    ppermute x1, starting transfers between devices, body(): left = lax.ppermute(out_grad, 'tp', beside)  4.16 us
    pallas_call x1, Pallas kernels, body(): call(backward_kernel, (shape(ROWS, CH, dtype=BF16), shape(ROWS, CH, dtype...  4.08 us
  transfers between devices with their start and end apart: 11, of which 5 were waited for; matrix products, arithmetic and copies ran while one was open for 0% of the time, Pallas kernels for 14%

profile of v11, /device:TPU:1, one launch (start us, length us, event | category | flops | bytes accessed | tf_op | source)
XLA Modules:
  0.0 89.2 jit_solution(13058955199532762111)
XLA Ops:
  0.7 4.2 %collective-permute-start = (bf16[1024,256]{1,0:T(8,128)(2,1)}, bf16[1024,256]{1,0:T(8,128)(2,1)S(1)}, u32[]{:S(2)}, u32[]{:S(2)}) collective-permute-start(bf16[1024,256]{1,0:T(8,128)(2,1)} %own.1), channel_id=1, source_target_pairs={{0,1},{1,0},{2,3},{3,2},{4,5},{5,4},{6,7},{7,6},{8,9},{9,8},{10,11... | collective-permute-start | bytes 1572872 | tf_op jit(solution)/shard_map/ppermute | solution.py:372
  4.8 3.8 %collective-permute-start.2 = (bf16[1024,256]{1,0:T(8,128)(2,1)}, bf16[1024,256]{1,0:T(8,128)(2,1)S(1)}, u32[]{:S(2)}, u32[]{:S(2)}) collective-permute-start(bf16[1024,256]{1,0:T(8,128)(2,1)} %own.1), channel_id=1, source_target_pairs={{0,3},{1,2},{2,1},{3,0},{4,7},{5,6},{6,5},{7,4},{8,11},{9,10},{10,... | collective-permute-start | bytes 1572872 | tf_op jit(solution)/shard_map/ppermute | solution.py:373
  8.6 1.4 %edges.1 = bf16[32,256]{1,0:T(8,128)(2,1)} custom-call(bf16[1024,256]{1,0:T(8,128)(2,1)} %value.3, bf16[1024,256]{1,0:T(8,128)(2,1)} %gate.3, bf16[1024,256]{1,0:T(8,128)(2,1)} %value.3, bf16[1024,256]{1,0:T(8,128)(2,1)} %gate.3), custom_call_target="tpu_custom_call" | custom-call | tf_op jit(solution)/shard_map/edges/pallas_call | solution.py:362
  10.0 4.9 %collective-permute-start.4 = (bf16[32,256]{1,0:T(8,128)(2,1)}, bf16[32,256]{1,0:T(8,128)(2,1)S(1)}, u32[]{:S(2)}, u32[]{:S(2)}) collective-permute-start(bf16[32,256]{1,0:T(8,128)(2,1)} %edges.1), channel_id=1, source_target_pairs={{0,4},{4,0},{8,12},{12,8},{16,20},{20,16},{24,28},{28,24},{32,36},... | collective-permute-start | bytes 49160 | tf_op jit(solution)/shard_map/ppermute | solution.py:374
  14.9 1.9 %collective-permute-start.5 = (bf16[32,256]{1,0:T(8,128)(2,1)}, bf16[32,256]{1,0:T(8,128)(2,1)S(1)}, u32[]{:S(2)}, u32[]{:S(2)}) collective-permute-start(bf16[32,256]{1,0:T(8,128)(2,1)} %edges.1), channel_id=1, source_target_pairs={{4,8},{12,16},{20,24},{28,32},{36,40},{44,48},{52,56},{60,64},{68,... | collective-permute-start | bytes 49160 | tf_op jit(solution)/shard_map/ppermute | solution.py:375
  16.9 3.0 %shard_map.101 = (f32[2,1056,128]{2,1,0:T(8,128)S(1)}, f32[1024,256]{1,0:T(8,128)S(1)}) custom-call(bf16[1024,256]{1,0:T(8,128)(2,1)S(1)} %copy-done, bf16[1024,256]{1,0:T(8,128)(2,1)S(1)} %copy-done.1, bf16[31,256]{1,0:T(8,128)(2,1)S(1)} %copy-done.5), custom_call_target="tpu_custom_call" | custom-call | flops 800000000 | bytes 1048576 | tf_op jit(solution)/shard_map/pallas_call | solution.py:379
  19.8 0.6 collective-permute-done.5.outer
  20.5 2.3 %shard_map.102 = (f32[2,1056,128]{2,1,0:T(8,128)S(1)}, f32[1024,256]{1,0:T(8,128)S(1)}, f32[1024,256]{1,0:T(8,128)S(1)}, f32[1024,256]{1,0:T(8,128)S(1)}, bf16[1024,256]{1,0:T(8,128)(2,1)S(1)}) custom-call(bf16[32,256]{1,0:T(8,128)(2,1)S(1)} %collective-permute-done.4.inner, bf16[32,256]{1,0:T(8,128)(2,1)S(1)} %collective-permute-done.5.outer, ...), custom_call_target="tpu_custom_call" | custom-call | flops 600000000 | bytes 1048576 | tf_op jit(solution)/shard_map/pallas_call | solution.py:382
  22.8 4.9 %collective-permute-start.1 = (bf16[512,256]{1,0:T(8,128)(2,1)S(1)}, bf16[512,256]{1,0:T(8,128)(2,1)S(1)}, u32[]{:S(2)}, u32[]{:S(2)}) collective-permute-start(bf16[512,256]{1,0:T(8,128)(2,1)S(1)} %slice.8), channel_id=1, source_target_pairs={{0,3},{1,2},{2,1},{3,0},{4,7},{5,6},{6,5},{7,4},{8,11},{9,10},{10,... | collective-permute-start | bytes 786440 | tf_op jit(solution)/shard_map/ppermute | solution.py:376
  27.7 2.1 %collective-permute-start.3 = (bf16[512,256]{1,0:T(8,128)(2,1)S(1)}, bf16[512,256]{1,0:T(8,128)(2,1)S(1)}, u32[]{:S(2)}, u32[]{:S(2)}) collective-permute-start(bf16[512,256]{1,0:T(8,128)(2,1)S(1)} %slice.9), channel_id=1, source_target_pairs={{0,1},{1,0},{2,3},{3,2},{4,5},{5,4},{6,7},{7,6},{8,9},{9,8},{10,11... | collective-permute-start | bytes 786440 | tf_op jit(solution)/shard_map/ppermute | solution.py:377
  29.9 1.8 %shard_map.103 = (f32[1024,256]{1,0:T(8,128)S(1)}, bf16[8,6,8,256]{3,2,1,0:T(8,128)(2,1)S(1)}, bf16[8,6,8,256]{3,2,1,0:T(8,128)(2,1)S(1)}) custom-call(bf16[1024,256]{1,0:T(8,128)(2,1)S(1)} %copy-done.4, bf16[1024,256]{1,0:T(8,128)(2,1)S(1)} %collective-permute-done.left, bf16[1024,256]{1,0:T(8,128)(2,1)S(1)} %collective-permute-done.2.right, ...), custom_call_target="tpu_custom_call" | custom-call | flops 800000000 | bytes 1048576 | tf_op jit(solution)/shard_map/pallas_call | solution.py:397
  31.6 1.9 %collective-permute-start.6 = (bf16[8,6,8,256]{3,2,1,0:T(8,128)(2,1)S(1)}, bf16[8,6,8,256]{3,2,1,0:T(8,128)(2,1)S(1)}, u32[]{:S(2)}, u32[]{:S(2)}) collective-permute-start(bf16[8,6,8,256]{3,2,1,0:T(8,128)(2,1)S(1)} %get-tuple-element.36), channel_id=1, source_target_pairs={{0,4},{4,0},{8,12},{12,8},{16,20},{20,16},{24,28},{28,24},{32,36},... | collective-permute-start | bytes 589832 | tf_op jit(solution)/shard_map/ppermute | solution.py:401
  33.6 1.4 %collective-permute-done.6.taken = bf16[8,6,8,256]{3,2,1,0:T(8,128)(2,1)S(1)} collective-permute-done((bf16[8,6,8,256]{3,2,1,0:T(8,128)(2,1)S(1)}, bf16[8,6,8,256]{3,2,1,0:T(8,128)(2,1)S(1)}, u32[]{:S(2)}, u32[]{:S(2)}) %collective-permute-start.6) | collective-permute-done | bytes 196640 | tf_op jit(solution)/shard_map/ppermute | solution.py:401
  35.0 1.6 %collective-permute-done.3.far_bottom = bf16[512,256]{1,0:T(8,128)(2,1)S(1)} collective-permute-done((bf16[512,256]{1,0:T(8,128)(2,1)S(1)}, bf16[512,256]{1,0:T(8,128)(2,1)S(1)}, u32[]{:S(2)}, u32[]{:S(2)}) %collective-permute-start.3) | collective-permute-done | bytes 262176 | tf_op jit(solution)/shard_map/ppermute | solution.py:377
  36.5 5.4 %shard_map.104 = (f32[2,1024,128]{2,1,0:T(8,128)S(1)}, f32[32,256]{1,0:T(8,128)S(1)}, bf16[8,12,8,256]{3,2,1,0:T(8,128)(2,1)S(1)}) custom-call(bf16[512,256]{1,0:T(8,128)(2,1)S(1)} %collective-permute-done.1.far_top, bf16[512,256]{1,0:T(8,128)(2,1)S(1)} %collective-permute-done.3.far_bottom, bf16[1024,256]{1,0:T(8,128)(2,1)S(1)} %copy-done.2, ...), custom_call_target="tpu_custom_call" | custom-call | flops 1600000000 | bytes 1048576 | tf_op jit(solution)/shard_map/pallas_call | solution.py:403
  41.9 10.4 %all_to_all.10.late = bf16[8,12,8,256]{3,2,1,0:T(8,128)(2,1)S(1)} all-to-all(bf16[8,12,8,256]{3,2,1,0:T(8,128)(2,1)S(1)} %get-tuple-element.37), channel_id=1, replica_groups=mesh['z'=16,'x'=4,'c'=2,'tp'=4] {'x','c'}, dimensions={0} | all-to-all | bytes 786432 | tf_op jit(solution)/shard_map/all_to_all | solution.py:358
  52.3 0.7 shard_map.105
  53.0 14.9 %all-to-all-start.1 = ((bf16[16,3,8,256]{3,2,1,0:T(8,128)(2,1)}), bf16[16,3,8,256]{3,2,1,0:T(8,128)(2,1)S(1)}, u32[]{:S(2)}, u32[]{:S(2)}) async-start(bf16[16,3,8,256]{3,2,1,0:T(8,128)(2,1)} %shard_map.105), calls=%async_computation.1 | async-start | bytes 393216 | tf_op jit(solution)/shard_map/all_to_all | solution.py:358
  68.0 3.1 %collective-permute-start.7 = (f32[32,256]{1,0:T(8,128)S(1)}, f32[32,256]{1,0:T(8,128)S(1)}, u32[]{:S(2)}, u32[]{:S(2)}) collective-permute-start(f32[32,256]{1,0:T(8,128)S(1)} %get-tuple-element.39), channel_id=1, source_target_pairs={{0,4},{4,0},{8,12},{12,8},{16,20},{20,16},{24,28},{28,24},{32,36},... | collective-permute-start | bytes 98312 | tf_op jit(solution)/shard_map/ppermute | solution.py:419
  71.0 2.1 %collective-permute-start.8 = (f32[32,256]{1,0:T(8,128)S(1)}, f32[32,256]{1,0:T(8,128)S(1)}, u32[]{:S(2)}, u32[]{:S(2)}) collective-permute-start(f32[32,256]{1,0:T(8,128)S(1)} %get-tuple-element.39), channel_id=1, source_target_pairs={{4,8},{12,16},{20,24},{28,32},{36,40},{44,48},{52,56},{60,64},{68,... | collective-permute-start | bytes 98312 | tf_op jit(solution)/shard_map/ppermute | solution.py:420
  73.1 3.4 %collective-permute-done.8.outer = f32[32,256]{1,0:T(8,128)S(1)} collective-permute-done((f32[32,256]{1,0:T(8,128)S(1)}, f32[32,256]{1,0:T(8,128)S(1)}, u32[]{:S(2)}, u32[]{:S(2)}) %collective-permute-start.8) | collective-permute-done | bytes 32800 | tf_op jit(solution)/shard_map/ppermute | solution.py:420
  76.6 4.1 %shard_map.106 = (bf16[1024,256]{1,0:T(8,128)(2,1)}, bf16[1024,256]{1,0:T(8,128)(2,1)}) custom-call(bf16[1024,256]{1,0:T(8,128)(2,1)S(1)} %copy-done, bf16[1024,256]{1,0:T(8,128)(2,1)S(1)} %copy-done.1, f32[2,1024,128]{2,1,0:T(8,128)S(1)} %get-tuple-element.38.grad, f32[32,256]{1,0:T(8,128)S(1)} %collective-permute-done.7.inner, ...), custom_call_target="tpu_custom_call" | custom-call | flops 1200000000 | bytes 1048576 | tf_op jit(solution)/shard_map/pallas_call | solution.py:421
  81.3 6.5 %collective-permute-start.9 = (f32[16,256]{1,0:T(8,128)S(1)}, f32[16,256]{1,0:T(8,128)S(1)}, u32[]{:S(2)}, u32[]{:S(2)}) collective-permute-start(f32[16,256]{1,0:T(8,128)S(1)} %get-tuple-element.45.mine), channel_id=1, source_target_pairs={{0,4},{4,0},{1,5},{5,1},{2,6},{6,2},{3,7},{7,3},{8,12},{12,8},{9,1... | collective-permute-start | bytes 49160 | tf_op jit(solution)/shard_map/ppermute | solution.py:431
  87.8 0.8 collective-permute-done.9.other
  (22 shorter events, 1.3 us)
Async XLA Ops:
  0.6 16.2 %copy-start = (bf16[1024,256]{1,0:T(8,128)(2,1)S(1)}, bf16[1024,256]{1,0:T(8,128)(2,1)}, u32[]{:S(2)}) copy-start(bf16[1024,256]{1,0:T(8,128)(2,1)} %value.3) | copy-start | bytes 1572868
  0.6 16.2 %copy-start.1 = (bf16[1024,256]{1,0:T(8,128)(2,1)S(1)}, bf16[1024,256]{1,0:T(8,128)(2,1)}, u32[]{:S(2)}) copy-start(bf16[1024,256]{1,0:T(8,128)(2,1)} %gate.3) | copy-start | bytes 1572868
  0.7 16.2 %copy-start.5 = (bf16[31,256]{1,0:T(8,128)(2,1)S(1)}, bf16[31,256]{1,0:T(8,128)(2,1)}, u32[]{:S(2)}) copy-start(bf16[31,256]{1,0:T(8,128)(2,1)} %taps.5) | copy-start | bytes 47620
  0.7 22.1 %collective-permute-start = (bf16[1024,256]{1,0:T(8,128)(2,1)}, bf16[1024,256]{1,0:T(8,128)(2,1)S(1)}, u32[]{:S(2)}, u32[]{:S(2)}) collective-permute-start(bf16[1024,256]{1,0:T(8,128)(2,1)} %own.1), channel_id=1, source_target_pairs={{0,1},{1,0},{2,3},{3,2},{4,5},{5,4},{6,7},{7,6},{8,9},{9,8},{10,11... | collective-permute-start | bytes 1572872 | tf_op jit(solution)/shard_map/ppermute | solution.py:372
  4.8 22.8 %collective-permute-start.2 = (bf16[1024,256]{1,0:T(8,128)(2,1)}, bf16[1024,256]{1,0:T(8,128)(2,1)S(1)}, u32[]{:S(2)}, u32[]{:S(2)}) collective-permute-start(bf16[1024,256]{1,0:T(8,128)(2,1)} %own.1), channel_id=1, source_target_pairs={{0,3},{1,2},{2,1},{3,0},{4,7},{5,6},{6,5},{7,4},{8,11},{9,10},{10,... | collective-permute-start | bytes 1572872 | tf_op jit(solution)/shard_map/ppermute | solution.py:373
  10.0 10.4 %copy-start.3 = (f32[256]{0:T(256)S(1)}, f32[256]{0:T(256)}, u32[]{:S(2)}) copy-start(f32[256]{0:T(256)} %param.9) | copy-start | bytes 3076
  10.0 9.8 %collective-permute-start.4 = (bf16[32,256]{1,0:T(8,128)(2,1)}, bf16[32,256]{1,0:T(8,128)(2,1)S(1)}, u32[]{:S(2)}, u32[]{:S(2)}) collective-permute-start(bf16[32,256]{1,0:T(8,128)(2,1)} %edges.1), channel_id=1, source_target_pairs={{0,4},{4,0},{8,12},{12,8},{16,20},{20,16},{24,28},{28,24},{32,36},... | collective-permute-start | bytes 49160 | tf_op jit(solution)/shard_map/ppermute | solution.py:374
  14.9 5.6 %collective-permute-start.5 = (bf16[32,256]{1,0:T(8,128)(2,1)}, bf16[32,256]{1,0:T(8,128)(2,1)S(1)}, u32[]{:S(2)}, u32[]{:S(2)}) collective-permute-start(bf16[32,256]{1,0:T(8,128)(2,1)} %edges.1), channel_id=1, source_target_pairs={{4,8},{12,16},{20,24},{28,32},{36,40},{44,48},{52,56},{60,64},{68,... | collective-permute-start | bytes 49160 | tf_op jit(solution)/shard_map/ppermute | solution.py:375
  20.5 9.4 %copy-start.2 = (bf16[1024,256]{1,0:T(8,128)(2,1)S(1)}, bf16[1024,256]{1,0:T(8,128)(2,1)}, u32[]{:S(2)}) copy-start(bf16[1024,256]{1,0:T(8,128)(2,1)} %weight.3) | copy-start | bytes 1572868
  20.5 9.4 %copy-start.4 = (bf16[1024,256]{1,0:T(8,128)(2,1)S(1)}, bf16[1024,256]{1,0:T(8,128)(2,1)}, u32[]{:S(2)}) copy-start(bf16[1024,256]{1,0:T(8,128)(2,1)} %own.1) | copy-start | bytes 1572868
  22.8 12.2 %collective-permute-start.1 = (bf16[512,256]{1,0:T(8,128)(2,1)S(1)}, bf16[512,256]{1,0:T(8,128)(2,1)S(1)}, u32[]{:S(2)}, u32[]{:S(2)}) collective-permute-start(bf16[512,256]{1,0:T(8,128)(2,1)S(1)} %slice.8), channel_id=1, source_target_pairs={{0,3},{1,2},{2,1},{3,0},{4,7},{5,6},{6,5},{7,4},{8,11},{9,10},{10,... | collective-permute-start | bytes 786440 | tf_op jit(solution)/shard_map/ppermute | solution.py:376
  27.7 8.8 %collective-permute-start.3 = (bf16[512,256]{1,0:T(8,128)(2,1)S(1)}, bf16[512,256]{1,0:T(8,128)(2,1)S(1)}, u32[]{:S(2)}, u32[]{:S(2)}) collective-permute-start(bf16[512,256]{1,0:T(8,128)(2,1)S(1)} %slice.9), channel_id=1, source_target_pairs={{0,1},{1,0},{2,3},{3,2},{4,5},{5,4},{6,7},{7,6},{8,9},{9,8},{10,11... | collective-permute-start | bytes 786440 | tf_op jit(solution)/shard_map/ppermute | solution.py:377
  31.6 3.3 %collective-permute-start.6 = (bf16[8,6,8,256]{3,2,1,0:T(8,128)(2,1)S(1)}, bf16[8,6,8,256]{3,2,1,0:T(8,128)(2,1)S(1)}, u32[]{:S(2)}, u32[]{:S(2)}) collective-permute-start(bf16[8,6,8,256]{3,2,1,0:T(8,128)(2,1)S(1)} %get-tuple-element.36), channel_id=1, source_target_pairs={{0,4},{4,0},{8,12},{12,8},{16,20},{20,16},{24,28},{28,24},{32,36},... | collective-permute-start | bytes 589832 | tf_op jit(solution)/shard_map/ppermute | solution.py:401
  53.0 27.6 %all-to-all-start.1 = ((bf16[16,3,8,256]{3,2,1,0:T(8,128)(2,1)}), bf16[16,3,8,256]{3,2,1,0:T(8,128)(2,1)S(1)}, u32[]{:S(2)}, u32[]{:S(2)}) async-start(bf16[16,3,8,256]{3,2,1,0:T(8,128)(2,1)} %shard_map.105), calls=%async_computation.1 | async-start | bytes 393216 | tf_op jit(solution)/shard_map/all_to_all | solution.py:358
  68.0 5.2 %collective-permute-start.7 = (f32[32,256]{1,0:T(8,128)S(1)}, f32[32,256]{1,0:T(8,128)S(1)}, u32[]{:S(2)}, u32[]{:S(2)}) collective-permute-start(f32[32,256]{1,0:T(8,128)S(1)} %get-tuple-element.39), channel_id=1, source_target_pairs={{0,4},{4,0},{8,12},{12,8},{16,20},{20,16},{24,28},{28,24},{32,36},... | collective-permute-start | bytes 98312 | tf_op jit(solution)/shard_map/ppermute | solution.py:419
  71.0 5.5 %collective-permute-start.8 = (f32[32,256]{1,0:T(8,128)S(1)}, f32[32,256]{1,0:T(8,128)S(1)}, u32[]{:S(2)}, u32[]{:S(2)}) collective-permute-start(f32[32,256]{1,0:T(8,128)S(1)} %get-tuple-element.39), channel_id=1, source_target_pairs={{4,8},{12,16},{20,24},{28,32},{36,40},{44,48},{52,56},{60,64},{68,... | collective-permute-start | bytes 98312 | tf_op jit(solution)/shard_map/ppermute | solution.py:420
  81.3 7.3 %collective-permute-start.9 = (f32[16,256]{1,0:T(8,128)S(1)}, f32[16,256]{1,0:T(8,128)S(1)}, u32[]{:S(2)}, u32[]{:S(2)}) collective-permute-start(f32[16,256]{1,0:T(8,128)S(1)} %get-tuple-element.45.mine), channel_id=1, source_target_pairs={{0,4},{4,0},{1,5},{5,1},{2,6},{6,2},{3,7},{7,3},{8,12},{12,8},{9,1... | collective-permute-start | bytes 49160 | tf_op jit(solution)/shard_map/ppermute | solution.py:431

commit v12 on v11

--- a/solution.py
+++ b/solution.py
@@ -31,6 +31,10 @@
     return jnp.dot(high, avg, preferred_element_type=F32) + jnp.dot(
         low, avg, preferred_element_type=F32
     )
+
+
+def rounded_mean(x, avg):
+    return jnp.dot(x.astype(BF16), avg, preferred_element_type=F32)
 
 
 def averaging():
@@ -128,7 +132,7 @@
     def norm_rows(start, raw):
         rows = pl.ds(start, CHUNK)
         centred = raw - group_mean(raw, avg)
-        scale = lax.rsqrt(group_mean(centred * centred, avg) + EPS)
+        scale = lax.rsqrt(rounded_mean(centred * centred, avg) + EPS)
         unit_rows = centred * scale
         pre = unit_rows * gain_row
         s = jax.nn.sigmoid(pre)
@@ -196,7 +200,7 @@
         hat = act * gain_row
         hat_unit = au * gain_row
         rows_grad = inv[rows, :] * (
-            hat - group_mean(hat, avg) - u * group_mean(hat_unit, avg)
+            hat - group_mean(hat, avg) - u * rounded_mean(hat_unit, avg)
         )
         for b in range(2):
             grad[b, rows, :] = rows_grad[:, b * LANES : (b + 1) * LANES]

time: 89.8 us -> 89.3 us (level)
  no operation moved by 1% of the time
where the time goes in v12:
time: 89.3 us; the launch traced here: 88.7 us
  starting transfers between devices  50.2 us (56%)
  Pallas kernels  19.3 us (22%)
  blocking collectives  10.4 us (12%)
  waiting for transfers between devices  7.85 us (9%)
    all_to_all x1, starting transfers between devices, exchange(): return lax.all_to_all(array, axis, 0, 0, tiled=True)  14.9 us
    all_to_all x1, blocking collectives, exchange(): return lax.all_to_all(array, axis, 0, 0, tiled=True)  10.4 us
    ppermute x1, starting transfers between devices, body(): other = lax.ppermute(mine, 'c', ring(2, 1))  6.52 us
    pallas_call x1, Pallas kernels, body(): call(late_kernel, (shape(2, ROWS, LANES), shape(2 * PAD, CH), shape(8, 12...  5.2 us
    ppermute x1, starting transfers between devices, body(): inner = lax.ppermute(edges, SP, pairs)  4.87 us
    ppermute x1, starting transfers between devices, body(): far_top = lax.ppermute(left[:HALF], 'tp', around)  4.85 us
    ppermute x1, starting transfers between devices, body(): left = lax.ppermute(out_grad, 'tp', beside)  4.16 us
    pallas_call x1, Pallas kernels, body(): call(backward_kernel, (shape(ROWS, CH, dtype=BF16), shape(ROWS, CH, dtype...  4.08 us
  transfers between devices with their start and end apart: 11, of which 5 were waited for; matrix products, arithmetic and copies ran while one was open for 0% of the time, Pallas kernels for 14%

profile of v12, /device:TPU:1, one launch (start us, length us, event | category | flops | bytes accessed | tf_op | source)
XLA Modules:
  0.0 88.7 jit_solution(17406721336951635676)
XLA Ops:
  0.7 4.2 %collective-permute-start = (bf16[1024,256]{1,0:T(8,128)(2,1)}, bf16[1024,256]{1,0:T(8,128)(2,1)S(1)}, u32[]{:S(2)}, u32[]{:S(2)}) collective-permute-start(bf16[1024,256]{1,0:T(8,128)(2,1)} %own.1), channel_id=1, source_target_pairs={{0,1},{1,0},{2,3},{3,2},{4,5},{5,4},{6,7},{7,6},{8,9},{9,8},{10,11... | collective-permute-start | bytes 1572872 | tf_op jit(solution)/shard_map/ppermute | solution.py:376
  4.8 3.8 %collective-permute-start.2 = (bf16[1024,256]{1,0:T(8,128)(2,1)}, bf16[1024,256]{1,0:T(8,128)(2,1)S(1)}, u32[]{:S(2)}, u32[]{:S(2)}) collective-permute-start(bf16[1024,256]{1,0:T(8,128)(2,1)} %own.1), channel_id=1, source_target_pairs={{0,3},{1,2},{2,1},{3,0},{4,7},{5,6},{6,5},{7,4},{8,11},{9,10},{10,... | collective-permute-start | bytes 1572872 | tf_op jit(solution)/shard_map/ppermute | solution.py:377
  8.6 1.4 %edges.1 = bf16[32,256]{1,0:T(8,128)(2,1)} custom-call(bf16[1024,256]{1,0:T(8,128)(2,1)} %value.3, bf16[1024,256]{1,0:T(8,128)(2,1)} %gate.3, bf16[1024,256]{1,0:T(8,128)(2,1)} %value.3, bf16[1024,256]{1,0:T(8,128)(2,1)} %gate.3), custom_call_target="tpu_custom_call" | custom-call | tf_op jit(solution)/shard_map/edges/pallas_call | solution.py:366
  10.0 4.9 %collective-permute-start.4 = (bf16[32,256]{1,0:T(8,128)(2,1)}, bf16[32,256]{1,0:T(8,128)(2,1)S(1)}, u32[]{:S(2)}, u32[]{:S(2)}) collective-permute-start(bf16[32,256]{1,0:T(8,128)(2,1)} %edges.1), channel_id=1, source_target_pairs={{0,4},{4,0},{8,12},{12,8},{16,20},{20,16},{24,28},{28,24},{32,36},... | collective-permute-start | bytes 49160 | tf_op jit(solution)/shard_map/ppermute | solution.py:378
  14.9 1.9 %collective-permute-start.5 = (bf16[32,256]{1,0:T(8,128)(2,1)}, bf16[32,256]{1,0:T(8,128)(2,1)S(1)}, u32[]{:S(2)}, u32[]{:S(2)}) collective-permute-start(bf16[32,256]{1,0:T(8,128)(2,1)} %edges.1), channel_id=1, source_target_pairs={{4,8},{12,16},{20,24},{28,32},{36,40},{44,48},{52,56},{60,64},{68,... | collective-permute-start | bytes 49160 | tf_op jit(solution)/shard_map/ppermute | solution.py:379
  16.9 3.0 %shard_map.101 = (f32[2,1056,128]{2,1,0:T(8,128)S(1)}, f32[1024,256]{1,0:T(8,128)S(1)}) custom-call(bf16[1024,256]{1,0:T(8,128)(2,1)S(1)} %copy-done, bf16[1024,256]{1,0:T(8,128)(2,1)S(1)} %copy-done.1, bf16[31,256]{1,0:T(8,128)(2,1)S(1)} %copy-done.5), custom_call_target="tpu_custom_call" | custom-call | flops 800000000 | bytes 1048576 | tf_op jit(solution)/shard_map/pallas_call | solution.py:383
  19.8 0.6 collective-permute-done.5.outer
  20.5 2.0 %shard_map.102 = (f32[2,1056,128]{2,1,0:T(8,128)S(1)}, f32[1024,256]{1,0:T(8,128)S(1)}, f32[1024,256]{1,0:T(8,128)S(1)}, f32[1024,256]{1,0:T(8,128)S(1)}, bf16[1024,256]{1,0:T(8,128)(2,1)S(1)}) custom-call(bf16[32,256]{1,0:T(8,128)(2,1)S(1)} %collective-permute-done.4.inner, bf16[32,256]{1,0:T(8,128)(2,1)S(1)} %collective-permute-done.5.outer, ...), custom_call_target="tpu_custom_call" | custom-call | flops 600000000 | bytes 1048576 | tf_op jit(solution)/shard_map/pallas_call | solution.py:386
  22.5 4.8 %collective-permute-start.1 = (bf16[512,256]{1,0:T(8,128)(2,1)S(1)}, bf16[512,256]{1,0:T(8,128)(2,1)S(1)}, u32[]{:S(2)}, u32[]{:S(2)}) collective-permute-start(bf16[512,256]{1,0:T(8,128)(2,1)S(1)} %slice.8), channel_id=1, source_target_pairs={{0,3},{1,2},{2,1},{3,0},{4,7},{5,6},{6,5},{7,4},{8,11},{9,10},{10,... | collective-permute-start | bytes 786440 | tf_op jit(solution)/shard_map/ppermute | solution.py:380
  27.4 2.1 %collective-permute-start.3 = (bf16[512,256]{1,0:T(8,128)(2,1)S(1)}, bf16[512,256]{1,0:T(8,128)(2,1)S(1)}, u32[]{:S(2)}, u32[]{:S(2)}) collective-permute-start(bf16[512,256]{1,0:T(8,128)(2,1)S(1)} %slice.9), channel_id=1, source_target_pairs={{0,1},{1,0},{2,3},{3,2},{4,5},{5,4},{6,7},{7,6},{8,9},{9,8},{10,11... | collective-permute-start | bytes 786440 | tf_op jit(solution)/shard_map/ppermute | solution.py:381
  29.5 1.8 %shard_map.103 = (f32[1024,256]{1,0:T(8,128)S(1)}, bf16[8,6,8,256]{3,2,1,0:T(8,128)(2,1)S(1)}, bf16[8,6,8,256]{3,2,1,0:T(8,128)(2,1)S(1)}) custom-call(bf16[1024,256]{1,0:T(8,128)(2,1)S(1)} %copy-done.4, bf16[1024,256]{1,0:T(8,128)(2,1)S(1)} %collective-permute-done.left, bf16[1024,256]{1,0:T(8,128)(2,1)S(1)} %collective-permute-done.2.right, ...), custom_call_target="tpu_custom_call" | custom-call | flops 800000000 | bytes 1048576 | tf_op jit(solution)/shard_map/pallas_call | solution.py:401
  31.3 1.9 %collective-permute-start.6 = (bf16[8,6,8,256]{3,2,1,0:T(8,128)(2,1)S(1)}, bf16[8,6,8,256]{3,2,1,0:T(8,128)(2,1)S(1)}, u32[]{:S(2)}, u32[]{:S(2)}) collective-permute-start(bf16[8,6,8,256]{3,2,1,0:T(8,128)(2,1)S(1)} %get-tuple-element.36), channel_id=1, source_target_pairs={{0,4},{4,0},{8,12},{12,8},{16,20},{20,16},{24,28},{28,24},{32,36},... | collective-permute-start | bytes 589832 | tf_op jit(solution)/shard_map/ppermute | solution.py:405
  33.2 1.4 %collective-permute-done.6.taken = bf16[8,6,8,256]{3,2,1,0:T(8,128)(2,1)S(1)} collective-permute-done((bf16[8,6,8,256]{3,2,1,0:T(8,128)(2,1)S(1)}, bf16[8,6,8,256]{3,2,1,0:T(8,128)(2,1)S(1)}, u32[]{:S(2)}, u32[]{:S(2)}) %collective-permute-start.6) | collective-permute-done | bytes 196640 | tf_op jit(solution)/shard_map/ppermute | solution.py:405
  34.6 1.6 %collective-permute-done.3.far_bottom = bf16[512,256]{1,0:T(8,128)(2,1)S(1)} collective-permute-done((bf16[512,256]{1,0:T(8,128)(2,1)S(1)}, bf16[512,256]{1,0:T(8,128)(2,1)S(1)}, u32[]{:S(2)}, u32[]{:S(2)}) %collective-permute-start.3) | collective-permute-done | bytes 262176 | tf_op jit(solution)/shard_map/ppermute | solution.py:381
  36.2 5.2 %shard_map.104 = (f32[2,1024,128]{2,1,0:T(8,128)S(1)}, f32[32,256]{1,0:T(8,128)S(1)}, bf16[8,12,8,256]{3,2,1,0:T(8,128)(2,1)S(1)}) custom-call(bf16[512,256]{1,0:T(8,128)(2,1)S(1)} %collective-permute-done.1.far_top, bf16[512,256]{1,0:T(8,128)(2,1)S(1)} %collective-permute-done.3.far_bottom, bf16[1024,256]{1,0:T(8,128)(2,1)S(1)} %copy-done.2, ...), custom_call_target="tpu_custom_call" | custom-call | flops 1600000000 | bytes 1048576 | tf_op jit(solution)/shard_map/pallas_call | solution.py:407
  41.4 10.4 %all_to_all.10.late = bf16[8,12,8,256]{3,2,1,0:T(8,128)(2,1)S(1)} all-to-all(bf16[8,12,8,256]{3,2,1,0:T(8,128)(2,1)S(1)} %get-tuple-element.37), channel_id=1, replica_groups=mesh['z'=16,'x'=4,'c'=2,'tp'=4] {'x','c'}, dimensions={0} | all-to-all | bytes 786432 | tf_op jit(solution)/shard_map/all_to_all | solution.py:362
  51.8 0.7 shard_map.105
  52.5 14.9 %all-to-all-start.1 = ((bf16[16,3,8,256]{3,2,1,0:T(8,128)(2,1)}), bf16[16,3,8,256]{3,2,1,0:T(8,128)(2,1)S(1)}, u32[]{:S(2)}, u32[]{:S(2)}) async-start(bf16[16,3,8,256]{3,2,1,0:T(8,128)(2,1)} %shard_map.105), calls=%async_computation.1 | async-start | bytes 393216 | tf_op jit(solution)/shard_map/all_to_all | solution.py:362
  67.5 3.1 %collective-permute-start.7 = (f32[32,256]{1,0:T(8,128)S(1)}, f32[32,256]{1,0:T(8,128)S(1)}, u32[]{:S(2)}, u32[]{:S(2)}) collective-permute-start(f32[32,256]{1,0:T(8,128)S(1)} %get-tuple-element.39), channel_id=1, source_target_pairs={{0,4},{4,0},{8,12},{12,8},{16,20},{20,16},{24,28},{28,24},{32,36},... | collective-permute-start | bytes 98312 | tf_op jit(solution)/shard_map/ppermute | solution.py:423
  70.5 2.1 %collective-permute-start.8 = (f32[32,256]{1,0:T(8,128)S(1)}, f32[32,256]{1,0:T(8,128)S(1)}, u32[]{:S(2)}, u32[]{:S(2)}) collective-permute-start(f32[32,256]{1,0:T(8,128)S(1)} %get-tuple-element.39), channel_id=1, source_target_pairs={{4,8},{12,16},{20,24},{28,32},{36,40},{44,48},{52,56},{60,64},{68,... | collective-permute-start | bytes 98312 | tf_op jit(solution)/shard_map/ppermute | solution.py:424
  72.6 3.4 %collective-permute-done.8.outer = f32[32,256]{1,0:T(8,128)S(1)} collective-permute-done((f32[32,256]{1,0:T(8,128)S(1)}, f32[32,256]{1,0:T(8,128)S(1)}, u32[]{:S(2)}, u32[]{:S(2)}) %collective-permute-start.8) | collective-permute-done | bytes 32800 | tf_op jit(solution)/shard_map/ppermute | solution.py:424
  76.0 4.1 %shard_map.106 = (bf16[1024,256]{1,0:T(8,128)(2,1)}, bf16[1024,256]{1,0:T(8,128)(2,1)}) custom-call(bf16[1024,256]{1,0:T(8,128)(2,1)S(1)} %copy-done, bf16[1024,256]{1,0:T(8,128)(2,1)S(1)} %copy-done.1, f32[2,1024,128]{2,1,0:T(8,128)S(1)} %get-tuple-element.38.grad, f32[32,256]{1,0:T(8,128)S(1)} %collective-permute-done.7.inner, ...), custom_call_target="tpu_custom_call" | custom-call | flops 1200000000 | bytes 1048576 | tf_op jit(solution)/shard_map/pallas_call | solution.py:425
  80.7 6.5 %collective-permute-start.9 = (f32[16,256]{1,0:T(8,128)S(1)}, f32[16,256]{1,0:T(8,128)S(1)}, u32[]{:S(2)}, u32[]{:S(2)}) collective-permute-start(f32[16,256]{1,0:T(8,128)S(1)} %get-tuple-element.45.mine), channel_id=1, source_target_pairs={{0,4},{4,0},{1,5},{5,1},{2,6},{6,2},{3,7},{7,3},{8,12},{12,8},{9,1... | collective-permute-start | bytes 49160 | tf_op jit(solution)/shard_map/ppermute | solution.py:435
  87.3 0.8 collective-permute-done.9.other
  (22 shorter events, 1.3 us)
Async XLA Ops:
  0.6 16.2 %copy-start = (bf16[1024,256]{1,0:T(8,128)(2,1)S(1)}, bf16[1024,256]{1,0:T(8,128)(2,1)}, u32[]{:S(2)}) copy-start(bf16[1024,256]{1,0:T(8,128)(2,1)} %value.3) | copy-start | bytes 1572868
  0.6 16.2 %copy-start.1 = (bf16[1024,256]{1,0:T(8,128)(2,1)S(1)}, bf16[1024,256]{1,0:T(8,128)(2,1)}, u32[]{:S(2)}) copy-start(bf16[1024,256]{1,0:T(8,128)(2,1)} %gate.3) | copy-start | bytes 1572868
  0.7 16.2 %copy-start.5 = (bf16[31,256]{1,0:T(8,128)(2,1)S(1)}, bf16[31,256]{1,0:T(8,128)(2,1)}, u32[]{:S(2)}) copy-start(bf16[31,256]{1,0:T(8,128)(2,1)} %taps.5) | copy-start | bytes 47620
  0.7 21.8 %collective-permute-start = (bf16[1024,256]{1,0:T(8,128)(2,1)}, bf16[1024,256]{1,0:T(8,128)(2,1)S(1)}, u32[]{:S(2)}, u32[]{:S(2)}) collective-permute-start(bf16[1024,256]{1,0:T(8,128)(2,1)} %own.1), channel_id=1, source_target_pairs={{0,1},{1,0},{2,3},{3,2},{4,5},{5,4},{6,7},{7,6},{8,9},{9,8},{10,11... | collective-permute-start | bytes 1572872 | tf_op jit(solution)/shard_map/ppermute | solution.py:376
  4.8 22.5 %collective-permute-start.2 = (bf16[1024,256]{1,0:T(8,128)(2,1)}, bf16[1024,256]{1,0:T(8,128)(2,1)S(1)}, u32[]{:S(2)}, u32[]{:S(2)}) collective-permute-start(bf16[1024,256]{1,0:T(8,128)(2,1)} %own.1), channel_id=1, source_target_pairs={{0,3},{1,2},{2,1},{3,0},{4,7},{5,6},{6,5},{7,4},{8,11},{9,10},{10,... | collective-permute-start | bytes 1572872 | tf_op jit(solution)/shard_map/ppermute | solution.py:377
  10.0 10.4 %copy-start.3 = (f32[256]{0:T(256)S(1)}, f32[256]{0:T(256)}, u32[]{:S(2)}) copy-start(f32[256]{0:T(256)} %param.9) | copy-start | bytes 3076
  10.0 9.8 %collective-permute-start.4 = (bf16[32,256]{1,0:T(8,128)(2,1)}, bf16[32,256]{1,0:T(8,128)(2,1)S(1)}, u32[]{:S(2)}, u32[]{:S(2)}) collective-permute-start(bf16[32,256]{1,0:T(8,128)(2,1)} %edges.1), channel_id=1, source_target_pairs={{0,4},{4,0},{8,12},{12,8},{16,20},{20,16},{24,28},{28,24},{32,36},... | collective-permute-start | bytes 49160 | tf_op jit(solution)/shard_map/ppermute | solution.py:378
  14.9 5.6 %collective-permute-start.5 = (bf16[32,256]{1,0:T(8,128)(2,1)}, bf16[32,256]{1,0:T(8,128)(2,1)S(1)}, u32[]{:S(2)}, u32[]{:S(2)}) collective-permute-start(bf16[32,256]{1,0:T(8,128)(2,1)} %edges.1), channel_id=1, source_target_pairs={{4,8},{12,16},{20,24},{28,32},{36,40},{44,48},{52,56},{60,64},{68,... | collective-permute-start | bytes 49160 | tf_op jit(solution)/shard_map/ppermute | solution.py:379
  20.5 9.0 %copy-start.2 = (bf16[1024,256]{1,0:T(8,128)(2,1)S(1)}, bf16[1024,256]{1,0:T(8,128)(2,1)}, u32[]{:S(2)}) copy-start(bf16[1024,256]{1,0:T(8,128)(2,1)} %weight.3) | copy-start | bytes 1572868
  20.5 9.1 %copy-start.4 = (bf16[1024,256]{1,0:T(8,128)(2,1)S(1)}, bf16[1024,256]{1,0:T(8,128)(2,1)}, u32[]{:S(2)}) copy-start(bf16[1024,256]{1,0:T(8,128)(2,1)} %own.1) | copy-start | bytes 1572868
  22.5 12.2 %collective-permute-start.1 = (bf16[512,256]{1,0:T(8,128)(2,1)S(1)}, bf16[512,256]{1,0:T(8,128)(2,1)S(1)}, u32[]{:S(2)}, u32[]{:S(2)}) collective-permute-start(bf16[512,256]{1,0:T(8,128)(2,1)S(1)} %slice.8), channel_id=1, source_target_pairs={{0,3},{1,2},{2,1},{3,0},{4,7},{5,6},{6,5},{7,4},{8,11},{9,10},{10,... | collective-permute-start | bytes 786440 | tf_op jit(solution)/shard_map/ppermute | solution.py:380
  27.4 8.8 %collective-permute-start.3 = (bf16[512,256]{1,0:T(8,128)(2,1)S(1)}, bf16[512,256]{1,0:T(8,128)(2,1)S(1)}, u32[]{:S(2)}, u32[]{:S(2)}) collective-permute-start(bf16[512,256]{1,0:T(8,128)(2,1)S(1)} %slice.9), channel_id=1, source_target_pairs={{0,1},{1,0},{2,3},{3,2},{4,5},{5,4},{6,7},{7,6},{8,9},{9,8},{10,11... | collective-permute-start | bytes 786440 | tf_op jit(solution)/shard_map/ppermute | solution.py:381
  31.3 3.3 %collective-permute-start.6 = (bf16[8,6,8,256]{3,2,1,0:T(8,128)(2,1)S(1)}, bf16[8,6,8,256]{3,2,1,0:T(8,128)(2,1)S(1)}, u32[]{:S(2)}, u32[]{:S(2)}) collective-permute-start(bf16[8,6,8,256]{3,2,1,0:T(8,128)(2,1)S(1)} %get-tuple-element.36), channel_id=1, source_target_pairs={{0,4},{4,0},{8,12},{12,8},{16,20},{20,16},{24,28},{28,24},{32,36},... | collective-permute-start | bytes 589832 | tf_op jit(solution)/shard_map/ppermute | solution.py:405
  52.5 27.6 %all-to-all-start.1 = ((bf16[16,3,8,256]{3,2,1,0:T(8,128)(2,1)}), bf16[16,3,8,256]{3,2,1,0:T(8,128)(2,1)S(1)}, u32[]{:S(2)}, u32[]{:S(2)}) async-start(bf16[16,3,8,256]{3,2,1,0:T(8,128)(2,1)} %shard_map.105), calls=%async_computation.1 | async-start | bytes 393216 | tf_op jit(solution)/shard_map/all_to_all | solution.py:362
  67.5 5.2 %collective-permute-start.7 = (f32[32,256]{1,0:T(8,128)S(1)}, f32[32,256]{1,0:T(8,128)S(1)}, u32[]{:S(2)}, u32[]{:S(2)}) collective-permute-start(f32[32,256]{1,0:T(8,128)S(1)} %get-tuple-element.39), channel_id=1, source_target_pairs={{0,4},{4,0},{8,12},{12,8},{16,20},{20,16},{24,28},{28,24},{32,36},... | collective-permute-start | bytes 98312 | tf_op jit(solution)/shard_map/ppermute | solution.py:423
  70.5 5.5 %collective-permute-start.8 = (f32[32,256]{1,0:T(8,128)S(1)}, f32[32,256]{1,0:T(8,128)S(1)}, u32[]{:S(2)}, u32[]{:S(2)}) collective-permute-start(f32[32,256]{1,0:T(8,128)S(1)} %get-tuple-element.39), channel_id=1, source_target_pairs={{4,8},{12,16},{20,24},{28,32},{36,40},{44,48},{52,56},{60,64},{68,... | collective-permute-start | bytes 98312 | tf_op jit(solution)/shard_map/ppermute | solution.py:424
  80.7 7.3 %collective-permute-start.9 = (f32[16,256]{1,0:T(8,128)S(1)}, f32[16,256]{1,0:T(8,128)S(1)}, u32[]{:S(2)}, u32[]{:S(2)}) collective-permute-start(f32[16,256]{1,0:T(8,128)S(1)} %get-tuple-element.45.mine), channel_id=1, source_target_pairs={{0,4},{4,0},{1,5},{5,1},{2,6},{6,2},{3,7},{7,3},{8,12},{12,8},{9,1... | collective-permute-start | bytes 49160 | tf_op jit(solution)/shard_map/ppermute | solution.py:435
